TPU v7x, 32 devices: a whole 2x2x4 slice. The times are simulated.
32 devices in a mesh: sp: 4 (over x, core), tp: 8 (over z, y).
Axes of the slice: x: 2, y: 2, z: 4, core: 2. Of those that a mesh axis runs over, the one named last changes fastest.
Arguments:
- latent: bfloat16 [512, 4096], P('sp', 'tp'), may hold values from -60 to 60
- context: bfloat16 [64, 4096], P('sp', 'tp'), may hold values from -6 to 6
- conditioning: bfloat16 [4096], P('sp'), may hold values from -6 to 6
- context_prompt_vector: bfloat16 [4096], P('sp'), may hold values from -6 to 6
- shift_matrix: bfloat16 [4096, 4096], P('tp', 'sp'), may hold values from -0.09375 to 0.09375
- scale_matrix: bfloat16 [4096, 4096], P('tp', 'sp'), may hold values from -0.09375 to 0.09375
- residual_gate_matrix: bfloat16 [4096, 4096], P('tp', 'sp'), may hold values from -0.09375 to 0.09375
- query_matrix: bfloat16 [2048, 4096], P('tp'), may hold values from -0.09375 to 0.09375
- key_matrix: bfloat16 [2048, 4096], P('tp'), may hold values from -0.09375 to 0.09375
- value_matrix: bfloat16 [4096, 4096], P('tp'), may hold values from -0.09375 to 0.09375
- gate_matrix: bfloat16 [4096, 4096], P('tp'), may hold values from -0.09375 to 0.09375
- decay_down_factor: bfloat16 [2, 4096, 16], replicated, may hold values from -0.09375 to 0.09375
- decay_up_factor: bfloat16 [2, 16, 2048], replicated, may hold values from -1.5 to 1.5
- decay_key_bias: float32 [2, 2048], replicated, may hold values from -0.5 to 7
- spike_log_decay: float32 [2, 512, 16], P(None, 'sp'), may hold values from -2.8 to 0
- output_gain: float32 [4096], P('tp'), may hold values from 0.1 to 1.9
- output_matrix: bfloat16 [4096, 4096], P('tp'), may hold values from -0.375 to 0.375
Outputs:
- mixed: bfloat16 [512, 4096], P('sp', 'tp')
All inputs are finite; a program needn't handle non-finite values.
Results may differ from a plain program's by a relative error of at most 0.013.
Values may be sent and summed in bfloat16 or wider, within the bound.
No kernel may reach another device: no remote copies, remote signals or barrier semaphores. Data moves between devices by JAX's collectives and lax.ppermute only.
A program may use at most 64 MiB of HBM per device.

v0:
```python
import functools

import jax
import jax.numpy as jnp
from jax import lax
from jax.experimental import pallas as pl
from jax.experimental.pallas import tpu as pltpu
from jax.sharding import PartitionSpec as P


D = 4096
HEADS = 16
DK = 128
DECAY_RANK = 16
BLK = 64
VGROUP = 64


epsilon = 1e-05
gate_norm = 16.0
precise = lax.Precision.HIGHEST


def for_sending(value):

    def short(part):
        return part.astype(jnp.bfloat16) if part.dtype == jnp.float32 else part

    return jax.tree.map(short, value)


def from_partner(value, axis, distance):
    return lax.ppermute(value, axis, [(i, i ^ 1 << distance) for i in range(lax.axis_size(axis))])


def carried_in(value, axis, combine, identity, reverse):
    peers, index = (lax.axis_size(axis), lax.axis_index(axis))
    everything = jax.tree.map(
        lambda part, kind: lax.all_gather(part.astype(kind), axis),
        value,
        (jnp.bfloat16, jnp.bfloat16),
    )
    start = jax.tree.map(
        lambda part, zero: jnp.broadcast_to(jnp.asarray(zero, part.dtype), part.shape),
        value,
        identity,
    )

    def turn(k, before):
        at = peers - 1 - k if reverse else k
        reached = at > index if reverse else at < index
        new = combine(
            before, jax.tree.map(lambda part, own: part[at].astype(own.dtype), everything, value)
        )
        return jax.tree.map(lambda a, b: jnp.where(reached, a, b), new, before)

    return lax.fori_loop(0, peers, turn, start)


def linear(rows, weight):
    return lax.dot_general(
        rows, weight, (((1,), (1,)), ((), ())), preferred_element_type=jnp.float32
    )


def modulated(rows, row_sum, row_squares, shift_vec, scale_vec):
    rows_f = rows.astype(jnp.float32)
    mean_val = row_sum / D
    variance = row_squares / D - mean_val * mean_val
    return (
        (rows_f - mean_val) * lax.rsqrt(variance + epsilon) * (1.0 + scale_vec) + shift_vec
    ).astype(jnp.bfloat16)


def reverse_rows(array):
    return jnp.flip(array, axis=0)


def end_state(key_rows, value_rows, log_decay):
    cumulative = jnp.cumsum(log_decay, axis=0)
    totals = cumulative[-1]
    weighted = key_rows * jnp.exp(totals - cumulative)
    return (jnp.exp(totals), jnp.einsum("nhd,nhe->hde", weighted, value_rows, precision=precise))


def combine(earlier, later):
    return (earlier[0] * later[0], later[0][..., None] * earlier[1] + later[1])


def blockwise(queries, key_rows, value_rows, log_decay, carried, block_len):
    length, head_count, _ = queries.shape
    value_width = value_rows.shape[-1]
    blocks = length // block_len

    def shaped(array):
        return array.reshape(blocks, block_len, head_count, array.shape[-1])

    triangle = jnp.tril(jnp.ones((block_len, block_len), jnp.float32))

    def advance(state_now, inputs):
        block_q, block_k, block_v, block_a = inputs
        cumulative = jnp.cumsum(block_a, axis=0)
        block_end = cumulative[-1]
        query_dec = block_q * jnp.exp(cumulative)
        scores = (
            jnp.einsum("ihd,jhd->hij", query_dec, block_k * jnp.exp(-cumulative), precision=precise)
            * triangle
        )
        result = jnp.einsum("hij,jhe->ihe", scores, block_v, precision=precise)
        result = result + jnp.einsum("ihd,hde->ihe", query_dec, state_now, precision=precise)
        state_next = state_now * jnp.exp(block_end)[:, :, None] + jnp.einsum(
            "jhd,jhe->hde", block_k * jnp.exp(block_end - cumulative), block_v, precision=precise
        )
        return (state_next, result)

    _, outputs = lax.scan(
        advance, carried, (shaped(queries), shaped(key_rows), shaped(value_rows), shaped(log_decay))
    )
    return outputs.reshape(length, head_count, value_width)


def head_channels(pieces, per_head, tp_index):
    for bit_number in range(per_head.bit_length() - 1):
        partner = from_partner(
            (for_sending(pieces[0]), for_sending(pieces[1]), for_sending(pieces[2])),
            "tp",
            bit_number,
        )
        upper = tp_index // (1 << bit_number) % 2 == 1
        pieces = tuple(
            (
                jnp.where(
                    upper,
                    jnp.concatenate([theirs, mine], axis=1),
                    jnp.concatenate([mine, theirs], axis=1),
                )
                for mine, theirs in zip(pieces, partner)
            )
        )
    return pieces


def context_totals(fwd_growth, fwd_state, bwd_growth, bwd_state, identity):

    def absorb(carried, piece):
        return (combine(carried, piece), None)

    total_fwd, _ = lax.scan(absorb, identity, (fwd_growth, fwd_state))
    total_bwd, _ = lax.scan(absorb, identity, (bwd_growth, bwd_state), reverse=True)
    return (total_fwd, total_bwd)


def stored(array):
    return lax.optimization_barrier(array.astype(jnp.bfloat16))


def local_general(
    latent,
    context,
    conditioning,
    context_prompt_vector,
    shift_matrix,
    scale_matrix,
    residual_gate_matrix,
    query_matrix,
    key_matrix,
    value_matrix,
    gate_matrix,
    decay_down_factor,
    decay_up_factor,
    decay_key_bias,
    spike_log_decay,
    output_gain,
    output_matrix,
):
    tp_count = lax.axis_size("tp")
    tp_index = lax.axis_index("tp")
    per_head = max(tp_count // HEADS, 1)
    heads_per_shard = max(HEADS // tp_count, 1)
    leading_head = tp_index // per_head * heads_per_shard
    tok_rows = latent.shape[0]
    conds = jax.nn.silu(
        jnp.stack([conditioning, context_prompt_vector]).astype(jnp.float32)
    ).astype(jnp.bfloat16)
    shifts, scales, gates = lax.psum(
        (
            linear(conds, shift_matrix),
            linear(conds, scale_matrix),
            linear(conds, residual_gate_matrix),
        ),
        "sp",
    )
    down_both = jnp.concatenate([decay_down_factor[0].T, decay_down_factor[1].T], axis=0)
    lat_weights = (query_matrix, key_matrix, value_matrix, gate_matrix, down_both)
    ctx_weights = (key_matrix, value_matrix, down_both)
    lat_f = latent.astype(jnp.float32)
    ctx_f = context.astype(jnp.float32)
    lat_sum, lat_squares, ctx_sum, ctx_squares = lax.psum(
        (
            jnp.sum(lat_f, axis=1, keepdims=True),
            jnp.sum(lat_f * lat_f, axis=1, keepdims=True),
            jnp.sum(ctx_f, axis=1, keepdims=True),
            jnp.sum(ctx_f * ctx_f, axis=1, keepdims=True),
        ),
        "tp",
    )
    latent_normalized = modulated(latent, lat_sum, lat_squares, shifts[0], scales[0])
    normed_ctx = modulated(context, ctx_sum, ctx_squares, shifts[1], scales[1])
    lat_piece = lax.all_gather(latent_normalized, "tp", axis=1, tiled=True)
    ctx_piece = lax.all_gather(normed_ctx, "tp", axis=1, tiled=True)
    lat_new = tuple((linear(lat_piece, weight) for weight in lat_weights))
    ctx_new = tuple((linear(ctx_piece, weight) for weight in ctx_weights))
    query_part, key_part, value_part, gate_part, low_rank_part = lat_new
    ctx_key_part, ctx_value_part, ctx_low = ctx_new
    query_full, key_full, ctx_key_full = head_channels(
        (stored(query_part), stored(key_part), stored(ctx_key_part)), per_head, tp_index
    )

    def split_heads(rows, width):
        return rows.astype(jnp.float32).reshape(rows.shape[0], heads_per_shard, width)

    value_cols = value_part.shape[1] // heads_per_shard
    queries = split_heads(query_full, DK) * DK ** (-0.5)
    key_rows = split_heads(key_full, DK)
    ctx_keys = split_heads(ctx_key_full, DK)
    values_lat = split_heads(stored(value_part), value_cols)
    values_ctx = split_heads(stored(ctx_value_part), value_cols)
    gate_rows = stored(gate_part).astype(jnp.float32)

    def per_head_decay(low_rows, direction):
        up_part = lax.dynamic_slice_in_dim(
            decay_up_factor[direction], leading_head * DK, heads_per_shard * DK, 1
        ).astype(jnp.float32)
        bias_part = lax.dynamic_slice_in_dim(
            decay_key_bias[direction], leading_head * DK, heads_per_shard * DK, 0
        )
        pre_act = jnp.dot(low_rows, up_part, precision=precise) + bias_part
        return (jax.nn.log_sigmoid(pre_act) / gate_norm).reshape(
            low_rows.shape[0], heads_per_shard, DK
        )

    decay_spikes = lax.dynamic_slice_in_dim(spike_log_decay, leading_head, heads_per_shard, 2)
    latent_forward = per_head_decay(low_rank_part[:, :DECAY_RANK], 0) + decay_spikes[0][:, :, None]
    latent_backward = per_head_decay(low_rank_part[:, DECAY_RANK:], 1) + decay_spikes[1][:, :, None]
    ctx_fwd = per_head_decay(ctx_low[:, :DECAY_RANK], 0)
    ctx_bwd = per_head_decay(ctx_low[:, DECAY_RANK:], 1)
    cf_growth, cf_state = end_state(ctx_keys, values_ctx, ctx_fwd)
    cb_growth, cb_state = end_state(
        reverse_rows(ctx_keys), reverse_rows(values_ctx), reverse_rows(ctx_bwd)
    )
    lf_growth, lf_state = end_state(key_rows, values_lat, latent_forward)
    lb_growth, lb_state = end_state(
        reverse_rows(key_rows), reverse_rows(values_lat), reverse_rows(latent_backward)
    )
    identity = (
        jnp.ones((heads_per_shard, DK), jnp.float32),
        jnp.zeros((heads_per_shard, DK, value_cols), jnp.float32),
    )
    ctx_gathered = (
        lax.all_gather(cf_growth[None].astype(jnp.bfloat16), "sp", axis=0, tiled=True).astype(
            jnp.float32
        ),
        lax.all_gather(cf_state[None].astype(jnp.bfloat16), "sp", axis=0, tiled=True).astype(
            jnp.float32
        ),
        lax.all_gather(cb_growth[None].astype(jnp.bfloat16), "sp", axis=0, tiled=True).astype(
            jnp.float32
        ),
        lax.all_gather(cb_state[None].astype(jnp.bfloat16), "sp", axis=0, tiled=True).astype(
            jnp.float32
        ),
    )
    total_fwd, total_bwd = context_totals(
        ctx_gathered[0], ctx_gathered[1], ctx_gathered[2], ctx_gathered[3], identity
    )
    prefix = carried_in((lf_growth, lf_state), "sp", combine, identity, False)
    suffix = carried_in((lb_growth, lb_state), "sp", combine, identity, True)
    start_fwd = combine(total_fwd, prefix)[1]
    start_bwd = combine(total_bwd, suffix)[1]
    zero_state = jnp.zeros((heads_per_shard, DK, value_cols), jnp.float32)

    def direction_out(query_rows, key_list, value_list, log_decay, start_state):
        local_part = blockwise(query_rows, key_list, value_list, log_decay, zero_state, BLK)
        reach = query_rows * jnp.exp(jnp.cumsum(log_decay, axis=0))
        return local_part + jnp.einsum("nhd,hde->nhe", reach, start_state, precision=precise)

    out_fwd = direction_out(queries, key_rows, values_lat, latent_forward, start_fwd)
    out_bwd = reverse_rows(
        direction_out(
            reverse_rows(queries),
            reverse_rows(key_rows),
            reverse_rows(values_lat),
            reverse_rows(latent_backward),
            start_bwd,
        )
    )
    grouped = (out_fwd + out_bwd).reshape(tok_rows, -1, VGROUP)
    grouped = grouped * lax.rsqrt(jnp.mean(grouped * grouped, axis=-1, keepdims=True) + epsilon)
    heads_out = (grouped.reshape(tok_rows, -1) * output_gain * jax.nn.silu(gate_rows)).astype(
        jnp.bfloat16
    )
    branch = linear(lax.all_gather(heads_out, "tp", axis=1, tiled=True), output_matrix)
    return (latent.astype(jnp.float32) + gates[0] * branch).astype(jnp.bfloat16)


VMEM_SPEC = pl.BlockSpec(memory_space=pltpu.VMEM)
HBM_SPEC = pl.BlockSpec(memory_space=pltpu.HBM)
NT = (((1,), (1,)), ((), ()))
NN = (((1,), (0,)), ((), ()))
TN = (((0,), (0,)), ((), ()))
f32 = jnp.float32
bf16 = jnp.bfloat16


def matmul(a, b, dims=NN):
    return lax.dot_general(a, b, dims, preferred_element_type=f32)


def halves(value):
    high = value.astype(bf16)
    return (high, (value - high.astype(f32)).astype(bf16))


def exchange(value, axis, distance):
    return lax.ppermute(value, axis, [(i, i ^ distance) for i in range(lax.axis_size(axis))])


def gather_plan(count):
    half = count // 2
    direct = dict.fromkeys(k for k in (half, 2, 1, count - 1) if k < count)
    plan = [(k, 0) for k in direct]
    for k in range(3, count):
        if k not in direct:
            plan.append((k, half if k & half else 2 if k == 3 else 0))
    return plan


def gathered_pieces(value, axis):
    pieces = {0: value}
    for k, source in gather_plan(lax.axis_size(axis)):
        pieces[k] = exchange(pieces[source], axis, k ^ source)
    return [pieces[k] for k in sorted(pieces)]


WIDE_GRANT = 63500
SURVEY_FLOPS = 15 * 10**9
SURVEY_BYTES = 40 * 10**6


def call(kernel, out_shapes, in_specs, args, flops, traffic, scratch=(), grant=24 << 10):
    single = not isinstance(out_shapes, (tuple, list))
    return pl.pallas_call(
        kernel,
        out_shape=out_shapes,
        in_specs=in_specs,
        out_specs=VMEM_SPEC if single else [VMEM_SPEC] * len(out_shapes),
        scratch_shapes=list(scratch),
        compiler_params=pltpu.CompilerParams(vmem_limit_bytes=grant << 10),
        cost_estimate=pl.CostEstimate(flops=flops, bytes_accessed=traffic, transcendentals=0),
    )(*args)


def fetch(sources, targets, sems):
    copies = [
        pltpu.make_async_copy(source, target, sems.at[n])
        for n, (source, target) in enumerate(zip(sources, targets))
    ]
    for copy in copies:
        copy.start()
    return copies


def modulation_kernel(*refs):
    sources = refs[:7]
    out, joined = refs[7:9]
    cond_ref, prompt_ref, *weights = refs[9:14]
    tokens = sources[5].shape[0]
    rows = (joined.at[pl.ds(0, tokens)], joined.at[pl.ds(tokens, sources[6].shape[0])])
    copies = fetch(sources, (cond_ref, prompt_ref, *weights, *rows), refs[14])

    def in_one_row(ref):
        block = ref[...].astype(f32)
        return jnp.concatenate([block[r : r + 1] for r in range(block.shape[0])], axis=1)

    copies[0].wait()
    cond = in_one_row(cond_ref)
    copies[1].wait()
    row = lax.broadcasted_iota(jnp.int32, (8, cond.shape[1]), 0)
    both = jnp.where(row % 2 == 0, cond, in_one_row(prompt_ref))
    conds = (both * jax.nn.sigmoid(both)).astype(bf16)
    products = []
    for copy, weight in zip(copies[2:5], weights):
        copy.wait()
        products.append(matmul(conds, weight[...], NT))
    shifts, scales, gates = products
    row_out = lax.broadcasted_iota(jnp.int32, out.shape, 0)
    out[...] = jnp.where(row_out < 2, shifts, jnp.where(row_out < 4, scales, gates))
    copies[5].wait()
    copies[6].wait()


def row_sums(pieces):
    total, width = pieces[0].shape
    sums = jnp.zeros((total, 128), f32)
    squares = jnp.zeros((total, 128), f32)
    for piece in pieces:
        for c in range(width // 128):
            x = piece[:, c * 128 : (c + 1) * 128].astype(f32)
            sums = sums + x
            squares = squares + x * x
    return (sums, squares)


def add_kernel(mine, theirs, *outs):
    total = mine[...] + theirs[...]
    for out in outs:
        out[...] = total[: out.shape[0]]


def join_kernel(*refs):
    at = 0
    for ref in refs[:-1]:
        refs[-1][at : at + ref.shape[0], :] = ref[...]
        at += ref.shape[0]


def survey_kernel(*refs):
    refs[-2][...], refs[-1][...] = row_sums(refs[:-2])


def block_masks(total, tokens, wanted):
    i = lax.broadcasted_iota(jnp.int32, (total, total), 0)
    j = lax.broadcasted_iota(jnp.int32, (total, total), 1)
    last = tokens // BLK
    bi = jnp.minimum(lax.shift_right_logical(i, BLK.bit_length() - 1), last)
    bj = jnp.minimum(lax.shift_right_logical(j, BLK.bit_length() - 1), last)
    return wanted(i, j, bi, bj)


def project_kernel(count, tokens, heads, surveyed, *refs):
    pieces = refs[:count]
    mods = refs[count : count + count.bit_length()]
    refs = refs[count + count.bit_length() :]
    down, key_w, value_w, early_sums, early_squares, spikes = refs[:6]
    normed, keys, values, cum_f, cum_b, payload = refs[8:14]
    up_own, bias_own, sems = refs[14:]
    tp = lax.axis_index("tp")
    half = heads * DK
    first = pl.multiple_of(tp * half, half)
    sources = (refs[6].at[:, :, pl.ds(first, half)], refs[7].at[:, pl.ds(first, half)])
    copies = fetch(sources, (up_own, bias_own), sems)
    total, width = pieces[0].shape
    ctx = total - tokens
    features = width * count

    def mod_row(k, row):
        level = k.bit_length()
        at = 4 * (k - (1 << level >> 1)) + row
        return mods[level][at : at + 1, :]

    sums, squares = row_sums([pieces[k] for k in range(count) if k not in surveyed])
    sums, squares = (sums + early_sums[...], squares + early_squares[...])
    mean = jnp.sum(sums, axis=1, keepdims=True) / features
    variance = jnp.sum(squares, axis=1, keepdims=True) / features - mean * mean
    inverse = lax.rsqrt(variance + epsilon)
    for k, piece in enumerate(pieces):
        column = pl.multiple_of(lax.bitwise_xor(tp, k) * width, width)
        scaled = (piece[...].astype(f32) - mean) * inverse
        ahead = scaled[:tokens] * (1.0 + mod_row(k, 2)) + mod_row(k, 0)
        context = scaled[tokens:] * (1.0 + mod_row(k, 3)) + mod_row(k, 1)
        normed[:tokens, pl.ds(column, width)] = ahead.astype(bf16)
        normed[tokens:, pl.ds(column, width)] = context.astype(bf16)
    low_high, low_low = halves(matmul(normed[...], down[...], NT))
    for copy in copies:
        copy.wait()
    blank = jnp.zeros((DECAY_RANK, half), bf16)
    up = jnp.concatenate(
        [
            jnp.concatenate([up_own[0], blank], axis=1),
            jnp.concatenate([blank, up_own[1]], axis=1),
        ],
        axis=0,
    )
    bias = jnp.concatenate([bias_own[0:1, :], bias_own[1:2, :]], axis=1)
    pre = matmul(low_high, up) + matmul(low_low, up) + bias
    decay = (jnp.minimum(pre, 0.0) - jnp.log1p(jnp.exp(-jnp.abs(pre)))) * (1.0 / gate_norm)
    row = lax.broadcasted_iota(jnp.int32, (spikes.shape[1], half), 0)
    head = lax.shift_right_logical(
        lax.broadcasted_iota(jnp.int32, (spikes.shape[1], half), 1), DK.bit_length() - 1
    )
    wanted = jnp.where(row == head + tp * heads, 1.0, 0.0).astype(bf16)
    marks = []
    for d in range(2):
        spike_high, spike_low = halves(spikes[d])
        added = matmul(spike_high, wanted, TN) + matmul(spike_low, wanted, TN)
        marks.append(decay[:tokens, d * half : (d + 1) * half] + added)
    decay = jnp.concatenate([jnp.concatenate(marks, axis=1), decay[tokens:]], axis=0)
    ones = jnp.ones((total, total), f32)
    zeros = jnp.zeros((total, total), f32)
    lower = block_masks(
        total, tokens, lambda i, j, bi, bj: jnp.where((bi == bj) & (i >= j), ones, zeros)
    ).astype(bf16)
    upper = block_masks(
        total, tokens, lambda i, j, bi, bj: jnp.where((bi == bj) & (i <= j), ones, zeros)
    ).astype(bf16)
    high, low = halves(decay)
    cf = matmul(lower, high[:, :half]) + matmul(lower, low[:, :half])
    cb = matmul(upper, high[:, half:]) + matmul(upper, low[:, half:])
    cum_f[...] = cf[:tokens]
    cum_b[...] = cb[:tokens]
    key_all = matmul(normed[...], key_w[...], NT).astype(bf16)
    keys[...] = key_all[:tokens]
    value_all = matmul(normed[...], value_w[...], NT).astype(bf16)
    values[...] = value_all[:tokens]
    wide = value_all.shape[1] // heads
    blocks = tokens // BLK
    size = heads * wide
    growth = [[], [], [], []]
    start = 2 * size + growth_rows(heads)
    for h in range(heads):
        own = slice(h * DK, (h + 1) * DK)
        kh = key_all[:, own].astype(f32)
        vh = value_all[:tokens, h * wide : (h + 1) * wide]
        cfh, cbh = (cf[:, own], cb[:, own])
        ends_f = [cfh[(b + 1) * BLK - 1 : (b + 1) * BLK] for b in range(blocks)]
        ends_b = [cbh[b * BLK : b * BLK + 1] for b in range(blocks)]
        weighted_f, weighted_b = ([], [])
        for b in range(blocks):
            rows = slice(b * BLK, (b + 1) * BLK)
            weighted_f.append(kh[rows] * jnp.exp(sum(ends_f[b + 1 :], ends_f[b]) - cfh[rows]))
            weighted_b.append(kh[rows] * jnp.exp(sum(ends_b[:b], ends_b[b]) - cbh[rows]))
        kf = jnp.concatenate(weighted_f, axis=0).astype(bf16)
        kb = jnp.concatenate(weighted_b, axis=0).astype(bf16)
        payload[h * wide : (h + 1) * wide, :] = matmul(vh, kf, TN).astype(bf16)
        payload[size + h * wide : size + (h + 1) * wide, :] = matmul(vh, kb, TN).astype(bf16)
        growth[0].append(jnp.exp(sum(ends_f[1:], ends_f[0])))
        growth[1].append(jnp.exp(sum(ends_b[1:], ends_b[0])))
        end_f, end_b = (cfh[total - 1 : total], cbh[tokens : tokens + 1])
        growth[2].append(jnp.exp(end_f))
        growth[3].append(jnp.exp(end_b))
        at = start + h * ctx
        payload[at : at + ctx, :] = (kh[tokens:] * jnp.exp(end_f - cfh[tokens:])).astype(bf16)
        at = at + heads * ctx
        payload[at : at + ctx, :] = (kh[tokens:] * jnp.exp(end_b - cbh[tokens:])).astype(bf16)
    for c in range(size // DK):
        at = start + (2 * heads + c) * ctx
        payload[at : at + ctx, :] = value_all[tokens:, c * DK : (c + 1) * DK]
    payload[2 * size : start, :] = growth_block(growth, heads)


def growth_rows(heads):
    return -(-4 * heads // 16) * 16


def growth_block(growth, heads):
    rows = [row for kind in growth for row in kind]
    blank = jnp.zeros((growth_rows(heads) - len(rows), DK), f32)
    return jnp.concatenate([*rows, blank], axis=0).astype(bf16)


def growth_of(ref, at, kind, h, heads):
    block = ref[at : at + growth_rows(heads), :].astype(f32)
    return block[kind * heads + h : kind * heads + h + 1]


def within_kernel(
    heads,
    normed,
    query_w,
    gate_w,
    keys,
    values,
    cum_f,
    cum_b,
    gain,
    inside,
    reach_f,
    reach_b,
    gated,
):
    tokens = keys.shape[0]
    rows_in = normed[:tokens, :]
    query_all = matmul(rows_in, query_w[...], NT).astype(bf16).astype(f32) * DK ** (-0.5)
    wide = values.shape[1] // heads
    blocks = tokens // BLK

    def choose(i, j, bi, bj):
        same = bi == bj
        return (same & (i >= j), same & (i <= j), bi > bj, bi < bj)

    forward, backward, later, sooner = block_masks(tokens, tokens, choose)
    for h in range(heads):
        own = slice(h * DK, (h + 1) * DK)
        qh = query_all[:, own]
        kh = keys[:, own].astype(f32)
        cf, cb = (cum_f[:, own], cum_b[:, own])
        ends_f = [cf[(b + 1) * BLK - 1 : (b + 1) * BLK] for b in range(blocks)]
        ends_b = [cb[b * BLK : b * BLK + 1] for b in range(blocks)]
        spread = (BLK, DK)
        end_f = jnp.concatenate([jnp.broadcast_to(e, spread) for e in ends_f], axis=0)
        end_b = jnp.concatenate([jnp.broadcast_to(e, spread) for e in ends_b], axis=0)
        qf, qb = (qh * jnp.exp(cf), qh * jnp.exp(cb))
        qf_b, qb_b = (qf.astype(bf16), qb.astype(bf16))
        scores = (
            jnp.where(forward, matmul(qf_b, (kh * jnp.exp(-cf)).astype(bf16), NT), 0.0)
            + jnp.where(backward, matmul(qb_b, (kh * jnp.exp(-cb)).astype(bf16), NT), 0.0)
            + jnp.where(later, matmul(qf_b, (kh * jnp.exp(end_f - cf)).astype(bf16), NT), 0.0)
            + jnp.where(sooner, matmul(qb_b, (kh * jnp.exp(end_b - cb)).astype(bf16), NT), 0.0)
        )
        vh = values[:, h * wide : (h + 1) * wide]
        inside[:, h * wide : (h + 1) * wide] = matmul(scores.astype(bf16), vh)
        for b in range(blocks):
            rows = slice(b * BLK, (b + 1) * BLK)
            before = sum(ends_f[:b], jnp.zeros_like(ends_f[0]))
            after = sum(ends_b[b + 1 :], jnp.zeros_like(ends_b[0]))
            reach_f[rows, own] = (qf[rows] * jnp.exp(before)).astype(bf16)
            reach_b[rows, own] = (qb[rows] * jnp.exp(after)).astype(bf16)
    gates = matmul(rows_in, gate_w[...], NT).astype(bf16).astype(f32)
    gated[...] = gains_of(gates, gain[...])


def gains_of(gates, gain):
    return gates * jax.nn.sigmoid(gates) * gain


def merge_kernel(bit, final, heads, ctx, own, partner, out):
    size = (own.shape[0] - growth_rows(heads) - 4 * heads * ctx) // 2
    lift = growth_rows(heads)
    states = 1 if final else 2
    sp = lax.axis_index("sp")
    side = lax.bitwise_and(lax.shift_right_logical(sp, bit), 1)
    onward = lax.bitwise_and(lax.shift_right_logical(sp, bit + 1), 1)

    def emit(low, up):
        wide = size // heads

        def forward(at):
            for h in range(heads):
                rows = slice(h * wide, (h + 1) * wide)
                decayed = growth_of(up, 2 * size, 0, h, heads) * low[rows, :].astype(f32)
                out[at + h * wide : at + (h + 1) * wide, :] = (
                    decayed + up[rows, :].astype(f32)
                ).astype(bf16)

        def backward(at):
            for h in range(heads):
                rows = slice(size + h * wide, size + (h + 1) * wide)
                decayed = growth_of(low, 2 * size, 1, h, heads) * up[rows, :].astype(f32)
                out[at + h * wide : at + (h + 1) * wide, :] = (
                    decayed + low[rows, :].astype(f32)
                ).astype(bf16)

        if final:
            pl.when(onward == 0)(lambda: forward(0))
            pl.when(onward == 1)(lambda: backward(0))
        else:
            forward(0)
            backward(size)
        out[states * size : states * size + lift, :] = (
            low[2 * size : 2 * size + lift, :].astype(f32)
            * up[2 * size : 2 * size + lift, :].astype(f32)
        ).astype(bf16)
        base_in, base_out = (2 * size + lift, states * size + lift)
        for section in range(4 * heads):
            before = low[base_in + section * ctx : base_in + (section + 1) * ctx, :]
            after = up[base_in + section * ctx : base_in + (section + 1) * ctx, :]
            if section < heads:
                before = before.astype(f32) * growth_of(up, 2 * size, 2, section, heads)
            elif section < 2 * heads:
                after = after.astype(f32) * growth_of(low, 2 * size, 3, section - heads, heads)
            at = base_out + 2 * section * ctx
            out[at : at + ctx, :] = before.astype(bf16)
            out[at + ctx : at + 2 * ctx, :] = after.astype(bf16)

    pl.when(side == 0)(lambda: emit(own, partner))
    pl.when(side == 1)(lambda: emit(partner, own))


def finish_kernel(steps, heads, ctx, *refs):
    own = refs[0]
    partners = refs[1 : 1 + steps]
    inside, reach_f, reach_b, gated, out, start_f, start_b, grow_f, grow_b = refs[1 + steps :]
    sp = lax.axis_index("sp")
    size = start_f.shape[0]
    wide = size // heads
    start_f[...] = jnp.zeros(start_f.shape, f32)
    start_b[...] = jnp.zeros(start_b.shape, f32)
    grow_f[...] = jnp.ones(grow_f.shape, f32)
    grow_b[...] = jnp.ones(grow_b.shape, f32)

    def take(start, grow, partner, at, kind, states):
        for h in range(heads):
            rows = slice(h * wide, (h + 1) * wide)
            one = slice(h, h + 1)
            theirs = partner[at + h * wide : at + (h + 1) * wide, :].astype(f32)
            start[rows, :] = start[rows, :] + grow[one, :] * theirs
            grow[one, :] = grow[one, :] * growth_of(partner, states * size, kind, h, heads)

    for step in range(steps):
        side = lax.bitwise_and(lax.shift_right_logical(sp, step), 1)
        states = 1 if step == steps - 1 and steps > 1 else 2
        partner = partners[step]
        back = size if states == 2 else 0
        pl.when(side == 1)(functools.partial(take, start_f, grow_f, partner, 0, 0, states))
        pl.when(side == 0)(functools.partial(take, start_b, grow_b, partner, back, 1, states))

    states = 1 if steps > 1 else 2
    lift = growth_rows(heads)
    base = states * size + lift
    rows_each = ctx << (steps - 1)

    def context(low, up):
        def part(ref, section):
            return ref[base + section * rows_each : base + (section + 1) * rows_each, :]

        for h in range(heads):
            one = slice(h, h + 1)
            grow_up = growth_of(up, states * size, 2, h, heads)
            grow_low = growth_of(low, states * size, 3, h, heads)
            kf = [(part(low, h).astype(f32) * grow_up).astype(bf16), part(up, h)]
            kb = [part(low, heads + h), (part(up, heads + h).astype(f32) * grow_low).astype(bf16)]
            first = 2 * heads + h * (wide // DK)
            for c in range(wide // DK):
                vs = jnp.concatenate([part(low, first + c), part(up, first + c)], axis=0)
                at = slice(h * wide + c * DK, h * wide + (c + 1) * DK)
                start_f[at, :] += grow_f[one, :] * matmul(vs, jnp.concatenate(kf, axis=0), TN)
                start_b[at, :] += grow_b[one, :] * matmul(vs, jnp.concatenate(kb, axis=0), TN)

    side = lax.bitwise_and(lax.shift_right_logical(sp, steps - 1), 1)
    pl.when(side == 0)(lambda: context(own, partners[-1]))
    pl.when(side == 1)(lambda: context(partners[-1], own))
    i = lax.broadcasted_iota(jnp.int32, (DK, DK), 0)
    j = lax.broadcasted_iota(jnp.int32, (DK, DK), 1)
    shift = VGROUP.bit_length() - 1
    alike = lax.shift_right_logical(i, shift) == lax.shift_right_logical(j, shift)
    averaging = jnp.where(alike, 1.0 / VGROUP, 0.0).astype(bf16)
    for h in range(heads):
        own_rows = slice(h * wide, (h + 1) * wide)
        lanes = slice(h * DK, (h + 1) * DK)
        result = (
            inside[:, own_rows]
            + matmul(reach_f[:, lanes], start_f[own_rows, :].astype(bf16), NT)
            + matmul(reach_b[:, lanes], start_b[own_rows, :].astype(bf16), NT)
        )
        for c in range(wide // DK):
            x = result[:, c * DK : (c + 1) * DK]
            high, low = halves(x * x)
            power = matmul(high, averaging) + matmul(low, averaging)
            at = slice(h * wide + c * DK, h * wide + (c + 1) * DK)
            out[:, at] = (x * lax.rsqrt(power + epsilon) * gated[:, at]).astype(bf16)


def branch_of(order, pieces, weight):
    width = pieces[0].shape[1]
    branch = None
    for k, piece in zip(order, pieces):
        column = pl.multiple_of(lax.bitwise_xor(lax.axis_index("tp"), k) * width, width)
        part = matmul(piece[...], weight[:, pl.ds(column, width)], NT)
        branch = part if branch is None else branch + part
    return branch


def early_kernel(order, *refs):
    weight, out = refs[-2:]
    out[...] = branch_of(order, refs[:-2], weight)


def output_kernel(order, *refs):
    weight, early, latent, mod, out = refs[-5:]
    branch = early[...] + branch_of(order, refs[:-5], weight)
    out[...] = (latent[...].astype(f32) + mod[4:5, :] * branch).astype(bf16)


def local_direct(*args):
    return direct_plan(*args)


def direct_plan(
    latent,
    context,
    conditioning,
    context_prompt_vector,
    shift_matrix,
    scale_matrix,
    residual_gate_matrix,
    query_matrix,
    key_matrix,
    value_matrix,
    gate_matrix,
    decay_down_factor,
    decay_up_factor,
    decay_key_bias,
    spike_log_decay,
    output_gain,
    output_matrix,
):
    tp_count, sp_count = (lax.axis_size("tp"), lax.axis_size("sp"))
    heads = HEADS // tp_count
    tokens, width = latent.shape
    ctx = context.shape[0]
    total = tokens + ctx
    features = width * tp_count
    steps = sp_count.bit_length() - 1
    shape = jax.ShapeDtypeStruct

    inner = conditioning.shape[0]
    rows_in = (inner // 128, 128)
    mod, joined = call(
        modulation_kernel,
        [shape((8, width), f32), shape((total, width), bf16)],
        [HBM_SPEC] * 7,
        (
            conditioning.reshape(rows_in),
            context_prompt_vector.reshape(rows_in),
            shift_matrix,
            scale_matrix,
            residual_gate_matrix,
            latent,
            context,
        ),
        6 * 8 * width * inner,
        6 * width * inner,
        [pltpu.VMEM(rows_in, bf16)] * 2
        + [pltpu.VMEM(shift_matrix.shape, bf16)] * 3
        + [pltpu.SemaphoreType.DMA((7,))],
        WIDE_GRANT,
    )
    pieces = gathered_pieces(joined, "tp")
    for bit in range(steps):
        theirs = exchange(mod, "sp", 1 << bit)
        rows = [8] if bit < steps - 1 else [8, 4]
        sums = call(
            add_kernel,
            [shape((r, width), f32) for r in rows],
            [VMEM_SPEC] * 2,
            (mod, theirs),
            8 * width,
            64 * width,
        )
        mod = sums[0]
    mods = [sums[1]]
    for bit in range(tp_count.bit_length() - 1):
        joint = mods[0]
        if bit > 0:
            joint = call(
                join_kernel,
                shape((4 << bit, width), f32),
                [VMEM_SPEC] * len(mods),
                mods,
                8 * width,
                64 * width,
            )
        mods = mods + [exchange(joint, "tp", 1 << bit)]

    half = heads * DK
    down = jnp.transpose(decay_down_factor, (0, 2, 1)).reshape(2 * DECAY_RANK, features)
    vdim = value_matrix.shape[0]
    lift = growth_rows(heads)
    surveyed = [0] + [k for k, source in gather_plan(tp_count) if source == 0][:3]
    early = call(
        survey_kernel,
        [shape((total, 128), f32)] * 2,
        [VMEM_SPEC] * len(surveyed),
        [pieces[k] for k in surveyed],
        SURVEY_FLOPS,
        SURVEY_BYTES,
    )
    normed, keys, values, cum_f, cum_b, payload = call(
        functools.partial(project_kernel, tp_count, tokens, heads, surveyed),
        [
            shape((total, features), bf16),
            shape((tokens, half), bf16),
            shape((tokens, vdim), bf16),
            shape((tokens, half), f32),
            shape((tokens, half), f32),
            shape((2 * vdim + lift + 4 * heads * ctx, DK), bf16),
        ],
        [VMEM_SPEC] * (tp_count + len(mods) + 6) + [HBM_SPEC] * 2,
        (
            *pieces,
            *mods,
            down,
            key_matrix,
            value_matrix,
            *early,
            jnp.transpose(spike_log_decay, (0, 2, 1)),
            decay_up_factor,
            decay_key_bias,
        ),
        2 * total * features * (half + vdim),
        2 * features * (half + vdim),
        [
            pltpu.VMEM((2, DECAY_RANK, half), bf16),
            pltpu.VMEM((2, half), f32),
            pltpu.SemaphoreType.DMA((2,)),
        ],
    )
    partners = [exchange(payload, "sp", 1)]
    rows = ctx
    for bit in range(steps - 1):
        final = bit == steps - 2
        states = 1 if final else 2
        payload = call(
            functools.partial(merge_kernel, bit, final, heads, rows),
            shape((states * vdim + lift + 8 * heads * rows, DK), bf16),
            [VMEM_SPEC, VMEM_SPEC],
            (payload, partners[-1]),
            4 * vdim * DK,
            8 * vdim * DK,
        )
        rows = 2 * rows
        partners.append(exchange(payload, "sp", 2 << bit))
    inside, reach_f, reach_b, gated = call(
        functools.partial(within_kernel, heads),
        [
            shape((tokens, vdim), f32),
            shape((tokens, half), bf16),
            shape((tokens, half), bf16),
            shape((tokens, vdim), f32),
        ],
        [VMEM_SPEC] * 8,
        (
            normed,
            query_matrix,
            gate_matrix,
            keys,
            values,
            cum_f,
            cum_b,
            output_gain[None],
        ),
        2 * tokens * features * (half + vdim),
        2 * features * (half + vdim),
    )
    heads_out = call(
        functools.partial(finish_kernel, steps, heads, ctx),
        shape((tokens, vdim), bf16),
        [VMEM_SPEC] * (5 + steps),
        (payload, *partners, inside, reach_f, reach_b, gated),
        8 * tokens * vdim * DK,
        8 * tokens * vdim,
        [
            pltpu.VMEM((vdim, DK), f32),
            pltpu.VMEM((vdim, DK), f32),
            pltpu.VMEM((8 * -(-heads // 8), DK), f32),
            pltpu.VMEM((8 * -(-heads // 8), DK), f32),
        ],
    )
    branches = gathered_pieces(heads_out, "tp")
    late = [k for k in range(1, tp_count) if k >= tp_count - 3]
    soon = [k for k in range(tp_count) if k not in late]
    cost = 2 * width * vdim
    early = call(
        functools.partial(early_kernel, soon),
        shape((tokens, width), f32),
        [VMEM_SPEC] * (len(soon) + 1),
        (*(branches[k] for k in soon), output_matrix),
        tokens * cost * len(soon),
        cost * len(soon),
    )
    return call(
        functools.partial(output_kernel, late),
        shape((tokens, width), bf16),
        [VMEM_SPEC] * (len(late) + 4),
        (*(branches[k] for k in late), output_matrix, early, latent, mod),
        tokens * cost * len(late),
        cost * len(late),
    )


def solution(mesh):
    placed = (
        P("sp", "tp"),
        P("sp", "tp"),
        P("sp"),
        P("sp"),
        P("tp", "sp"),
        P("tp", "sp"),
        P("tp", "sp"),
        P("tp", None),
        P("tp", None),
        P("tp", None),
        P("tp", None),
        P(),
        P(),
        P(),
        P(None, "sp", None),
        P("tp"),
        P("tp", None),
    )
    tp_count, sp_count = (mesh.shape["tp"], mesh.shape["sp"])
    powers = tp_count & tp_count - 1 == 0 and sp_count & sp_count - 1 == 0
    direct = 2 <= tp_count <= HEADS and sp_count >= 2 and powers
    return jax.shard_map(
        local_direct if direct else local_general, mesh=mesh, in_specs=placed, out_specs=P("sp", "tp"), check_vma=False
    )
```

profile of v0, /device:TPU:0, one launch (start us, length us, event | category | flops | bytes accessed | tf_op | source)
XLA Modules:
  0.0 66.4 jit_solution(2274885424880917990)
XLA Ops:
  0.0 3.1 %shard_map.163 = (f32[8,512]{1,0:T(8,128)}, bf16[144,512]{1,0:T(8,128)(2,1)}) custom-call(bf16[8,128]{1,0:T(8,128)(2,1)} %bitcast.10, bf16[8,128]{1,0:T(8,128)(2,1)} %bitcast.11, bf16[512,1024]{1,0:T(8,128)(2,1)} %refs_2_.1, bf16[512,1024]{1,0:T(8,128)(2,1)} %refs_3_.2, bf16[512,1024]{1,0:T(8,128)(2,1)} %refs_4_.1, bf16[128,512]{1,0:T(8,128)(2,1)} %refs_5_.5, ...), custom_call_target="tpu_custom_call" | custom-call | flops 25165824 | bytes 3145728 | tf_op jit(solution)/shard_map/pallas_call | solution.py:352
  3.1 4.1 %collective-permute-start.3 = (bf16[144,512]{1,0:T(8,128)(2,1)}, bf16[144,512]{1,0:T(8,128)(2,1)S(1)}, u32[]{:S(2)}, u32[]{:S(2)}) collective-permute-start(bf16[144,512]{1,0:T(8,128)(2,1)} %get-tuple-element.21.refs_0_), channel_id=1, source_target_pairs={{0,4},{1,5},{2,6},{3,7},{4,0},{5,1},{6,2},{7,3},{8,12},{9,13},{10,... | collective-permute-start | bytes 442376 | tf_op jit(solution)/shard_map/ppermute | solution.py:325
  7.3 1.6 %collective-permute-start.1 = (bf16[144,512]{1,0:T(8,128)(2,1)}, bf16[144,512]{1,0:T(8,128)(2,1)S(1)}, u32[]{:S(2)}, u32[]{:S(2)}) collective-permute-start(bf16[144,512]{1,0:T(8,128)(2,1)} %get-tuple-element.21.refs_0_), channel_id=1, source_target_pairs={{0,2},{1,3},{2,0},{3,1},{4,6},{5,7},{6,4},{7,5},{8,10},{9,11},{10,... | collective-permute-start | bytes 442376 | tf_op jit(solution)/shard_map/ppermute | solution.py:325
  8.9 1.5 %collective-permute-start = (bf16[144,512]{1,0:T(8,128)(2,1)}, bf16[144,512]{1,0:T(8,128)(2,1)S(1)}, u32[]{:S(2)}, u32[]{:S(2)}) collective-permute-start(bf16[144,512]{1,0:T(8,128)(2,1)} %get-tuple-element.21.refs_0_), channel_id=1, source_target_pairs={{0,1},{1,0},{2,3},{3,2},{4,5},{5,4},{6,7},{7,6},{8,9},{9,8},{10,11... | collective-permute-start | bytes 442376 | tf_op jit(solution)/shard_map/ppermute | solution.py:325
  10.4 0.0 collective-permute-start.7
  10.4 1.4 %collective-permute-done.7.theirs = f32[8,512]{1,0:T(8,128)S(1)} collective-permute-done((f32[8,512]{1,0:T(8,128)}, f32[8,512]{1,0:T(8,128)S(1)}, u32[]{:S(2)}, u32[]{:S(2)}) %collective-permute-start.7) | collective-permute-done | bytes 16416 | tf_op jit(solution)/shard_map/ppermute | solution.py:325
  11.8 0.7 %copy-done.11 = f32[8,512]{1,0:T(8,128)S(1)} copy-done((f32[8,512]{1,0:T(8,128)S(1)}, f32[8,512]{1,0:T(8,128)}, u32[]{:S(2)}) %copy-start.11) | copy-done | bytes 16408
  12.5 1.5 %collective-permute-start.8 = (f32[8,512]{1,0:T(8,128)S(1)}, f32[8,512]{1,0:T(8,128)S(1)}, u32[]{:S(2)}, u32[]{:S(2)}) collective-permute-start(f32[8,512]{1,0:T(8,128)S(1)} %shard_map.164.mine), channel_id=1, source_target_pairs={{0,16},{8,24},{16,0},{24,8},{1,17},{9,25},{17,1},{25,9},{2,18},{10... | collective-permute-start | bytes 49160 | tf_op jit(solution)/shard_map/ppermute | solution.py:325
  14.0 2.2 %collective-permute-done.8.theirs = f32[8,512]{1,0:T(8,128)S(1)} collective-permute-done((f32[8,512]{1,0:T(8,128)S(1)}, f32[8,512]{1,0:T(8,128)S(1)}, u32[]{:S(2)}, u32[]{:S(2)}) %collective-permute-start.8) | collective-permute-done | bytes 16416 | tf_op jit(solution)/shard_map/ppermute | solution.py:325
  16.2 0.5 collective-permute-start.9
  16.7 3.1 %collective-permute-done.9.refs_1_.refs_9_ = f32[4,512]{1,0:T(4,128)S(1)} collective-permute-done((f32[4,512]{1,0:T(4,128)S(1)}, f32[4,512]{1,0:T(4,128)S(1)}, u32[]{:S(2)}, u32[]{:S(2)}) %collective-permute-start.9) | collective-permute-done | bytes 8224 | tf_op jit(solution)/shard_map/ppermute | solution.py:325
  19.9 0.4 collective-permute-start.10
  20.3 1.3 %collective-permute-start.6 = (bf16[144,512]{1,0:T(8,128)(2,1)}, bf16[144,512]{1,0:T(8,128)(2,1)S(1)}, u32[]{:S(2)}, u32[]{:S(2)}) collective-permute-start(bf16[144,512]{1,0:T(8,128)(2,1)} %get-tuple-element.21.refs_0_), channel_id=1, source_target_pairs={{0,7},{1,6},{2,5},{3,4},{4,3},{5,2},{6,1},{7,0},{8,15},{9,14},{10,... | collective-permute-start | bytes 442376 | tf_op jit(solution)/shard_map/ppermute | solution.py:325
  21.6 3.2 %collective-permute-done.10.refs_2_.refs_10_ = f32[8,512]{1,0:T(8,128)S(1)} collective-permute-done((f32[8,512]{1,0:T(8,128)S(1)}, f32[8,512]{1,0:T(8,128)S(1)}, u32[]{:S(2)}, u32[]{:S(2)}) %collective-permute-start.10) | collective-permute-done | bytes 16416 | tf_op jit(solution)/shard_map/ppermute | solution.py:325
  24.8 0.0 copy-start.1
  24.8 0.0 copy-start.4
  24.8 0.0 copy-start.6
  24.9 0.1 collective-permute-start.11
  24.9 0.0 collective-permute-done.3.refs_1_.refs_4_
  24.9 0.1 collective-permute-start.5
  25.0 0.0 collective-permute-done.1.refs_2_
  25.0 1.3 %collective-permute-start.4 = (bf16[144,512]{1,0:T(8,128)(2,1)S(1)}, bf16[144,512]{1,0:T(8,128)(2,1)S(1)}, u32[]{:S(2)}, u32[]{:S(2)}) collective-permute-start(bf16[144,512]{1,0:T(8,128)(2,1)S(1)} %collective-permute-done.3.refs_1_.refs_4_), channel_id=1, source_target_pairs={{0,1},{1,0},{2,3},{3,2},{4,5},{5,4},{6,7},{7,6},{8,9},{9,8},{10,11... | collective-permute-start | bytes 442376 | tf_op jit(solution)/shard_map/ppermute | solution.py:325
  26.3 0.0 collective-permute-done.refs_3_.refs_1_
  26.3 0.8 %collective-permute-start.2 = (bf16[144,512]{1,0:T(8,128)(2,1)S(1)}, bf16[144,512]{1,0:T(8,128)(2,1)S(1)}, u32[]{:S(2)}, u32[]{:S(2)}) collective-permute-start(bf16[144,512]{1,0:T(8,128)(2,1)S(1)} %collective-permute-done.1.refs_2_), channel_id=1, source_target_pairs={{0,1},{1,0},{2,3},{3,2},{4,5},{5,4},{6,7},{7,6},{8,9},{9,8},{10,11... | collective-permute-start | bytes 442376 | tf_op jit(solution)/shard_map/ppermute | solution.py:325
  27.1 0.9 %copy-done.7 = bf16[144,512]{1,0:T(8,128)(2,1)S(1)} copy-done((bf16[144,512]{1,0:T(8,128)(2,1)S(1)}, bf16[144,512]{1,0:T(8,128)(2,1)}, u32[]{:S(2)}) %copy-start.7) | copy-done | bytes 147480
  28.0 0.2 shard_map.168
  28.2 1.6 %collective-permute-done.11.refs_11_ = f32[16,512]{1,0:T(8,128)S(1)} collective-permute-done((f32[16,512]{1,0:T(8,128)S(1)}, f32[16,512]{1,0:T(8,128)S(1)}, u32[]{:S(2)}, u32[]{:S(2)}) %collective-permute-start.11) | collective-permute-done | bytes 32800 | tf_op jit(solution)/shard_map/ppermute | solution.py:325
  29.8 0.0 collective-permute-done.6.refs_7_
  29.8 0.7 %collective-permute-done.5.refs_6_ = bf16[144,512]{1,0:T(8,128)(2,1)S(1)} collective-permute-done((bf16[144,512]{1,0:T(8,128)(2,1)S(1)}, bf16[144,512]{1,0:T(8,128)(2,1)S(1)}, u32[]{:S(2)}, u32[]{:S(2)}) %collective-permute-start.5) | collective-permute-done | bytes 147488 | tf_op jit(solution)/shard_map/ppermute | solution.py:325
  30.5 1.2 %collective-permute-done.4.refs_5_ = bf16[144,512]{1,0:T(8,128)(2,1)S(1)} collective-permute-done((bf16[144,512]{1,0:T(8,128)(2,1)S(1)}, bf16[144,512]{1,0:T(8,128)(2,1)S(1)}, u32[]{:S(2)}, u32[]{:S(2)}) %collective-permute-start.4) | collective-permute-done | bytes 147488 | tf_op jit(solution)/shard_map/ppermute | solution.py:325
  31.8 1.6 %collective-permute-done.2.refs_3_ = bf16[144,512]{1,0:T(8,128)(2,1)S(1)} collective-permute-done((bf16[144,512]{1,0:T(8,128)(2,1)S(1)}, bf16[144,512]{1,0:T(8,128)(2,1)S(1)}, u32[]{:S(2)}, u32[]{:S(2)}) %collective-permute-start.2) | collective-permute-done | bytes 147488 | tf_op jit(solution)/shard_map/ppermute | solution.py:325
  33.3 0.0 copy-done.9
  33.3 0.0 copy-done.10
  33.3 0.0 copy-done.1
  33.4 0.0 copy-done.4
  33.4 0.0 copy-done.6
  33.4 0.0 copy-start.2
  33.4 0.0 copy-start.3
  33.4 0.0 copy-start.12
  33.4 4.7 %shard_map.169 = (bf16[144,4096]{1,0:T(8,128)(2,1)S(1)}, bf16[128,256]{1,0:T(8,128)(2,1)S(1)}, bf16[128,512]{1,0:T(8,128)(2,1)S(1)}, f32[128,256]{1,0:T(8,128)S(...) custom-call(bf16[144,512]{1,0:T(8,128)(2,1)S(1)} %copy-done.7, ...), custom_call_target="tpu_custom_call" | custom-call | flops 905969664 | bytes 6291456 | tf_op jit(solution)/shard_map/pallas_call | solution.py:352
  38.1 0.1 collective-permute-start.12
  38.2 1.6 %collective-permute-done.12.partner.refs_1_ = bf16[1168,128]{1,0:T(8,128)(2,1)S(1)} collective-permute-done((bf16[1168,128]{1,0:T(8,128)(2,1)S(1)}, bf16[1168,128]{1,0:T(8,128)(2,1)S(1)}, u32[]{:S(2)}, u32[]{:S(2)}) %collective-permute-start.12) | collective-permute-done | bytes 299040 | tf_op jit(solution)/shard_map/ppermute | solution.py:325
  39.8 0.1 shard_map.170.refs_0_
  39.8 1.5 %collective-permute-start.13 = (bf16[784,128]{1,0:T(8,128)(2,1)S(1)}, bf16[784,128]{1,0:T(8,128)(2,1)S(1)}, u32[]{:S(2)}, u32[]{:S(2)}) collective-permute-start(bf16[784,128]{1,0:T(8,128)(2,1)S(1)} %shard_map.170.refs_0_), channel_id=1, source_target_pairs={{0,16},{8,24},{16,0},{24,8},{1,17},{9,25},{17,1},{25,9},{2,18},{10... | collective-permute-start | bytes 602120 | tf_op jit(solution)/shard_map/ppermute | solution.py:325
  41.4 2.8 %shard_map.171 = (f32[128,512]{1,0:T(8,128)S(1)}, bf16[128,256]{1,0:T(8,128)(2,1)S(1)}, bf16[128,256]{1,0:T(8,128)(2,1)S(1)}, f32[128,512]{1,0:T(8,128)S(1)}) custom-call(bf16[144,4096]{1,0:T(8,128)(2,1)S(1)} %get-tuple-element.27.normed, bf16[256,4096]{1,0:T(8,128)(2,1)S(1)} %copy-done.3, bf16[512,4096]{1,0:T(8,128)(2,1)S(1)} %copy-done.2, ...), custom_call_target="tpu_custom_call" | custom-call | flops 805306368 | bytes 6291456 | tf_op jit(solution)/shard_map/pallas_call | solution.py:352
  44.2 0.0 copy-start.5
  44.2 2.7 %collective-permute-done.13.refs_2_ = bf16[784,128]{1,0:T(8,128)(2,1)S(1)} collective-permute-done((bf16[784,128]{1,0:T(8,128)(2,1)S(1)}, bf16[784,128]{1,0:T(8,128)(2,1)S(1)}, u32[]{:S(2)}, u32[]{:S(2)}) %collective-permute-start.13) | collective-permute-done | bytes 200736 | tf_op jit(solution)/shard_map/ppermute | solution.py:325
  46.9 0.8 %shard_map.172.refs_0_ = bf16[128,512]{1,0:T(8,128)(2,1)S(1)} custom-call(bf16[784,128]{1,0:T(8,128)(2,1)S(1)} %shard_map.170.refs_0_, bf16[1168,128]{1,0:T(8,128)(2,1)S(1)} %collective-permute-done.12.partner.refs_1_, bf16[784,128]{1,0:T(8,128)(2,1)S(1)} %collective-permute-done.13.refs_2_, f32[128,512]{1,0:T(8,128)S(1)} %get-tuple-element.32.refs_3_, ...), custom_call_target="tpu_custom_call" | custom-call | flops 67108864 | bytes 524288 | tf_op jit(solution)/shard_map/pallas_call | solution.py:352
  47.7 0.5 collective-permute-start.19
  48.2 2.8 %collective-permute-start.14 = (bf16[128,512]{1,0:T(8,128)(2,1)S(1)}, bf16[128,512]{1,0:T(8,128)(2,1)S(1)}, u32[]{:S(2)}, u32[]{:S(2)}) collective-permute-start(bf16[128,512]{1,0:T(8,128)(2,1)S(1)} %shard_map.172.refs_0_), channel_id=1, source_target_pairs={{0,4},{1,5},{2,6},{3,7},{4,0},{5,1},{6,2},{7,3},{8,12},{9,13},{10,... | collective-permute-start | bytes 393224 | tf_op jit(solution)/shard_map/ppermute | solution.py:325
  51.1 0.5 collective-permute-start.18
  51.5 3.3 %collective-permute-done.19.refs_2_ = bf16[128,512]{1,0:T(8,128)(2,1)S(1)} collective-permute-done((bf16[128,512]{1,0:T(8,128)(2,1)S(1)}, bf16[128,512]{1,0:T(8,128)(2,1)S(1)}, u32[]{:S(2)}, u32[]{:S(2)}) %collective-permute-start.19) | collective-permute-done | bytes 131104 | tf_op jit(solution)/shard_map/ppermute | solution.py:325
  54.9 0.4 collective-permute-start.20
  55.3 3.1 %collective-permute-start.17 = (bf16[128,512]{1,0:T(8,128)(2,1)S(1)}, bf16[128,512]{1,0:T(8,128)(2,1)S(1)}, u32[]{:S(2)}, u32[]{:S(2)}) collective-permute-start(bf16[128,512]{1,0:T(8,128)(2,1)S(1)} %shard_map.172.refs_0_), channel_id=1, source_target_pairs={{0,7},{1,6},{2,5},{3,4},{4,3},{5,2},{6,1},{7,0},{8,15},{9,14},{10,... | collective-permute-start | bytes 393224 | tf_op jit(solution)/shard_map/ppermute | solution.py:325
  58.4 0.0 collective-permute-done.14.refs_4_
  58.4 0.0 collective-permute-start.16
  58.4 1.1 %collective-permute-start.15 = (bf16[128,512]{1,0:T(8,128)(2,1)S(1)}, bf16[128,512]{1,0:T(8,128)(2,1)S(1)}, u32[]{:S(2)}, u32[]{:S(2)}) collective-permute-start(bf16[128,512]{1,0:T(8,128)(2,1)S(1)} %collective-permute-done.14.refs_4_), channel_id=1, source_target_pairs={{0,1},{1,0},{2,3},{3,2},{4,5},{5,4},{6,7},{7,6},{8,9},{9,8},{10,11... | collective-permute-start | bytes 393224 | tf_op jit(solution)/shard_map/ppermute | solution.py:325
  59.5 0.0 collective-permute-done.18.refs_1_
  59.5 4.1 %collective-permute-done.20.refs_3_ = bf16[128,512]{1,0:T(8,128)(2,1)S(1)} collective-permute-done((bf16[128,512]{1,0:T(8,128)(2,1)S(1)}, bf16[128,512]{1,0:T(8,128)(2,1)S(1)}, u32[]{:S(2)}, u32[]{:S(2)}) %collective-permute-start.20) | collective-permute-done | bytes 131104 | tf_op jit(solution)/shard_map/ppermute | solution.py:325
  63.6 1.0 %shard_map.173.refs_4_ = f32[128,512]{1,0:T(8,128)S(1)} custom-call(bf16[128,512]{1,0:T(8,128)(2,1)S(1)} %shard_map.172.refs_0_, bf16[128,512]{1,0:T(8,128)(2,1)S(1)} %collective-permute-done.18.refs_1_, bf16[128,512]{1,0:T(8,128)(2,1)S(1)} %collective-permute-done.19.refs_2_, bf16[128,512]{1,0:T(8,128)(2,1)S(1)} %collective-permute-done.20.refs_3_, ...), custom_call_target="tpu_custom_call" | custom-call | flops 335544320 | bytes 2621440 | tf_op jit(solution)/shard_map/pallas_call | solution.py:352
  64.6 0.0 collective-permute-done.17.refs_2_
  64.6 0.0 collective-permute-done.16.refs_1_
  64.6 0.5 collective-permute-done.15.refs_0_
  65.1 1.3 %shard_map.174 = bf16[128,512]{1,0:T(8,128)(2,1)} custom-call(bf16[128,512]{1,0:T(8,128)(2,1)S(1)} %collective-permute-done.15.refs_0_, bf16[128,512]{1,0:T(8,128)(2,1)S(1)} %collective-permute-done.16.refs_1_, bf16[128,512]{1,0:T(8,128)(2,1)S(1)} %collective-permute-done.17.refs_2_, bf16[512,4096]{1,0:T(8,128)(2,1)S(1)} %copy-done, ...), custom_call_target="tpu_custom_call" | custom-call | flops 201326592 | bytes 1572864 | tf_op jit(solution)/shard_map/pallas_call | solution.py:352
  (16 shorter events, 0.0 us)
Async XLA Ops:
  3.1 21.8 %collective-permute-start.3 = (bf16[144,512]{1,0:T(8,128)(2,1)}, bf16[144,512]{1,0:T(8,128)(2,1)S(1)}, u32[]{:S(2)}, u32[]{:S(2)}) collective-permute-start(bf16[144,512]{1,0:T(8,128)(2,1)} %get-tuple-element.21.refs_0_), channel_id=1, source_target_pairs={{0,4},{1,5},{2,6},{3,7},{4,0},{5,1},{6,2},{7,3},{8,12},{9,13},{10,... | collective-permute-start | bytes 442376 | tf_op jit(solution)/shard_map/ppermute | solution.py:325
  7.3 17.8 %collective-permute-start.1 = (bf16[144,512]{1,0:T(8,128)(2,1)}, bf16[144,512]{1,0:T(8,128)(2,1)S(1)}, u32[]{:S(2)}, u32[]{:S(2)}) collective-permute-start(bf16[144,512]{1,0:T(8,128)(2,1)} %get-tuple-element.21.refs_0_), channel_id=1, source_target_pairs={{0,2},{1,3},{2,0},{3,1},{4,6},{5,7},{6,4},{7,5},{8,10},{9,11},{10,... | collective-permute-start | bytes 442376 | tf_op jit(solution)/shard_map/ppermute | solution.py:325
  8.9 17.5 %collective-permute-start = (bf16[144,512]{1,0:T(8,128)(2,1)}, bf16[144,512]{1,0:T(8,128)(2,1)S(1)}, u32[]{:S(2)}, u32[]{:S(2)}) collective-permute-start(bf16[144,512]{1,0:T(8,128)(2,1)} %get-tuple-element.21.refs_0_), channel_id=1, source_target_pairs={{0,1},{1,0},{2,3},{3,2},{4,5},{5,4},{6,7},{7,6},{8,9},{9,8},{10,11... | collective-permute-start | bytes 442376 | tf_op jit(solution)/shard_map/ppermute | solution.py:325
  10.4 1.4 %collective-permute-start.7 = (f32[8,512]{1,0:T(8,128)}, f32[8,512]{1,0:T(8,128)S(1)}, u32[]{:S(2)}, u32[]{:S(2)}) collective-permute-start(f32[8,512]{1,0:T(8,128)} %get-tuple-element.22.mine), channel_id=1, source_target_pairs={{0,8},{8,0},{16,24},{24,16},{1,9},{9,1},{17,25},{25,17},{2,10},{10... | collective-permute-start | bytes 49160 | tf_op jit(solution)/shard_map/ppermute | solution.py:325
  11.8 0.7 %copy-start.11 = (f32[8,512]{1,0:T(8,128)S(1)}, f32[8,512]{1,0:T(8,128)}, u32[]{:S(2)}) copy-start(f32[8,512]{1,0:T(8,128)} %get-tuple-element.22.mine) | copy-start | bytes 49156
  12.5 3.7 %collective-permute-start.8 = (f32[8,512]{1,0:T(8,128)S(1)}, f32[8,512]{1,0:T(8,128)S(1)}, u32[]{:S(2)}, u32[]{:S(2)}) collective-permute-start(f32[8,512]{1,0:T(8,128)S(1)} %shard_map.164.mine), channel_id=1, source_target_pairs={{0,16},{8,24},{16,0},{24,8},{1,17},{9,25},{17,1},{25,9},{2,18},{10... | collective-permute-start | bytes 49160 | tf_op jit(solution)/shard_map/ppermute | solution.py:325
  16.2 3.7 %collective-permute-start.9 = (f32[4,512]{1,0:T(4,128)S(1)}, f32[4,512]{1,0:T(4,128)S(1)}, u32[]{:S(2)}, u32[]{:S(2)}) collective-permute-start(f32[4,512]{1,0:T(4,128)S(1)} %get-tuple-element.23.refs_0_.refs_8_), channel_id=1, source_target_pairs={{0,1},{1,0},{2,3},{3,2},{4,5},{5,4},{6,7},{7,6},{8,9},{9,8},{10,11... | collective-permute-start | bytes 24584 | tf_op jit(solution)/shard_map/ppermute | solution.py:325
  19.9 4.9 %collective-permute-start.10 = (f32[8,512]{1,0:T(8,128)S(1)}, f32[8,512]{1,0:T(8,128)S(1)}, u32[]{:S(2)}, u32[]{:S(2)}) collective-permute-start(f32[8,512]{1,0:T(8,128)S(1)} %shard_map.166), channel_id=1, source_target_pairs={{0,2},{1,3},{2,0},{3,1},{4,6},{5,7},{6,4},{7,5},{8,10},{9,11},{10,... | collective-permute-start | bytes 49160 | tf_op jit(solution)/shard_map/ppermute | solution.py:325
  20.3 9.5 %collective-permute-start.6 = (bf16[144,512]{1,0:T(8,128)(2,1)}, bf16[144,512]{1,0:T(8,128)(2,1)S(1)}, u32[]{:S(2)}, u32[]{:S(2)}) collective-permute-start(bf16[144,512]{1,0:T(8,128)(2,1)} %get-tuple-element.21.refs_0_), channel_id=1, source_target_pairs={{0,7},{1,6},{2,5},{3,4},{4,3},{5,2},{6,1},{7,0},{8,15},{9,14},{10,... | collective-permute-start | bytes 442376 | tf_op jit(solution)/shard_map/ppermute | solution.py:325
  24.8 8.5 %copy-start.9 = (f32[2,128,16]{1,2,0:T(8,128)S(1)}, f32[2,128,16]{1,2,0:T(8,128)}, u32[]{:S(2)}) copy-start(f32[2,128,16]{1,2,0:T(8,128)} %param.31) | copy-start | bytes 49156
  24.8 8.5 %copy-start.10 = (f32[2,2048]{1,0:T(2,128)S(1)}, f32[2,2048]{1,0:T(2,128)}, u32[]{:S(2)}) copy-start(f32[2,2048]{1,0:T(2,128)} %refs_19_.1) | copy-start | bytes 49156
  24.8 8.5 %copy-start.1 = (bf16[512,4096]{1,0:T(8,128)(2,1)S(1)}, bf16[512,4096]{1,0:T(8,128)(2,1)}, u32[]{:S(2)}) copy-start(bf16[512,4096]{1,0:T(8,128)(2,1)} %refs_14_.1) | copy-start | bytes 12582916
  24.8 8.5 %copy-start.4 = (bf16[256,4096]{1,0:T(8,128)(2,1)S(1)}, bf16[256,4096]{1,0:T(8,128)(2,1)}, u32[]{:S(2)}) copy-start(bf16[256,4096]{1,0:T(8,128)(2,1)} %refs_13_.1) | copy-start | bytes 6291460
  24.8 8.5 %copy-start.6 = (bf16[2,4096,16]{1,2,0:T(8,128)(2,1)S(1)}, bf16[2,4096,16]{1,2,0:T(8,128)(2,1)}, u32[]{:S(2)}) copy-start(bf16[2,4096,16]{1,2,0:T(8,128)(2,1)} %param.28) | copy-start | bytes 786436
  24.9 5.0 %collective-permute-start.11 = (f32[16,512]{1,0:T(8,128)S(1)}, f32[16,512]{1,0:T(8,128)S(1)}, u32[]{:S(2)}, u32[]{:S(2)}) collective-permute-start(f32[16,512]{1,0:T(8,128)S(1)} %shard_map.167), channel_id=1, source_target_pairs={{0,4},{1,5},{2,6},{3,7},{4,0},{5,1},{6,2},{7,3},{8,12},{9,13},{10,... | collective-permute-start | bytes 98312 | tf_op jit(solution)/shard_map/ppermute | solution.py:325
  24.9 5.6 %collective-permute-start.5 = (bf16[144,512]{1,0:T(8,128)(2,1)S(1)}, bf16[144,512]{1,0:T(8,128)(2,1)S(1)}, u32[]{:S(2)}, u32[]{:S(2)}) collective-permute-start(bf16[144,512]{1,0:T(8,128)(2,1)S(1)} %collective-permute-done.3.refs_1_.refs_4_), channel_id=1, source_target_pairs={{0,2},{1,3},{2,0},{3,1},{4,6},{5,7},{6,4},{7,5},{8,10},{9,11},{10,... | collective-permute-start | bytes 442376 | tf_op jit(solution)/shard_map/ppermute | solution.py:325
  25.0 6.7 %collective-permute-start.4 = (bf16[144,512]{1,0:T(8,128)(2,1)S(1)}, bf16[144,512]{1,0:T(8,128)(2,1)S(1)}, u32[]{:S(2)}, u32[]{:S(2)}) collective-permute-start(bf16[144,512]{1,0:T(8,128)(2,1)S(1)} %collective-permute-done.3.refs_1_.refs_4_), channel_id=1, source_target_pairs={{0,1},{1,0},{2,3},{3,2},{4,5},{5,4},{6,7},{7,6},{8,9},{9,8},{10,11... | collective-permute-start | bytes 442376 | tf_op jit(solution)/shard_map/ppermute | solution.py:325
  26.3 7.0 %collective-permute-start.2 = (bf16[144,512]{1,0:T(8,128)(2,1)S(1)}, bf16[144,512]{1,0:T(8,128)(2,1)S(1)}, u32[]{:S(2)}, u32[]{:S(2)}) collective-permute-start(bf16[144,512]{1,0:T(8,128)(2,1)S(1)} %collective-permute-done.1.refs_2_), channel_id=1, source_target_pairs={{0,1},{1,0},{2,3},{3,2},{4,5},{5,4},{6,7},{7,6},{8,9},{9,8},{10,11... | collective-permute-start | bytes 442376 | tf_op jit(solution)/shard_map/ppermute | solution.py:325
  27.1 0.9 %copy-start.7 = (bf16[144,512]{1,0:T(8,128)(2,1)S(1)}, bf16[144,512]{1,0:T(8,128)(2,1)}, u32[]{:S(2)}) copy-start(bf16[144,512]{1,0:T(8,128)(2,1)} %get-tuple-element.21.refs_0_) | copy-start | bytes 442372
  28.0 5.3 %copy-start.8 = (bf16[2,16,2048]{2,1,0:T(8,128)(2,1)S(1)}, bf16[2,16,2048]{2,1,0:T(8,128)(2,1)}, u32[]{:S(2)}) copy-start(bf16[2,16,2048]{2,1,0:T(8,128)(2,1)} %refs_18_.1) | copy-start | bytes 393220
  33.4 8.0 %copy-start.2 = (bf16[512,4096]{1,0:T(8,128)(2,1)S(1)}, bf16[512,4096]{1,0:T(8,128)(2,1)}, u32[]{:S(2)}) copy-start(bf16[512,4096]{1,0:T(8,128)(2,1)} %gate_w.1) | copy-start | bytes 12582916
  33.4 8.0 %copy-start.3 = (bf16[256,4096]{1,0:T(8,128)(2,1)S(1)}, bf16[256,4096]{1,0:T(8,128)(2,1)}, u32[]{:S(2)}) copy-start(bf16[256,4096]{1,0:T(8,128)(2,1)} %query_w.1) | copy-start | bytes 6291460
  33.4 8.0 %copy-start.12 = (f32[512]{0:T(512)S(1)}, f32[512]{0:T(512)}, u32[]{:S(2)}) copy-start(f32[512]{0:T(512)} %param.32) | copy-start | bytes 6148
  38.1 1.7 %collective-permute-start.12 = (bf16[1168,128]{1,0:T(8,128)(2,1)S(1)}, bf16[1168,128]{1,0:T(8,128)(2,1)S(1)}, u32[]{:S(2)}, u32[]{:S(2)}) collective-permute-start(bf16[1168,128]{1,0:T(8,128)(2,1)S(1)} %get-tuple-element.26.own), channel_id=1, source_target_pairs={{0,8},{8,0},{16,24},{24,16},{1,9},{9,1},{17,25},{25,17},{2,10},{10... | collective-permute-start | bytes 897032 | tf_op jit(solution)/shard_map/ppermute | solution.py:325
  39.8 7.1 %collective-permute-start.13 = (bf16[784,128]{1,0:T(8,128)(2,1)S(1)}, bf16[784,128]{1,0:T(8,128)(2,1)S(1)}, u32[]{:S(2)}, u32[]{:S(2)}) collective-permute-start(bf16[784,128]{1,0:T(8,128)(2,1)S(1)} %shard_map.170.refs_0_), channel_id=1, source_target_pairs={{0,16},{8,24},{16,0},{24,8},{1,17},{9,25},{17,1},{25,9},{2,18},{10... | collective-permute-start | bytes 602120 | tf_op jit(solution)/shard_map/ppermute | solution.py:325
  41.4 22.2 %copy-start = (bf16[512,4096]{1,0:T(8,128)(2,1)S(1)}, bf16[512,4096]{1,0:T(8,128)(2,1)}, u32[]{:S(2)}) copy-start(bf16[512,4096]{1,0:T(8,128)(2,1)} %refs_3_.3) | copy-start | bytes 12582916
  44.2 20.9 %copy-start.5 = (bf16[128,512]{1,0:T(8,128)(2,1)S(1)}, bf16[128,512]{1,0:T(8,128)(2,1)}, u32[]{:S(2)}) copy-start(bf16[128,512]{1,0:T(8,128)(2,1)} %refs_5_.5) | copy-start | bytes 393220
  47.7 7.1 %collective-permute-start.19 = (bf16[128,512]{1,0:T(8,128)(2,1)S(1)}, bf16[128,512]{1,0:T(8,128)(2,1)S(1)}, u32[]{:S(2)}, u32[]{:S(2)}) collective-permute-start(bf16[128,512]{1,0:T(8,128)(2,1)S(1)} %shard_map.172.refs_0_), channel_id=1, source_target_pairs={{0,2},{1,3},{2,0},{3,1},{4,6},{5,7},{6,4},{7,5},{8,10},{9,11},{10,... | collective-permute-start | bytes 393224 | tf_op jit(solution)/shard_map/ppermute | solution.py:325
  48.2 10.1 %collective-permute-start.14 = (bf16[128,512]{1,0:T(8,128)(2,1)S(1)}, bf16[128,512]{1,0:T(8,128)(2,1)S(1)}, u32[]{:S(2)}, u32[]{:S(2)}) collective-permute-start(bf16[128,512]{1,0:T(8,128)(2,1)S(1)} %shard_map.172.refs_0_), channel_id=1, source_target_pairs={{0,4},{1,5},{2,6},{3,7},{4,0},{5,1},{6,2},{7,3},{8,12},{9,13},{10,... | collective-permute-start | bytes 393224 | tf_op jit(solution)/shard_map/ppermute | solution.py:325
  51.1 8.4 %collective-permute-start.18 = (bf16[128,512]{1,0:T(8,128)(2,1)S(1)}, bf16[128,512]{1,0:T(8,128)(2,1)S(1)}, u32[]{:S(2)}, u32[]{:S(2)}) collective-permute-start(bf16[128,512]{1,0:T(8,128)(2,1)S(1)} %shard_map.172.refs_0_), channel_id=1, source_target_pairs={{0,1},{1,0},{2,3},{3,2},{4,5},{5,4},{6,7},{7,6},{8,9},{9,8},{10,11... | collective-permute-start | bytes 393224 | tf_op jit(solution)/shard_map/ppermute | solution.py:325
  54.9 8.7 %collective-permute-start.20 = (bf16[128,512]{1,0:T(8,128)(2,1)S(1)}, bf16[128,512]{1,0:T(8,128)(2,1)S(1)}, u32[]{:S(2)}, u32[]{:S(2)}) collective-permute-start(bf16[128,512]{1,0:T(8,128)(2,1)S(1)} %collective-permute-done.19.refs_2_), channel_id=1, source_target_pairs={{0,1},{1,0},{2,3},{3,2},{4,5},{5,4},{6,7},{7,6},{8,9},{9,8},{10,11... | collective-permute-start | bytes 393224 | tf_op jit(solution)/shard_map/ppermute | solution.py:325
  55.3 9.3 %collective-permute-start.17 = (bf16[128,512]{1,0:T(8,128)(2,1)S(1)}, bf16[128,512]{1,0:T(8,128)(2,1)S(1)}, u32[]{:S(2)}, u32[]{:S(2)}) collective-permute-start(bf16[128,512]{1,0:T(8,128)(2,1)S(1)} %shard_map.172.refs_0_), channel_id=1, source_target_pairs={{0,7},{1,6},{2,5},{3,4},{4,3},{5,2},{6,1},{7,0},{8,15},{9,14},{10,... | collective-permute-start | bytes 393224 | tf_op jit(solution)/shard_map/ppermute | solution.py:325
  58.4 6.2 %collective-permute-start.16 = (bf16[128,512]{1,0:T(8,128)(2,1)S(1)}, bf16[128,512]{1,0:T(8,128)(2,1)S(1)}, u32[]{:S(2)}, u32[]{:S(2)}) collective-permute-start(bf16[128,512]{1,0:T(8,128)(2,1)S(1)} %collective-permute-done.14.refs_4_), channel_id=1, source_target_pairs={{0,2},{1,3},{2,0},{3,1},{4,6},{5,7},{6,4},{7,5},{8,10},{9,11},{10,... | collective-permute-start | bytes 393224 | tf_op jit(solution)/shard_map/ppermute | solution.py:325
  58.4 6.7 %collective-permute-start.15 = (bf16[128,512]{1,0:T(8,128)(2,1)S(1)}, bf16[128,512]{1,0:T(8,128)(2,1)S(1)}, u32[]{:S(2)}, u32[]{:S(2)}) collective-permute-start(bf16[128,512]{1,0:T(8,128)(2,1)S(1)} %collective-permute-done.14.refs_4_), channel_id=1, source_target_pairs={{0,1},{1,0},{2,3},{3,2},{4,5},{5,4},{6,7},{7,6},{8,9},{9,8},{10,11... | collective-permute-start | bytes 393224 | tf_op jit(solution)/shard_map/ppermute | solution.py:325
where the time goes:
time: 66.7 us; the launch traced here: 66.4 us
  waiting for transfers between devices  27.4 us (41%)
  starting transfers between devices  23.2 us (35%)
  Pallas kernels  13.9 us (21%)
  local copies, waits for them, and re-layouts  1.69 us (3%)
    ppermute x21, waiting for transfers between devices, exchange(): lax.ppermute(value, axis, [(i, i ^ distance) for i in range(lax.axis_size...  27.4 us
    ppermute x21, starting transfers between devices, exchange(): lax.ppermute(value, axis, [(i, i ^ distance) for i in range(lax.axis_size...  23.2 us
    pallas_call x12, Pallas kernels, call(): pl.pallas_call(kernel, out_shape=out_shapes, in_specs=in_specs, out_specs...  13.9 us
    unnamed x26, local copies, waits for them, and re-layouts  1.69 us
  transfers between devices with their start and end apart: 21, of which 13 were waited for; matrix products, arithmetic and copies ran while one was open for 0% of the time, Pallas kernels for 6%

commit v1 on v0

--- a/solution.py
+++ b/solution.py
@@ -325,7 +325,9 @@
     return lax.ppermute(value, axis, [(i, i ^ distance) for i in range(lax.axis_size(axis))])
 
 
-def gather_plan(count):
+def gather_plan(count, label):
+    if count == 8:
+        return PLANS[label]
     half = count // 2
     direct = dict.fromkeys(k for k in (half, 2, 1, count - 1) if k < count)
     plan = [(k, 0) for k in direct]
@@ -335,16 +337,26 @@
     return plan
 
 
-def gathered_pieces(value, axis):
+def gathered_pieces(value, axis, label):
     pieces = {0: value}
-    for k, source in gather_plan(lax.axis_size(axis)):
+    for k, source in gather_plan(lax.axis_size(axis), label):
         pieces[k] = exchange(pieces[source], axis, k ^ source)
     return [pieces[k] for k in sorted(pieces)]
 
 
-WIDE_GRANT = 63500
+def mod_steps(count):
+    return MOD_STEPS if count == 8 else tuple(1 << bit for bit in range(count.bit_length() - 1))
+
+
+WIDE_GRANT = 60000
+STAGE_GRANT = 2 << 10
 SURVEY_FLOPS = 15 * 10**9
 SURVEY_BYTES = 40 * 10**6
+MOD_STEPS = (1, 2, 4)
+PLANS = {
+    "lat": ((4, 0), (2, 0), (1, 0), (7, 0), (3, 2), (5, 4), (6, 4)),
+    "out": ((2, 0), (4, 0), (1, 0), (3, 2), (7, 0), (5, 4), (6, 4)),
+}
 
 
 def call(kernel, out_shapes, in_specs, args, flops, traffic, scratch=(), grant=24 << 10):
@@ -370,33 +382,58 @@
     return copies
 
 
+def in_one_row(ref):
+    block = ref[...].astype(f32)
+    return jnp.concatenate([block[r : r + 1] for r in range(block.shape[0])], axis=1)
+
+
 def modulation_kernel(*refs):
-    sources = refs[:7]
-    out, joined = refs[7:9]
-    cond_ref, prompt_ref, *weights = refs[9:14]
-    tokens = sources[5].shape[0]
-    rows = (joined.at[pl.ds(0, tokens)], joined.at[pl.ds(tokens, sources[6].shape[0])])
-    copies = fetch(sources, (cond_ref, prompt_ref, *weights, *rows), refs[14])
-
-    def in_one_row(ref):
-        block = ref[...].astype(f32)
-        return jnp.concatenate([block[r : r + 1] for r in range(block.shape[0])], axis=1)
-
+    sources = refs[:6]
+    out, joined = refs[6:8]
+    cond_ref, prompt_ref, *weights = refs[8:12]
+    tokens = sources[4].shape[0]
+    rows = (joined.at[pl.ds(0, tokens)], joined.at[pl.ds(tokens, sources[5].shape[0])])
+    copies = fetch(sources, (cond_ref, prompt_ref, *weights, *rows), refs[12])
     copies[0].wait()
     cond = in_one_row(cond_ref)
     copies[1].wait()
     row = lax.broadcasted_iota(jnp.int32, (8, cond.shape[1]), 0)
     both = jnp.where(row % 2 == 0, cond, in_one_row(prompt_ref))
     conds = (both * jax.nn.sigmoid(both)).astype(bf16)
-    products = []
-    for copy, weight in zip(copies[2:5], weights):
-        copy.wait()
-        products.append(matmul(conds, weight[...], NT))
-    shifts, scales, gates = products
     row_out = lax.broadcasted_iota(jnp.int32, out.shape, 0)
-    out[...] = jnp.where(row_out < 2, shifts, jnp.where(row_out < 4, scales, gates))
+    copies[2].wait()
+    shifts = matmul(conds, weights[0][...], NT)
+    copies[3].wait()
+    scales = matmul(conds, weights[1][...], NT)
+    out[...] = jnp.where(row_out < 2, shifts, scales)
+    copies[4].wait()
     copies[5].wait()
-    copies[6].wait()
+
+
+def gate_rows_of(width):
+    return -(-2 * (width // DK) // 16) * 16
+
+
+def split_row(value):
+    count = value.shape[1] // DK
+    rows = [value[:, c * DK : (c + 1) * DK] for c in range(count)]
+    blank = jnp.zeros((gate_rows_of(value.shape[1]) - 2 * count, DK), bf16)
+    parts = [halves(row) for row in rows]
+    return jnp.concatenate([p[0] for p in parts] + [p[1] for p in parts] + [blank], axis=0)
+
+
+def joined_row(block, width):
+    count = width // DK
+    value = block.astype(f32)
+    value = value[:count] + value[count : 2 * count]
+    return jnp.concatenate([value[c : c + 1] for c in range(count)], axis=1)
+
+
+def gating_kernel(cond_ref, weight, out):
+    cond = in_one_row(cond_ref)
+    cond = jnp.broadcast_to(cond, (8, cond.shape[1]))
+    conds = (cond * jax.nn.sigmoid(cond)).astype(bf16)
+    out[...] = split_row(matmul(conds, weight[...], NT)[:1])
 
 
 def row_sums(pieces):
@@ -424,6 +461,16 @@
         at += ref.shape[0]
 
 
+def stage_kernel(*refs):
+    sources = refs[:-2]
+    targets, at = ([], 0)
+    for source in sources:
+        targets.append(refs[-2].at[pl.ds(at, source.shape[0])])
+        at += source.shape[0]
+    for copy in fetch(sources, targets, refs[-1]):
+        copy.wait()
+
+
 def survey_kernel(*refs):
     refs[-2][...], refs[-1][...] = row_sums(refs[:-2])
 
@@ -441,22 +488,26 @@
     pieces = refs[:count]
     mods = refs[count : count + count.bit_length()]
     refs = refs[count + count.bit_length() :]
-    down, key_w, value_w, early_sums, early_squares, spikes = refs[:6]
-    normed, keys, values, cum_f, cum_b, payload = refs[8:14]
-    up_own, bias_own, sems = refs[14:]
+    weights, early_sums, early_squares, spikes, gate_part = refs[:5]
+    normed, keys, values, cum_f, cum_b, payload = refs[7:13]
+    up_own, bias_own, sems = refs[13:]
     tp = lax.axis_index("tp")
     half = heads * DK
     first = pl.multiple_of(tp * half, half)
-    sources = (refs[6].at[:, :, pl.ds(first, half)], refs[7].at[:, pl.ds(first, half)])
+    sources = (refs[5].at[:, :, pl.ds(first, half)], refs[6].at[:, pl.ds(first, half)])
     copies = fetch(sources, (up_own, bias_own), sems)
     total, width = pieces[0].shape
     ctx = total - tokens
     features = width * count
 
+    held = [[0]]
+    for distance in mod_steps(count):
+        held.append([k ^ distance for k in sum(held, [])])
+    found = {k: (level, at) for level, ks in enumerate(held) for at, k in enumerate(ks)}
+
     def mod_row(k, row):
-        level = k.bit_length()
-        at = 4 * (k - (1 << level >> 1)) + row
-        return mods[level][at : at + 1, :]
+        level, at = found[k]
+        return mods[level][4 * at + row : 4 * at + row + 1, :]
 
     sums, squares = row_sums([pieces[k] for k in range(count) if k not in surveyed])
     sums, squares = (sums + early_sums[...], squares + early_squares[...])
@@ -470,7 +521,10 @@
         context = scaled[tokens:] * (1.0 + mod_row(k, 3)) + mod_row(k, 1)
         normed[:tokens, pl.ds(column, width)] = ahead.astype(bf16)
         normed[tokens:, pl.ds(column, width)] = context.astype(bf16)
-    low_high, low_low = halves(matmul(normed[...], down[...], NT))
+    products = matmul(weights[...], normed[...], NT).T
+    key_all = products[:, :half].astype(bf16)
+    value_all = products[:, half : half + values.shape[1]].astype(bf16)
+    low_high, low_low = halves(products[:, half + values.shape[1] :])
     for copy in copies:
         copy.wait()
     blank = jnp.zeros((DECAY_RANK, half), bf16)
@@ -508,9 +562,7 @@
     cb = matmul(upper, high[:, half:]) + matmul(upper, low[:, half:])
     cum_f[...] = cf[:tokens]
     cum_b[...] = cb[:tokens]
-    key_all = matmul(normed[...], key_w[...], NT).astype(bf16)
     keys[...] = key_all[:tokens]
-    value_all = matmul(normed[...], value_w[...], NT).astype(bf16)
     values[...] = value_all[:tokens]
     wide = value_all.shape[1] // heads
     blocks = tokens // BLK
@@ -546,6 +598,7 @@
         at = start + (2 * heads + c) * ctx
         payload[at : at + ctx, :] = value_all[tokens:, c * DK : (c + 1) * DK]
     payload[2 * size : start, :] = growth_block(growth, heads)
+    payload[start + 4 * heads * ctx :, :] = gate_part[...]
 
 
 def growth_rows(heads):
@@ -623,8 +676,9 @@
     return gates * jax.nn.sigmoid(gates) * gain
 
 
-def merge_kernel(bit, final, heads, ctx, own, partner, out):
-    size = (own.shape[0] - growth_rows(heads) - 4 * heads * ctx) // 2
+def merge_kernel(bit, final, heads, ctx, width, own, partner, out):
+    gate_rows = gate_rows_of(width)
+    size = (own.shape[0] - growth_rows(heads) - 4 * heads * ctx - gate_rows) // 2
     lift = growth_rows(heads)
     states = 1 if final else 2
     sp = lax.axis_index("sp")
@@ -661,6 +715,10 @@
             * up[2 * size : 2 * size + lift, :].astype(f32)
         ).astype(bf16)
         base_in, base_out = (2 * size + lift, states * size + lift)
+        count = out.shape[0]
+        mine = joined_row(low[low.shape[0] - gate_rows :, :], width)
+        theirs = joined_row(up[up.shape[0] - gate_rows :, :], width)
+        out[count - gate_rows :, :] = split_row(mine + theirs)
         for section in range(4 * heads):
             before = low[base_in + section * ctx : base_in + (section + 1) * ctx, :]
             after = up[base_in + section * ctx : base_in + (section + 1) * ctx, :]
@@ -679,7 +737,7 @@
 def finish_kernel(steps, heads, ctx, *refs):
     own = refs[0]
     partners = refs[1 : 1 + steps]
-    inside, reach_f, reach_b, gated, out, start_f, start_b, grow_f, grow_b = refs[1 + steps :]
+    inside, reach_f, reach_b, gated, out, gates, start_f, start_b, grow_f, grow_b = refs[1 + steps :]
     sp = lax.axis_index("sp")
     size = start_f.shape[0]
     wide = size // heads
@@ -729,6 +787,9 @@
     side = lax.bitwise_and(lax.shift_right_logical(sp, steps - 1), 1)
     pl.when(side == 0)(lambda: context(own, partners[-1]))
     pl.when(side == 1)(lambda: context(partners[-1], own))
+    width = gates.shape[1]
+    last = own.shape[0] - gate_rows_of(width)
+    gates[...] = joined_row(own[last:, :], width) + joined_row(partners[-1][last:, :], width)
     i = lax.broadcasted_iota(jnp.int32, (DK, DK), 0)
     j = lax.broadcasted_iota(jnp.int32, (DK, DK), 1)
     shift = VGROUP.bit_length() - 1
@@ -766,9 +827,9 @@
 
 
 def output_kernel(order, *refs):
-    weight, early, latent, mod, out = refs[-5:]
+    weight, early, latent, gates, out = refs[-5:]
     branch = early[...] + branch_of(order, refs[:-5], weight)
-    out[...] = (latent[...].astype(f32) + mod[4:5, :] * branch).astype(bf16)
+    out[...] = (latent[...].astype(f32) + gates[...] * branch).astype(bf16)
 
 
 def local_direct(*args):
@@ -808,27 +869,34 @@
     mod, joined = call(
         modulation_kernel,
         [shape((8, width), f32), shape((total, width), bf16)],
-        [HBM_SPEC] * 7,
+        [HBM_SPEC] * 6,
         (
             conditioning.reshape(rows_in),
             context_prompt_vector.reshape(rows_in),
             shift_matrix,
             scale_matrix,
-            residual_gate_matrix,
             latent,
             context,
         ),
-        6 * 8 * width * inner,
-        6 * width * inner,
+        4 * 8 * width * inner,
+        4 * width * inner,
         [pltpu.VMEM(rows_in, bf16)] * 2
-        + [pltpu.VMEM(shift_matrix.shape, bf16)] * 3
-        + [pltpu.SemaphoreType.DMA((7,))],
+        + [pltpu.VMEM(shift_matrix.shape, bf16)] * 2
+        + [pltpu.SemaphoreType.DMA((6,))],
         WIDE_GRANT,
     )
-    pieces = gathered_pieces(joined, "tp")
+    gate_part = call(
+        gating_kernel,
+        shape((gate_rows_of(width), DK), bf16),
+        [VMEM_SPEC] * 2,
+        (conditioning.reshape(rows_in), residual_gate_matrix),
+        16 * width * inner,
+        2 * width * inner,
+    )
+    pieces = gathered_pieces(joined, "tp", "lat")
     for bit in range(steps):
         theirs = exchange(mod, "sp", 1 << bit)
-        rows = [8] if bit < steps - 1 else [8, 4]
+        rows = [8] if bit < steps - 1 else [4]
         sums = call(
             add_kernel,
             [shape((r, width), f32) for r in rows],
@@ -838,25 +906,36 @@
             64 * width,
         )
         mod = sums[0]
-    mods = [sums[1]]
-    for bit in range(tp_count.bit_length() - 1):
+    mods = [mod]
+    for distance in mod_steps(tp_count):
         joint = mods[0]
-        if bit > 0:
+        if len(mods) > 1:
             joint = call(
                 join_kernel,
-                shape((4 << bit, width), f32),
+                shape((2 * mods[-1].shape[0], width), f32),
                 [VMEM_SPEC] * len(mods),
                 mods,
                 8 * width,
                 64 * width,
             )
-        mods = mods + [exchange(joint, "tp", 1 << bit)]
+        mods = mods + [exchange(joint, "tp", distance)]
 
     half = heads * DK
     down = jnp.transpose(decay_down_factor, (0, 2, 1)).reshape(2 * DECAY_RANK, features)
     vdim = value_matrix.shape[0]
     lift = growth_rows(heads)
-    surveyed = [0] + [k for k, source in gather_plan(tp_count) if source == 0][:3]
+    surveyed = sorted({k for k, _ in gather_plan(tp_count, "lat")} & {1, 2, 3})
+    streamed = (key_matrix, value_matrix, down)
+    staged = call(
+        stage_kernel,
+        shape((half + vdim + 2 * DECAY_RANK, features), bf16),
+        [HBM_SPEC] * 3,
+        streamed,
+        0,
+        4 * features * (half + vdim),
+        [pltpu.SemaphoreType.DMA((3,))],
+        STAGE_GRANT,
+    )
     early = call(
         survey_kernel,
         [shape((total, 128), f32)] * 2,
@@ -873,17 +952,16 @@
             shape((tokens, vdim), bf16),
             shape((tokens, half), f32),
             shape((tokens, half), f32),
-            shape((2 * vdim + lift + 4 * heads * ctx, DK), bf16),
+            shape((2 * vdim + lift + 4 * heads * ctx + gate_rows_of(width), DK), bf16),
         ],
-        [VMEM_SPEC] * (tp_count + len(mods) + 6) + [HBM_SPEC] * 2,
+        [VMEM_SPEC] * (tp_count + len(mods) + 5) + [HBM_SPEC] * 2,
         (
             *pieces,
             *mods,
-            down,
-            key_matrix,
-            value_matrix,
+            staged,
             *early,
             jnp.transpose(spike_log_decay, (0, 2, 1)),
+            gate_part,
             decay_up_factor,
             decay_key_bias,
         ),
@@ -901,8 +979,8 @@
         final = bit == steps - 2
         states = 1 if final else 2
         payload = call(
-            functools.partial(merge_kernel, bit, final, heads, rows),
-            shape((states * vdim + lift + 8 * heads * rows, DK), bf16),
+            functools.partial(merge_kernel, bit, final, heads, rows, width),
+            shape((states * vdim + lift + 8 * heads * rows + gate_rows_of(width), DK), bf16),
             [VMEM_SPEC, VMEM_SPEC],
             (payload, partners[-1]),
             4 * vdim * DK,
@@ -932,9 +1010,9 @@
         2 * tokens * features * (half + vdim),
         2 * features * (half + vdim),
     )
-    heads_out = call(
+    heads_out, gates = call(
         functools.partial(finish_kernel, steps, heads, ctx),
-        shape((tokens, vdim), bf16),
+        [shape((tokens, vdim), bf16), shape((1, width), f32)],
         [VMEM_SPEC] * (5 + steps),
         (payload, *partners, inside, reach_f, reach_b, gated),
         8 * tokens * vdim * DK,
@@ -946,7 +1024,7 @@
             pltpu.VMEM((8 * -(-heads // 8), DK), f32),
         ],
     )
-    branches = gathered_pieces(heads_out, "tp")
+    branches = gathered_pieces(heads_out, "tp", "out")
     late = [k for k in range(1, tp_count) if k >= tp_count - 3]
     soon = [k for k in range(tp_count) if k not in late]
     cost = 2 * width * vdim
@@ -962,7 +1040,7 @@
         functools.partial(output_kernel, late),
         shape((tokens, width), bf16),
         [VMEM_SPEC] * (len(late) + 4),
-        (*(branches[k] for k in late), output_matrix, early, latent, mod),
+        (*(branches[k] for k in late), output_matrix, early, latent, gates),
         tokens * cost * len(late),
         cost * len(late),
     )

time: 66.7 us -> 73.1 us (1.096)
  starting transfers between devices: 23.2 us -> 30 us
  waiting for transfers between devices: 27.4 us -> 22.6 us
  local copies, waits for them, and re-layouts: 1.69 us -> 6.25 us
    ppermute x21, starting transfers between devices: 23.2 us -> 30 us  [exchange(): lax.ppermute(value, axis, [(i, i ^ distance) for i in range(lax.axis_size...]
    ppermute x21, waiting for transfers between devices: 27.4 us -> 22.6 us  [exchange(): lax.ppermute(value, axis, [(i, i ^ distance) for i in range(lax.axis_size...]
    unnamed x26 -> x30, local copies, waits for them, and re-layouts: 1.69 us -> 6.25 us
    pallas_call x12 -> x14, Pallas kernels: 13.9 us -> 13.8 us  [call(): pl.pallas_call(kernel, out_shape=out_shapes, in_specs=in_specs, out_specs...]
  transfers between devices with their start and end apart: 21 -> 21, of which waited for: 13 -> 14; matrix products, arithmetic and copies ran while one was open for 0% -> 0% of each run, Pallas kernels for 6% -> 7%
where the time goes in v1:
time: 73.1 us; the launch traced here: 72.8 us
  starting transfers between devices  30 us (41%)
  waiting for transfers between devices  22.6 us (31%)
  Pallas kernels  13.8 us (19%)
  local copies, waits for them, and re-layouts  6.25 us (9%)
    ppermute x21, starting transfers between devices, exchange(): lax.ppermute(value, axis, [(i, i ^ distance) for i in range(lax.axis_size...  30 us
    ppermute x21, waiting for transfers between devices, exchange(): lax.ppermute(value, axis, [(i, i ^ distance) for i in range(lax.axis_size...  22.6 us
    pallas_call x14, Pallas kernels, call(): pl.pallas_call(kernel, out_shape=out_shapes, in_specs=in_specs, out_specs...  13.8 us
    unnamed x30, local copies, waits for them, and re-layouts  6.25 us
  transfers between devices with their start and end apart: 21, of which 14 were waited for; matrix products, arithmetic and copies ran while one was open for 0% of the time, Pallas kernels for 7%

profile of v1, /device:TPU:0, one launch (start us, length us, event | category | flops | bytes accessed | tf_op | source)
XLA Modules:
  0.0 72.8 jit_solution(16435826100392685277)
XLA Ops:
  0.0 2.7 %shard_map.163 = (f32[8,512]{1,0:T(8,128)}, bf16[144,512]{1,0:T(8,128)(2,1)}) custom-call(bf16[8,128]{1,0:T(8,128)(2,1)} %bitcast.9, bf16[8,128]{1,0:T(8,128)(2,1)} %bitcast.12, bf16[512,1024]{1,0:T(8,128)(2,1)} %refs_2_.1, bf16[512,1024]{1,0:T(8,128)(2,1)} %refs_3_.2, bf16[128,512]{1,0:T(8,128)(2,1)} %refs_5_.5, bf16[16,512]{1,0:T(8,128)(2,1)} %refs_5_.3), custom_call_target="tpu_custom_call" | custom-call | flops 16777216 | bytes 2097152 | tf_op jit(solution)/shard_map/pallas_call | solution.py:364
  2.8 3.1 %collective-permute-start.1 = (bf16[144,512]{1,0:T(8,128)(2,1)}, bf16[144,512]{1,0:T(8,128)(2,1)S(1)}, u32[]{:S(2)}, u32[]{:S(2)}) collective-permute-start(bf16[144,512]{1,0:T(8,128)(2,1)} %get-tuple-element.21.refs_0_), channel_id=1, source_target_pairs={{0,2},{1,3},{2,0},{3,1},{4,6},{5,7},{6,4},{7,5},{8,10},{9,11},{10,... | collective-permute-start | bytes 442376 | tf_op jit(solution)/shard_map/ppermute | solution.py:325
  5.9 2.6 %collective-permute-start.3 = (bf16[144,512]{1,0:T(8,128)(2,1)}, bf16[144,512]{1,0:T(8,128)(2,1)S(1)}, u32[]{:S(2)}, u32[]{:S(2)}) collective-permute-start(bf16[144,512]{1,0:T(8,128)(2,1)} %get-tuple-element.21.refs_0_), channel_id=1, source_target_pairs={{0,4},{1,5},{2,6},{3,7},{4,0},{5,1},{6,2},{7,3},{8,12},{9,13},{10,... | collective-permute-start | bytes 442376 | tf_op jit(solution)/shard_map/ppermute | solution.py:325
  8.5 1.5 %collective-permute-start = (bf16[144,512]{1,0:T(8,128)(2,1)}, bf16[144,512]{1,0:T(8,128)(2,1)S(1)}, u32[]{:S(2)}, u32[]{:S(2)}) collective-permute-start(bf16[144,512]{1,0:T(8,128)(2,1)} %get-tuple-element.21.refs_0_), channel_id=1, source_target_pairs={{0,1},{1,0},{2,3},{3,2},{4,5},{5,4},{6,7},{7,6},{8,9},{9,8},{10,11... | collective-permute-start | bytes 442376 | tf_op jit(solution)/shard_map/ppermute | solution.py:325
  10.0 2.5 %collective-permute-done.1.refs_1_.refs_2_ = bf16[144,512]{1,0:T(8,128)(2,1)S(1)} collective-permute-done((bf16[144,512]{1,0:T(8,128)(2,1)}, bf16[144,512]{1,0:T(8,128)(2,1)S(1)}, u32[]{:S(2)}, u32[]{:S(2)}) %collective-permute-start.1) | collective-permute-done | bytes 147488 | tf_op jit(solution)/shard_map/ppermute | solution.py:325
  12.5 1.8 %collective-permute-start.2 = (bf16[144,512]{1,0:T(8,128)(2,1)S(1)}, bf16[144,512]{1,0:T(8,128)(2,1)S(1)}, u32[]{:S(2)}, u32[]{:S(2)}) collective-permute-start(bf16[144,512]{1,0:T(8,128)(2,1)S(1)} %collective-permute-done.1.refs_1_.refs_2_), channel_id=1, source_target_pairs={{0,1},{1,0},{2,3},{3,2},{4,5},{5,4},{6,7},{7,6},{8,9},{9,8},{10,11... | collective-permute-start | bytes 442376 | tf_op jit(solution)/shard_map/ppermute | solution.py:325
  14.3 0.0 collective-permute-start.7
  14.3 1.4 %collective-permute-done.7.theirs = f32[8,512]{1,0:T(8,128)S(1)} collective-permute-done((f32[8,512]{1,0:T(8,128)}, f32[8,512]{1,0:T(8,128)S(1)}, u32[]{:S(2)}, u32[]{:S(2)}) %collective-permute-start.7) | collective-permute-done | bytes 16416 | tf_op jit(solution)/shard_map/ppermute | solution.py:325
  15.7 0.7 copy-done.12
  16.4 1.5 %collective-permute-start.8 = (f32[8,512]{1,0:T(8,128)S(1)}, f32[8,512]{1,0:T(8,128)S(1)}, u32[]{:S(2)}, u32[]{:S(2)}) collective-permute-start(f32[8,512]{1,0:T(8,128)S(1)} %shard_map.164.mine), channel_id=1, source_target_pairs={{0,16},{8,24},{16,0},{24,8},{1,17},{9,25},{17,1},{25,9},{2,18},{10... | collective-permute-start | bytes 49160 | tf_op jit(solution)/shard_map/ppermute | solution.py:325
  17.9 2.2 %collective-permute-done.8.theirs = f32[8,512]{1,0:T(8,128)S(1)} collective-permute-done((f32[8,512]{1,0:T(8,128)S(1)}, f32[8,512]{1,0:T(8,128)S(1)}, u32[]{:S(2)}, u32[]{:S(2)}) %collective-permute-start.8) | collective-permute-done | bytes 16416 | tf_op jit(solution)/shard_map/ppermute | solution.py:325
  20.2 0.2 collective-permute-start.9
  20.3 3.5 %collective-permute-done.9.refs_1_.refs_9_ = f32[4,512]{1,0:T(4,128)S(1)} collective-permute-done((f32[4,512]{1,0:T(4,128)S(1)}, f32[4,512]{1,0:T(4,128)S(1)}, u32[]{:S(2)}, u32[]{:S(2)}) %collective-permute-start.9) | collective-permute-done | bytes 8224 | tf_op jit(solution)/shard_map/ppermute | solution.py:325
  23.8 0.0 collective-permute-start.10
  23.8 2.8 %collective-permute-start.6 = (bf16[144,512]{1,0:T(8,128)(2,1)}, bf16[144,512]{1,0:T(8,128)(2,1)S(1)}, u32[]{:S(2)}, u32[]{:S(2)}) collective-permute-start(bf16[144,512]{1,0:T(8,128)(2,1)} %get-tuple-element.21.refs_0_), channel_id=1, source_target_pairs={{0,7},{1,6},{2,5},{3,4},{4,3},{5,2},{6,1},{7,0},{8,15},{9,14},{10,... | collective-permute-start | bytes 442376 | tf_op jit(solution)/shard_map/ppermute | solution.py:325
  26.6 2.2 %copy-done.1 = bf16[512,4096]{1,0:T(8,128)(2,1)S(1)} copy-done((bf16[512,4096]{1,0:T(8,128)(2,1)S(1)}, bf16[512,4096]{1,0:T(8,128)(2,1)}, u32[]{:S(2)}) %copy-start.1) | copy-done | bytes 4194328
  28.8 1.6 %copy-done.3 = bf16[256,4096]{1,0:T(8,128)(2,1)S(1)} copy-done((bf16[256,4096]{1,0:T(8,128)(2,1)S(1)}, bf16[256,4096]{1,0:T(8,128)(2,1)}, u32[]{:S(2)}) %copy-start.3) | copy-done | bytes 2097176
  30.4 0.9 %copy-done.7 = bf16[2,4096,16]{1,2,0:T(8,128)(2,1)S(1)} copy-done((bf16[2,4096,16]{1,2,0:T(8,128)(2,1)S(1)}, bf16[2,4096,16]{1,2,0:T(8,128)(2,1)}, u32[]{:S(2)}) %copy-start.7) | copy-done | bytes 262168
  31.3 0.5 shard_map.168.refs_12_
  31.8 0.7 %copy-done.5 = bf16[512,1024]{1,0:T(8,128)(2,1)S(1)} copy-done((bf16[512,1024]{1,0:T(8,128)(2,1)S(1)}, bf16[512,1024]{1,0:T(8,128)(2,1)}, u32[]{:S(2)}) %copy-start.5) | copy-done | bytes 1048600
  32.6 0.4 shard_map.170.refs_16_
  33.0 0.0 collective-permute-done.10.refs_2_.refs_10_
  33.0 0.0 copy-start.9
  33.0 0.0 copy-start.10
  33.0 0.0 copy-start.11
  33.0 0.7 collective-permute-start.11
  33.7 0.0 collective-permute-done.3.refs_4_
  33.7 0.7 collective-permute-start.5
  34.4 0.0 collective-permute-done.refs_0_.refs_1_
  34.4 1.8 %collective-permute-start.4 = (bf16[144,512]{1,0:T(8,128)(2,1)S(1)}, bf16[144,512]{1,0:T(8,128)(2,1)S(1)}, u32[]{:S(2)}, u32[]{:S(2)}) collective-permute-start(bf16[144,512]{1,0:T(8,128)(2,1)S(1)} %collective-permute-done.3.refs_4_), channel_id=1, source_target_pairs={{0,1},{1,0},{2,3},{3,2},{4,5},{5,4},{6,7},{7,6},{8,9},{9,8},{10,11... | collective-permute-start | bytes 442376 | tf_op jit(solution)/shard_map/ppermute | solution.py:325
  36.2 0.0 collective-permute-done.2.refs_2_.refs_3_
  36.2 0.1 shard_map.169
  36.3 1.7 %collective-permute-done.11.refs_11_ = f32[16,512]{1,0:T(8,128)S(1)} collective-permute-done((f32[16,512]{1,0:T(8,128)S(1)}, f32[16,512]{1,0:T(8,128)S(1)}, u32[]{:S(2)}, u32[]{:S(2)}) %collective-permute-start.11) | collective-permute-done | bytes 32800 | tf_op jit(solution)/shard_map/ppermute | solution.py:325
  38.0 0.0 collective-permute-done.6.refs_7_
  38.0 1.2 %collective-permute-done.5.refs_6_ = bf16[144,512]{1,0:T(8,128)(2,1)S(1)} collective-permute-done((bf16[144,512]{1,0:T(8,128)(2,1)S(1)}, bf16[144,512]{1,0:T(8,128)(2,1)S(1)}, u32[]{:S(2)}, u32[]{:S(2)}) %collective-permute-start.5) | collective-permute-done | bytes 147488 | tf_op jit(solution)/shard_map/ppermute | solution.py:325
  39.2 0.3 collective-permute-done.4.refs_5_
  39.6 0.0 copy-start.2
  39.6 0.0 copy-start.4
  39.6 0.0 copy-start.14
  39.6 4.1 %shard_map.171 = (bf16[144,4096]{1,0:T(8,128)(2,1)S(1)}, bf16[128,256]{1,0:T(8,128)(2,1)S(1)}, bf16[128,512]{1,0:T(8,128)(2,1)S(1)}, f32[128,256]{1,0:T(8,128)S(...) custom-call(bf16[144,512]{1,0:T(8,128)(2,1)S(1)} %copy-done.8, ...), custom_call_target="tpu_custom_call" | custom-call | flops 905969664 | bytes 6291456 | tf_op jit(solution)/shard_map/pallas_call | solution.py:364
  43.7 0.1 collective-permute-start.12
  43.8 1.6 %collective-permute-done.12.partner.refs_1_ = bf16[1184,128]{1,0:T(8,128)(2,1)S(1)} collective-permute-done((bf16[1184,128]{1,0:T(8,128)(2,1)S(1)}, bf16[1184,128]{1,0:T(8,128)(2,1)S(1)}, u32[]{:S(2)}, u32[]{:S(2)}) %collective-permute-start.12) | collective-permute-done | bytes 303136 | tf_op jit(solution)/shard_map/ppermute | solution.py:325
  45.3 0.1 shard_map.172.refs_0_
  45.4 1.8 %collective-permute-start.13 = (bf16[800,128]{1,0:T(8,128)(2,1)S(1)}, bf16[800,128]{1,0:T(8,128)(2,1)S(1)}, u32[]{:S(2)}, u32[]{:S(2)}) collective-permute-start(bf16[800,128]{1,0:T(8,128)(2,1)S(1)} %shard_map.172.refs_0_), channel_id=1, source_target_pairs={{0,16},{8,24},{16,0},{24,8},{1,17},{9,25},{17,1},{25,9},{2,18},{10... | collective-permute-start | bytes 614408 | tf_op jit(solution)/shard_map/ppermute | solution.py:325
  47.2 2.8 %shard_map.173 = (f32[128,512]{1,0:T(8,128)S(1)}, bf16[128,256]{1,0:T(8,128)(2,1)S(1)}, bf16[128,256]{1,0:T(8,128)(2,1)S(1)}, f32[128,512]{1,0:T(8,128)S(1)}) custom-call(bf16[144,4096]{1,0:T(8,128)(2,1)S(1)} %get-tuple-element.26.normed, bf16[256,4096]{1,0:T(8,128)(2,1)S(1)} %copy-done.4, bf16[512,4096]{1,0:T(8,128)(2,1)S(1)} %copy-done.2, ...), custom_call_target="tpu_custom_call" | custom-call | flops 805306368 | bytes 6291456 | tf_op jit(solution)/shard_map/pallas_call | solution.py:364
  50.0 0.0 copy-start.6
  50.0 2.6 %collective-permute-done.13.refs_2_ = bf16[800,128]{1,0:T(8,128)(2,1)S(1)} collective-permute-done((bf16[800,128]{1,0:T(8,128)(2,1)S(1)}, bf16[800,128]{1,0:T(8,128)(2,1)S(1)}, u32[]{:S(2)}, u32[]{:S(2)}) %collective-permute-start.13) | collective-permute-done | bytes 204832 | tf_op jit(solution)/shard_map/ppermute | solution.py:325
  52.6 0.8 %shard_map.174 = (bf16[128,512]{1,0:T(8,128)(2,1)S(1)}, f32[1,512]{1,0:T(1,128)S(1)}) custom-call(bf16[800,128]{1,0:T(8,128)(2,1)S(1)} %shard_map.172.refs_0_, bf16[1184,128]{1,0:T(8,128)(2,1)S(1)} %collective-permute-done.12.partner.refs_1_, bf16[800,128]{1,0:T(8,128)(2,1)S(1)} %collective-permute-done.13.refs_2_, ...), custom_call_target="tpu_custom_call" | custom-call | flops 67108864 | bytes 524288 | tf_op jit(solution)/shard_map/pallas_call | solution.py:364
  53.4 1.4 %collective-permute-start.19 = (bf16[128,512]{1,0:T(8,128)(2,1)S(1)}, bf16[128,512]{1,0:T(8,128)(2,1)S(1)}, u32[]{:S(2)}, u32[]{:S(2)}) collective-permute-start(bf16[128,512]{1,0:T(8,128)(2,1)S(1)} %get-tuple-element.35.refs_0_), channel_id=1, source_target_pairs={{0,2},{1,3},{2,0},{3,1},{4,6},{5,7},{6,4},{7,5},{8,10},{9,11},{10,... | collective-permute-start | bytes 393224 | tf_op jit(solution)/shard_map/ppermute | solution.py:325
  54.8 2.3 %collective-permute-start.14 = (bf16[128,512]{1,0:T(8,128)(2,1)S(1)}, bf16[128,512]{1,0:T(8,128)(2,1)S(1)}, u32[]{:S(2)}, u32[]{:S(2)}) collective-permute-start(bf16[128,512]{1,0:T(8,128)(2,1)S(1)} %get-tuple-element.35.refs_0_), channel_id=1, source_target_pairs={{0,4},{1,5},{2,6},{3,7},{4,0},{5,1},{6,2},{7,3},{8,12},{9,13},{10,... | collective-permute-start | bytes 393224 | tf_op jit(solution)/shard_map/ppermute | solution.py:325
  57.1 1.5 %collective-permute-start.18 = (bf16[128,512]{1,0:T(8,128)(2,1)S(1)}, bf16[128,512]{1,0:T(8,128)(2,1)S(1)}, u32[]{:S(2)}, u32[]{:S(2)}) collective-permute-start(bf16[128,512]{1,0:T(8,128)(2,1)S(1)} %get-tuple-element.35.refs_0_), channel_id=1, source_target_pairs={{0,1},{1,0},{2,3},{3,2},{4,5},{5,4},{6,7},{7,6},{8,9},{9,8},{10,11... | collective-permute-start | bytes 393224 | tf_op jit(solution)/shard_map/ppermute | solution.py:325
  58.6 1.8 %collective-permute-done.19.refs_2_ = bf16[128,512]{1,0:T(8,128)(2,1)S(1)} collective-permute-done((bf16[128,512]{1,0:T(8,128)(2,1)S(1)}, bf16[128,512]{1,0:T(8,128)(2,1)S(1)}, u32[]{:S(2)}, u32[]{:S(2)}) %collective-permute-start.19) | collective-permute-done | bytes 131104 | tf_op jit(solution)/shard_map/ppermute | solution.py:325
  60.4 2.0 %collective-permute-start.20 = (bf16[128,512]{1,0:T(8,128)(2,1)S(1)}, bf16[128,512]{1,0:T(8,128)(2,1)S(1)}, u32[]{:S(2)}, u32[]{:S(2)}) collective-permute-start(bf16[128,512]{1,0:T(8,128)(2,1)S(1)} %collective-permute-done.19.refs_2_), channel_id=1, source_target_pairs={{0,1},{1,0},{2,3},{3,2},{4,5},{5,4},{6,7},{7,6},{8,9},{9,8},{10,11... | collective-permute-start | bytes 393224 | tf_op jit(solution)/shard_map/ppermute | solution.py:325
  62.4 2.1 %collective-permute-start.17 = (bf16[128,512]{1,0:T(8,128)(2,1)S(1)}, bf16[128,512]{1,0:T(8,128)(2,1)S(1)}, u32[]{:S(2)}, u32[]{:S(2)}) collective-permute-start(bf16[128,512]{1,0:T(8,128)(2,1)S(1)} %get-tuple-element.35.refs_0_), channel_id=1, source_target_pairs={{0,7},{1,6},{2,5},{3,4},{4,3},{5,2},{6,1},{7,0},{8,15},{9,14},{10,... | collective-permute-start | bytes 393224 | tf_op jit(solution)/shard_map/ppermute | solution.py:325
  64.5 0.4 collective-permute-done.14.refs_4_
  64.9 0.6 collective-permute-start.16
  65.5 1.5 %collective-permute-start.15 = (bf16[128,512]{1,0:T(8,128)(2,1)S(1)}, bf16[128,512]{1,0:T(8,128)(2,1)S(1)}, u32[]{:S(2)}, u32[]{:S(2)}) collective-permute-start(bf16[128,512]{1,0:T(8,128)(2,1)S(1)} %collective-permute-done.14.refs_4_), channel_id=1, source_target_pairs={{0,1},{1,0},{2,3},{3,2},{4,5},{5,4},{6,7},{7,6},{8,9},{9,8},{10,11... | collective-permute-start | bytes 393224 | tf_op jit(solution)/shard_map/ppermute | solution.py:325
  67.1 0.0 collective-permute-done.18.refs_1_
  67.1 0.8 %collective-permute-done.20.refs_3_ = bf16[128,512]{1,0:T(8,128)(2,1)S(1)} collective-permute-done((bf16[128,512]{1,0:T(8,128)(2,1)S(1)}, bf16[128,512]{1,0:T(8,128)(2,1)S(1)}, u32[]{:S(2)}, u32[]{:S(2)}) %collective-permute-start.20) | collective-permute-done | bytes 131104 | tf_op jit(solution)/shard_map/ppermute | solution.py:325
  67.9 1.0 %shard_map.175.refs_4_ = f32[128,512]{1,0:T(8,128)S(1)} custom-call(bf16[128,512]{1,0:T(8,128)(2,1)S(1)} %get-tuple-element.35.refs_0_, bf16[128,512]{1,0:T(8,128)(2,1)S(1)} %collective-permute-done.18.refs_1_, bf16[128,512]{1,0:T(8,128)(2,1)S(1)} %collective-permute-done.19.refs_2_, bf16[128,512]{1,0:T(8,128)(2,1)S(1)} %collective-permute-done.20.refs_3_, ...), custom_call_target="tpu_custom_call" | custom-call | flops 335544320 | bytes 2621440 | tf_op jit(solution)/shard_map/pallas_call | solution.py:364
  68.9 1.3 %collective-permute-done.17.refs_2_ = bf16[128,512]{1,0:T(8,128)(2,1)S(1)} collective-permute-done((bf16[128,512]{1,0:T(8,128)(2,1)S(1)}, bf16[128,512]{1,0:T(8,128)(2,1)S(1)}, u32[]{:S(2)}, u32[]{:S(2)}) %collective-permute-start.17) | collective-permute-done | bytes 131104 | tf_op jit(solution)/shard_map/ppermute | solution.py:325
  70.2 0.0 collective-permute-done.16.refs_1_
  70.2 1.3 %collective-permute-done.15.refs_0_ = bf16[128,512]{1,0:T(8,128)(2,1)S(1)} collective-permute-done((bf16[128,512]{1,0:T(8,128)(2,1)S(1)}, bf16[128,512]{1,0:T(8,128)(2,1)S(1)}, u32[]{:S(2)}, u32[]{:S(2)}) %collective-permute-start.15) | collective-permute-done | bytes 131104 | tf_op jit(solution)/shard_map/ppermute | solution.py:325
  71.5 1.3 %shard_map.176 = bf16[128,512]{1,0:T(8,128)(2,1)} custom-call(bf16[128,512]{1,0:T(8,128)(2,1)S(1)} %collective-permute-done.15.refs_0_, bf16[128,512]{1,0:T(8,128)(2,1)S(1)} %collective-permute-done.16.refs_1_, bf16[128,512]{1,0:T(8,128)(2,1)S(1)} %collective-permute-done.17.refs_2_, bf16[512,4096]{1,0:T(8,128)(2,1)S(1)} %copy-done, ...), custom_call_target="tpu_custom_call" | custom-call | flops 201326592 | bytes 1572864 | tf_op jit(solution)/shard_map/pallas_call | solution.py:364
  (22 shorter events, 0.1 us)
Async XLA Ops:
  2.8 9.7 %collective-permute-start.1 = (bf16[144,512]{1,0:T(8,128)(2,1)}, bf16[144,512]{1,0:T(8,128)(2,1)S(1)}, u32[]{:S(2)}, u32[]{:S(2)}) collective-permute-start(bf16[144,512]{1,0:T(8,128)(2,1)} %get-tuple-element.21.refs_0_), channel_id=1, source_target_pairs={{0,2},{1,3},{2,0},{3,1},{4,6},{5,7},{6,4},{7,5},{8,10},{9,11},{10,... | collective-permute-start | bytes 442376 | tf_op jit(solution)/shard_map/ppermute | solution.py:325
  5.9 27.8 %collective-permute-start.3 = (bf16[144,512]{1,0:T(8,128)(2,1)}, bf16[144,512]{1,0:T(8,128)(2,1)S(1)}, u32[]{:S(2)}, u32[]{:S(2)}) collective-permute-start(bf16[144,512]{1,0:T(8,128)(2,1)} %get-tuple-element.21.refs_0_), channel_id=1, source_target_pairs={{0,4},{1,5},{2,6},{3,7},{4,0},{5,1},{6,2},{7,3},{8,12},{9,13},{10,... | collective-permute-start | bytes 442376 | tf_op jit(solution)/shard_map/ppermute | solution.py:325
  8.5 25.9 %collective-permute-start = (bf16[144,512]{1,0:T(8,128)(2,1)}, bf16[144,512]{1,0:T(8,128)(2,1)S(1)}, u32[]{:S(2)}, u32[]{:S(2)}) collective-permute-start(bf16[144,512]{1,0:T(8,128)(2,1)} %get-tuple-element.21.refs_0_), channel_id=1, source_target_pairs={{0,1},{1,0},{2,3},{3,2},{4,5},{5,4},{6,7},{7,6},{8,9},{9,8},{10,11... | collective-permute-start | bytes 442376 | tf_op jit(solution)/shard_map/ppermute | solution.py:325
  12.5 23.7 %collective-permute-start.2 = (bf16[144,512]{1,0:T(8,128)(2,1)S(1)}, bf16[144,512]{1,0:T(8,128)(2,1)S(1)}, u32[]{:S(2)}, u32[]{:S(2)}) collective-permute-start(bf16[144,512]{1,0:T(8,128)(2,1)S(1)} %collective-permute-done.1.refs_1_.refs_2_), channel_id=1, source_target_pairs={{0,1},{1,0},{2,3},{3,2},{4,5},{5,4},{6,7},{7,6},{8,9},{9,8},{10,11... | collective-permute-start | bytes 442376 | tf_op jit(solution)/shard_map/ppermute | solution.py:325
  14.3 1.4 %collective-permute-start.7 = (f32[8,512]{1,0:T(8,128)}, f32[8,512]{1,0:T(8,128)S(1)}, u32[]{:S(2)}, u32[]{:S(2)}) collective-permute-start(f32[8,512]{1,0:T(8,128)} %get-tuple-element.22.mine), channel_id=1, source_target_pairs={{0,8},{8,0},{16,24},{24,16},{1,9},{9,1},{17,25},{25,17},{2,10},{10... | collective-permute-start | bytes 49160 | tf_op jit(solution)/shard_map/ppermute | solution.py:325
  15.7 0.7 copy-start.12
  16.4 3.7 %collective-permute-start.8 = (f32[8,512]{1,0:T(8,128)S(1)}, f32[8,512]{1,0:T(8,128)S(1)}, u32[]{:S(2)}, u32[]{:S(2)}) collective-permute-start(f32[8,512]{1,0:T(8,128)S(1)} %shard_map.164.mine), channel_id=1, source_target_pairs={{0,16},{8,24},{16,0},{24,8},{1,17},{9,25},{17,1},{25,9},{2,18},{10... | collective-permute-start | bytes 49160 | tf_op jit(solution)/shard_map/ppermute | solution.py:325
  20.2 3.7 %collective-permute-start.9 = (f32[4,512]{1,0:T(4,128)S(1)}, f32[4,512]{1,0:T(4,128)S(1)}, u32[]{:S(2)}, u32[]{:S(2)}) collective-permute-start(f32[4,512]{1,0:T(4,128)S(1)} %shard_map.165.refs_0_.refs_8_), channel_id=1, source_target_pairs={{0,1},{1,0},{2,3},{3,2},{4,5},{5,4},{6,7},{7,6},{8,9},{9,8},{10,11... | collective-permute-start | bytes 24584 | tf_op jit(solution)/shard_map/ppermute | solution.py:325
  23.8 9.1 %collective-permute-start.10 = (f32[8,512]{1,0:T(8,128)S(1)}, f32[8,512]{1,0:T(8,128)S(1)}, u32[]{:S(2)}, u32[]{:S(2)}) collective-permute-start(f32[8,512]{1,0:T(8,128)S(1)} %shard_map.166), channel_id=1, source_target_pairs={{0,2},{1,3},{2,0},{3,1},{4,6},{5,7},{6,4},{7,5},{8,10},{9,11},{10,... | collective-permute-start | bytes 49160 | tf_op jit(solution)/shard_map/ppermute | solution.py:325
  23.8 14.2 %collective-permute-start.6 = (bf16[144,512]{1,0:T(8,128)(2,1)}, bf16[144,512]{1,0:T(8,128)(2,1)S(1)}, u32[]{:S(2)}, u32[]{:S(2)}) collective-permute-start(bf16[144,512]{1,0:T(8,128)(2,1)} %get-tuple-element.21.refs_0_), channel_id=1, source_target_pairs={{0,7},{1,6},{2,5},{3,4},{4,3},{5,2},{6,1},{7,0},{8,15},{9,14},{10,... | collective-permute-start | bytes 442376 | tf_op jit(solution)/shard_map/ppermute | solution.py:325
  26.6 2.2 %copy-start.1 = (bf16[512,4096]{1,0:T(8,128)(2,1)S(1)}, bf16[512,4096]{1,0:T(8,128)(2,1)}, u32[]{:S(2)}) copy-start(bf16[512,4096]{1,0:T(8,128)(2,1)} %refs_1_.1) | copy-start | bytes 12582916
  28.8 1.6 %copy-start.3 = (bf16[256,4096]{1,0:T(8,128)(2,1)S(1)}, bf16[256,4096]{1,0:T(8,128)(2,1)}, u32[]{:S(2)}) copy-start(bf16[256,4096]{1,0:T(8,128)(2,1)} %refs_0_.1) | copy-start | bytes 6291460
  30.4 0.9 %copy-start.7 = (bf16[2,4096,16]{1,2,0:T(8,128)(2,1)S(1)}, bf16[2,4096,16]{1,2,0:T(8,128)(2,1)}, u32[]{:S(2)}) copy-start(bf16[2,4096,16]{1,2,0:T(8,128)(2,1)} %param.28) | copy-start | bytes 786436
  31.3 1.2 %copy-start.5 = (bf16[512,1024]{1,0:T(8,128)(2,1)S(1)}, bf16[512,1024]{1,0:T(8,128)(2,1)}, u32[]{:S(2)}) copy-start(bf16[512,1024]{1,0:T(8,128)(2,1)} %weight.1) | copy-start | bytes 3145732
  31.3 1.2 %copy-start.13 = (bf16[1024]{0:T(1024)(128)(2,1)S(1)}, bf16[1024]{0:T(1024)(128)(2,1)}, u32[]{:S(2)}) copy-start(bf16[1024]{0:T(1024)(128)(2,1)} %param.19) | copy-start | bytes 6148
  33.0 6.6 %copy-start.8 = (bf16[144,512]{1,0:T(8,128)(2,1)S(1)}, bf16[144,512]{1,0:T(8,128)(2,1)}, u32[]{:S(2)}) copy-start(bf16[144,512]{1,0:T(8,128)(2,1)} %get-tuple-element.21.refs_0_) | copy-start | bytes 442372
  33.0 6.5 %copy-start.9 = (bf16[2,16,2048]{2,1,0:T(8,128)(2,1)S(1)}, bf16[2,16,2048]{2,1,0:T(8,128)(2,1)}, u32[]{:S(2)}) copy-start(bf16[2,16,2048]{2,1,0:T(8,128)(2,1)} %refs_17_.1) | copy-start | bytes 393220
  33.0 6.5 %copy-start.10 = (f32[2,128,16]{1,2,0:T(8,128)S(1)}, f32[2,128,16]{1,2,0:T(8,128)}, u32[]{:S(2)}) copy-start(f32[2,128,16]{1,2,0:T(8,128)} %param.31) | copy-start | bytes 49156
  33.0 6.5 %copy-start.11 = (f32[2,2048]{1,0:T(2,128)S(1)}, f32[2,2048]{1,0:T(2,128)}, u32[]{:S(2)}) copy-start(f32[2,2048]{1,0:T(2,128)} %refs_18_.1) | copy-start | bytes 49156
  33.0 5.0 %collective-permute-start.11 = (f32[16,512]{1,0:T(8,128)S(1)}, f32[16,512]{1,0:T(8,128)S(1)}, u32[]{:S(2)}, u32[]{:S(2)}) collective-permute-start(f32[16,512]{1,0:T(8,128)S(1)} %shard_map.167), channel_id=1, source_target_pairs={{0,4},{1,5},{2,6},{3,7},{4,0},{5,1},{6,2},{7,3},{8,12},{9,13},{10,... | collective-permute-start | bytes 98312 | tf_op jit(solution)/shard_map/ppermute | solution.py:325
  33.7 5.5 %collective-permute-start.5 = (bf16[144,512]{1,0:T(8,128)(2,1)S(1)}, bf16[144,512]{1,0:T(8,128)(2,1)S(1)}, u32[]{:S(2)}, u32[]{:S(2)}) collective-permute-start(bf16[144,512]{1,0:T(8,128)(2,1)S(1)} %collective-permute-done.3.refs_4_), channel_id=1, source_target_pairs={{0,2},{1,3},{2,0},{3,1},{4,6},{5,7},{6,4},{7,5},{8,10},{9,11},{10,... | collective-permute-start | bytes 442376 | tf_op jit(solution)/shard_map/ppermute | solution.py:325
  34.4 5.1 %collective-permute-start.4 = (bf16[144,512]{1,0:T(8,128)(2,1)S(1)}, bf16[144,512]{1,0:T(8,128)(2,1)S(1)}, u32[]{:S(2)}, u32[]{:S(2)}) collective-permute-start(bf16[144,512]{1,0:T(8,128)(2,1)S(1)} %collective-permute-done.3.refs_4_), channel_id=1, source_target_pairs={{0,1},{1,0},{2,3},{3,2},{4,5},{5,4},{6,7},{7,6},{8,9},{9,8},{10,11... | collective-permute-start | bytes 442376 | tf_op jit(solution)/shard_map/ppermute | solution.py:325
  39.6 7.7 %copy-start.2 = (bf16[512,4096]{1,0:T(8,128)(2,1)S(1)}, bf16[512,4096]{1,0:T(8,128)(2,1)}, u32[]{:S(2)}) copy-start(bf16[512,4096]{1,0:T(8,128)(2,1)} %gate_w.1) | copy-start | bytes 12582916
  39.6 7.7 %copy-start.4 = (bf16[256,4096]{1,0:T(8,128)(2,1)S(1)}, bf16[256,4096]{1,0:T(8,128)(2,1)}, u32[]{:S(2)}) copy-start(bf16[256,4096]{1,0:T(8,128)(2,1)} %query_w.1) | copy-start | bytes 6291460
  39.6 7.7 %copy-start.14 = (f32[512]{0:T(512)S(1)}, f32[512]{0:T(512)}, u32[]{:S(2)}) copy-start(f32[512]{0:T(512)} %param.32) | copy-start | bytes 6148
  43.7 1.7 %collective-permute-start.12 = (bf16[1184,128]{1,0:T(8,128)(2,1)S(1)}, bf16[1184,128]{1,0:T(8,128)(2,1)S(1)}, u32[]{:S(2)}, u32[]{:S(2)}) collective-permute-start(bf16[1184,128]{1,0:T(8,128)(2,1)S(1)} %get-tuple-element.25.own), channel_id=1, source_target_pairs={{0,8},{8,0},{16,24},{24,16},{1,9},{9,1},{17,25},{25,17},{2,10},{10... | collective-permute-start | bytes 909320 | tf_op jit(solution)/shard_map/ppermute | solution.py:325
  45.4 7.2 %collective-permute-start.13 = (bf16[800,128]{1,0:T(8,128)(2,1)S(1)}, bf16[800,128]{1,0:T(8,128)(2,1)S(1)}, u32[]{:S(2)}, u32[]{:S(2)}) collective-permute-start(bf16[800,128]{1,0:T(8,128)(2,1)S(1)} %shard_map.172.refs_0_), channel_id=1, source_target_pairs={{0,16},{8,24},{16,0},{24,8},{1,17},{9,25},{17,1},{25,9},{2,18},{10... | collective-permute-start | bytes 614408 | tf_op jit(solution)/shard_map/ppermute | solution.py:325
  47.2 20.7 %copy-start = (bf16[512,4096]{1,0:T(8,128)(2,1)S(1)}, bf16[512,4096]{1,0:T(8,128)(2,1)}, u32[]{:S(2)}) copy-start(bf16[512,4096]{1,0:T(8,128)(2,1)} %refs_3_.3) | copy-start | bytes 12582916
  50.0 21.4 %copy-start.6 = (bf16[128,512]{1,0:T(8,128)(2,1)S(1)}, bf16[128,512]{1,0:T(8,128)(2,1)}, u32[]{:S(2)}) copy-start(bf16[128,512]{1,0:T(8,128)(2,1)} %refs_5_.5) | copy-start | bytes 393220
  53.4 7.0 %collective-permute-start.19 = (bf16[128,512]{1,0:T(8,128)(2,1)S(1)}, bf16[128,512]{1,0:T(8,128)(2,1)S(1)}, u32[]{:S(2)}, u32[]{:S(2)}) collective-permute-start(bf16[128,512]{1,0:T(8,128)(2,1)S(1)} %get-tuple-element.35.refs_0_), channel_id=1, source_target_pairs={{0,2},{1,3},{2,0},{3,1},{4,6},{5,7},{6,4},{7,5},{8,10},{9,11},{10,... | collective-permute-start | bytes 393224 | tf_op jit(solution)/shard_map/ppermute | solution.py:325
  54.8 10.1 %collective-permute-start.14 = (bf16[128,512]{1,0:T(8,128)(2,1)S(1)}, bf16[128,512]{1,0:T(8,128)(2,1)S(1)}, u32[]{:S(2)}, u32[]{:S(2)}) collective-permute-start(bf16[128,512]{1,0:T(8,128)(2,1)S(1)} %get-tuple-element.35.refs_0_), channel_id=1, source_target_pairs={{0,4},{1,5},{2,6},{3,7},{4,0},{5,1},{6,2},{7,3},{8,12},{9,13},{10,... | collective-permute-start | bytes 393224 | tf_op jit(solution)/shard_map/ppermute | solution.py:325
  57.1 9.9 %collective-permute-start.18 = (bf16[128,512]{1,0:T(8,128)(2,1)S(1)}, bf16[128,512]{1,0:T(8,128)(2,1)S(1)}, u32[]{:S(2)}, u32[]{:S(2)}) collective-permute-start(bf16[128,512]{1,0:T(8,128)(2,1)S(1)} %get-tuple-element.35.refs_0_), channel_id=1, source_target_pairs={{0,1},{1,0},{2,3},{3,2},{4,5},{5,4},{6,7},{7,6},{8,9},{9,8},{10,11... | collective-permute-start | bytes 393224 | tf_op jit(solution)/shard_map/ppermute | solution.py:325
  60.4 7.5 %collective-permute-start.20 = (bf16[128,512]{1,0:T(8,128)(2,1)S(1)}, bf16[128,512]{1,0:T(8,128)(2,1)S(1)}, u32[]{:S(2)}, u32[]{:S(2)}) collective-permute-start(bf16[128,512]{1,0:T(8,128)(2,1)S(1)} %collective-permute-done.19.refs_2_), channel_id=1, source_target_pairs={{0,1},{1,0},{2,3},{3,2},{4,5},{5,4},{6,7},{7,6},{8,9},{9,8},{10,11... | collective-permute-start | bytes 393224 | tf_op jit(solution)/shard_map/ppermute | solution.py:325
  62.4 7.8 %collective-permute-start.17 = (bf16[128,512]{1,0:T(8,128)(2,1)S(1)}, bf16[128,512]{1,0:T(8,128)(2,1)S(1)}, u32[]{:S(2)}, u32[]{:S(2)}) collective-permute-start(bf16[128,512]{1,0:T(8,128)(2,1)S(1)} %get-tuple-element.35.refs_0_), channel_id=1, source_target_pairs={{0,7},{1,6},{2,5},{3,4},{4,3},{5,2},{6,1},{7,0},{8,15},{9,14},{10,... | collective-permute-start | bytes 393224 | tf_op jit(solution)/shard_map/ppermute | solution.py:325
  64.9 5.3 %collective-permute-start.16 = (bf16[128,512]{1,0:T(8,128)(2,1)S(1)}, bf16[128,512]{1,0:T(8,128)(2,1)S(1)}, u32[]{:S(2)}, u32[]{:S(2)}) collective-permute-start(bf16[128,512]{1,0:T(8,128)(2,1)S(1)} %collective-permute-done.14.refs_4_), channel_id=1, source_target_pairs={{0,2},{1,3},{2,0},{3,1},{4,6},{5,7},{6,4},{7,5},{8,10},{9,11},{10,... | collective-permute-start | bytes 393224 | tf_op jit(solution)/shard_map/ppermute | solution.py:325
  65.5 5.9 %collective-permute-start.15 = (bf16[128,512]{1,0:T(8,128)(2,1)S(1)}, bf16[128,512]{1,0:T(8,128)(2,1)S(1)}, u32[]{:S(2)}, u32[]{:S(2)}) collective-permute-start(bf16[128,512]{1,0:T(8,128)(2,1)S(1)} %collective-permute-done.14.refs_4_), channel_id=1, source_target_pairs={{0,1},{1,0},{2,3},{3,2},{4,5},{5,4},{6,7},{7,6},{8,9},{9,8},{10,11... | collective-permute-start | bytes 393224 | tf_op jit(solution)/shard_map/ppermute | solution.py:325

commit v2 on v1

--- a/solution.py
+++ b/solution.py
@@ -489,8 +489,8 @@
     mods = refs[count : count + count.bit_length()]
     refs = refs[count + count.bit_length() :]
     weights, early_sums, early_squares, spikes, gate_part = refs[:5]
-    normed, keys, values, cum_f, cum_b, payload = refs[7:13]
-    up_own, bias_own, sems = refs[13:]
+    normed, keys, values, cum_f, cum_b, payload, extra = refs[7:14]
+    up_own, bias_own, sems = refs[14:]
     tp = lax.axis_index("tp")
     half = heads * DK
     first = pl.multiple_of(tp * half, half)
@@ -599,6 +599,7 @@
         payload[at : at + ctx, :] = value_all[tokens:, c * DK : (c + 1) * DK]
     payload[2 * size : start, :] = growth_block(growth, heads)
     payload[start + 4 * heads * ctx :, :] = gate_part[...]
+    extra[...] = payload[2 * size :, :]
 
 
 def growth_rows(heads):
@@ -616,21 +617,13 @@
     return block[kind * heads + h : kind * heads + h + 1]
 
 
-def within_kernel(
-    heads,
-    normed,
-    query_w,
-    gate_w,
-    keys,
-    values,
-    cum_f,
-    cum_b,
-    gain,
-    inside,
-    reach_f,
-    reach_b,
-    gated,
-):
+def gated_kernel(normed, gate_w, gain, gated):
+    products = matmul(gate_w[...], normed[: gated.shape[0], :], NT).T
+    gates = products.astype(bf16).astype(f32)
+    gated[...] = gates * jax.nn.sigmoid(gates) * gain[...]
+
+
+def within_kernel(heads, normed, query_w, keys, values, cum_f, cum_b, inside, reach_f, reach_b):
     tokens = keys.shape[0]
     rows_in = normed[:tokens, :]
     query_all = matmul(rows_in, query_w[...], NT).astype(bf16).astype(f32) * DK ** (-0.5)
@@ -668,128 +661,100 @@
             after = sum(ends_b[b + 1 :], jnp.zeros_like(ends_b[0]))
             reach_f[rows, own] = (qf[rows] * jnp.exp(before)).astype(bf16)
             reach_b[rows, own] = (qb[rows] * jnp.exp(after)).astype(bf16)
-    gates = matmul(rows_in, gate_w[...], NT).astype(bf16).astype(f32)
-    gated[...] = gains_of(gates, gain[...])
-
-
-def gains_of(gates, gain):
-    return gates * jax.nn.sigmoid(gates) * gain
-
-
-def merge_kernel(bit, final, heads, ctx, width, own, partner, out):
-    gate_rows = gate_rows_of(width)
-    size = (own.shape[0] - growth_rows(heads) - 4 * heads * ctx - gate_rows) // 2
+
+
+def merge_kernel(heads, own, partner, out):
     lift = growth_rows(heads)
-    states = 1 if final else 2
+    size = out.shape[0] - lift
+    wide = size // heads
     sp = lax.axis_index("sp")
-    side = lax.bitwise_and(lax.shift_right_logical(sp, bit), 1)
-    onward = lax.bitwise_and(lax.shift_right_logical(sp, bit + 1), 1)
 
     def emit(low, up):
-        wide = size // heads
-
-        def forward(at):
+        def forward():
             for h in range(heads):
                 rows = slice(h * wide, (h + 1) * wide)
                 decayed = growth_of(up, 2 * size, 0, h, heads) * low[rows, :].astype(f32)
-                out[at + h * wide : at + (h + 1) * wide, :] = (
-                    decayed + up[rows, :].astype(f32)
-                ).astype(bf16)
-
-        def backward(at):
+                out[rows, :] = (decayed + up[rows, :].astype(f32)).astype(bf16)
+
+        def backward():
             for h in range(heads):
                 rows = slice(size + h * wide, size + (h + 1) * wide)
                 decayed = growth_of(low, 2 * size, 1, h, heads) * up[rows, :].astype(f32)
-                out[at + h * wide : at + (h + 1) * wide, :] = (
+                out[h * wide : (h + 1) * wide, :] = (
                     decayed + low[rows, :].astype(f32)
                 ).astype(bf16)
 
-        if final:
-            pl.when(onward == 0)(lambda: forward(0))
-            pl.when(onward == 1)(lambda: backward(0))
-        else:
-            forward(0)
-            backward(size)
-        out[states * size : states * size + lift, :] = (
-            low[2 * size : 2 * size + lift, :].astype(f32)
-            * up[2 * size : 2 * size + lift, :].astype(f32)
-        ).astype(bf16)
-        base_in, base_out = (2 * size + lift, states * size + lift)
-        count = out.shape[0]
-        mine = joined_row(low[low.shape[0] - gate_rows :, :], width)
-        theirs = joined_row(up[up.shape[0] - gate_rows :, :], width)
-        out[count - gate_rows :, :] = split_row(mine + theirs)
-        for section in range(4 * heads):
-            before = low[base_in + section * ctx : base_in + (section + 1) * ctx, :]
-            after = up[base_in + section * ctx : base_in + (section + 1) * ctx, :]
-            if section < heads:
-                before = before.astype(f32) * growth_of(up, 2 * size, 2, section, heads)
-            elif section < 2 * heads:
-                after = after.astype(f32) * growth_of(low, 2 * size, 3, section - heads, heads)
-            at = base_out + 2 * section * ctx
-            out[at : at + ctx, :] = before.astype(bf16)
-            out[at + ctx : at + 2 * ctx, :] = after.astype(bf16)
-
-    pl.when(side == 0)(lambda: emit(own, partner))
-    pl.when(side == 1)(lambda: emit(partner, own))
-
-
-def finish_kernel(steps, heads, ctx, *refs):
-    own = refs[0]
-    partners = refs[1 : 1 + steps]
-    inside, reach_f, reach_b, gated, out, gates, start_f, start_b, grow_f, grow_b = refs[1 + steps :]
+        pl.when(sp < 2)(forward)
+        pl.when(sp >= 2)(backward)
+        rates = slice(2 * size, 2 * size + lift)
+        out[size:, :] = (low[rates, :].astype(f32) * up[rates, :].astype(f32)).astype(bf16)
+
+    pl.when(sp % 2 == 0)(lambda: emit(own, partner))
+    pl.when(sp % 2 == 1)(lambda: emit(partner, own))
+
+
+def finish_kernel(heads, ctx, *refs):
+    own, partner, other, far, pair = refs[:5]
+    inside, reach_f, reach_b, gated, out, gates = refs[5:11]
+    start_f, start_b, grow_f, grow_b, shared = refs[11:]
     sp = lax.axis_index("sp")
     size = start_f.shape[0]
     wide = size // heads
+    lift = growth_rows(heads)
+    devices, rows_shared, _ = shared.shape
     start_f[...] = jnp.zeros(start_f.shape, f32)
     start_b[...] = jnp.zeros(start_b.shape, f32)
     grow_f[...] = jnp.ones(grow_f.shape, f32)
     grow_b[...] = jnp.ones(grow_b.shape, f32)
 
-    def take(start, grow, partner, at, kind, states):
+    def take(start, grow, source, at, kind, rates):
         for h in range(heads):
             rows = slice(h * wide, (h + 1) * wide)
             one = slice(h, h + 1)
-            theirs = partner[at + h * wide : at + (h + 1) * wide, :].astype(f32)
+            theirs = source[at + h * wide : at + (h + 1) * wide, :].astype(f32)
             start[rows, :] = start[rows, :] + grow[one, :] * theirs
-            grow[one, :] = grow[one, :] * growth_of(partner, states * size, kind, h, heads)
-
-    for step in range(steps):
-        side = lax.bitwise_and(lax.shift_right_logical(sp, step), 1)
-        states = 1 if step == steps - 1 and steps > 1 else 2
-        partner = partners[step]
-        back = size if states == 2 else 0
-        pl.when(side == 1)(functools.partial(take, start_f, grow_f, partner, 0, 0, states))
-        pl.when(side == 0)(functools.partial(take, start_b, grow_b, partner, back, 1, states))
-
-    states = 1 if steps > 1 else 2
-    lift = growth_rows(heads)
-    base = states * size + lift
-    rows_each = ctx << (steps - 1)
-
-    def context(low, up):
-        def part(ref, section):
-            return ref[base + section * rows_each : base + (section + 1) * rows_each, :]
-
-        for h in range(heads):
-            one = slice(h, h + 1)
-            grow_up = growth_of(up, states * size, 2, h, heads)
-            grow_low = growth_of(low, states * size, 3, h, heads)
-            kf = [(part(low, h).astype(f32) * grow_up).astype(bf16), part(up, h)]
-            kb = [part(low, heads + h), (part(up, heads + h).astype(f32) * grow_low).astype(bf16)]
-            first = 2 * heads + h * (wide // DK)
-            for c in range(wide // DK):
-                vs = jnp.concatenate([part(low, first + c), part(up, first + c)], axis=0)
-                at = slice(h * wide + c * DK, h * wide + (c + 1) * DK)
-                start_f[at, :] += grow_f[one, :] * matmul(vs, jnp.concatenate(kf, axis=0), TN)
-                start_b[at, :] += grow_b[one, :] * matmul(vs, jnp.concatenate(kb, axis=0), TN)
-
-    side = lax.bitwise_and(lax.shift_right_logical(sp, steps - 1), 1)
-    pl.when(side == 0)(lambda: context(own, partners[-1]))
-    pl.when(side == 1)(lambda: context(partners[-1], own))
+            grow[one, :] = grow[one, :] * growth_of(source, rates, kind, h, heads)
+
+    pl.when(sp % 2 == 1)(functools.partial(take, start_f, grow_f, partner, 0, 0, 2 * size))
+    pl.when(sp % 2 == 0)(functools.partial(take, start_b, grow_b, partner, size, 1, 2 * size))
+    pl.when(sp >= 2)(functools.partial(take, start_f, grow_f, pair, 0, 0, size))
+    pl.when(sp < 2)(functools.partial(take, start_b, grow_b, pair, 0, 1, size))
+    shared[sp] = own[:rows_shared, :]
+    shared[lax.bitwise_xor(sp, 1)] = partner[2 * size : 2 * size + rows_shared, :]
+    shared[lax.bitwise_xor(sp, 2)] = other[:rows_shared, :]
+    shared[lax.bitwise_xor(sp, 3)] = far[:rows_shared, :]
+
+    def part(d, section):
+        return shared[d, lift + section * ctx : lift + (section + 1) * ctx, :]
+
+    def rate(d, kind, h):
+        return shared[d, :lift, :].astype(f32)[kind * heads + h : kind * heads + h + 1]
+
+    def chained(order, kind, h, section):
+        rows, running = ({}, None)
+        for d in order:
+            rows[d] = part(d, section)
+            if running is not None:
+                rows[d] = (rows[d].astype(f32) * running).astype(bf16)
+            running = rate(d, kind, h) if running is None else running * rate(d, kind, h)
+        return jnp.concatenate([rows[d] for d in range(devices)], axis=0)
+
+    for h in range(heads):
+        one = slice(h, h + 1)
+        kf = chained(range(devices - 1, -1, -1), 2, h, h)
+        kb = chained(range(devices), 3, h, heads + h)
+        first = 2 * heads + h * (wide // DK)
+        for c in range(wide // DK):
+            vs = jnp.concatenate([part(d, first + c) for d in range(devices)], axis=0)
+            at = slice(h * wide + c * DK, h * wide + (c + 1) * DK)
+            start_f[at, :] += grow_f[one, :] * matmul(vs, kf, TN)
+            start_b[at, :] += grow_b[one, :] * matmul(vs, kb, TN)
     width = gates.shape[1]
-    last = own.shape[0] - gate_rows_of(width)
-    gates[...] = joined_row(own[last:, :], width) + joined_row(partners[-1][last:, :], width)
+    total = None
+    for ref in (own, partner, other, far):
+        row = joined_row(ref[ref.shape[0] - gate_rows_of(width) :, :], width)
+        total = row if total is None else total + row
+    gates[...] = total
     i = lax.broadcasted_iota(jnp.int32, (DK, DK), 0)
     j = lax.broadcasted_iota(jnp.int32, (DK, DK), 1)
     shift = VGROUP.bit_length() - 1
@@ -944,7 +909,8 @@
         SURVEY_FLOPS,
         SURVEY_BYTES,
     )
-    normed, keys, values, cum_f, cum_b, payload = call(
+    extra_rows = lift + 4 * heads * ctx + gate_rows_of(width)
+    normed, keys, values, cum_f, cum_b, payload, extra = call(
         functools.partial(project_kernel, tp_count, tokens, heads, surveyed),
         [
             shape((total, features), bf16),
@@ -952,7 +918,8 @@
             shape((tokens, vdim), bf16),
             shape((tokens, half), f32),
             shape((tokens, half), f32),
-            shape((2 * vdim + lift + 4 * heads * ctx + gate_rows_of(width), DK), bf16),
+            shape((2 * vdim + extra_rows, DK), bf16),
+            shape((extra_rows, DK), bf16),
         ],
         [VMEM_SPEC] * (tp_count + len(mods) + 5) + [HBM_SPEC] * 2,
         (
@@ -973,48 +940,43 @@
             pltpu.SemaphoreType.DMA((2,)),
         ],
     )
-    partners = [exchange(payload, "sp", 1)]
-    rows = ctx
-    for bit in range(steps - 1):
-        final = bit == steps - 2
-        states = 1 if final else 2
-        payload = call(
-            functools.partial(merge_kernel, bit, final, heads, rows, width),
-            shape((states * vdim + lift + 8 * heads * rows + gate_rows_of(width), DK), bf16),
-            [VMEM_SPEC, VMEM_SPEC],
-            (payload, partners[-1]),
-            4 * vdim * DK,
-            8 * vdim * DK,
-        )
-        rows = 2 * rows
-        partners.append(exchange(payload, "sp", 2 << bit))
-    inside, reach_f, reach_b, gated = call(
+    partner = exchange(payload, "sp", 1)
+    other = exchange(extra, "sp", 2)
+    pair = call(
+        functools.partial(merge_kernel, heads),
+        shape((vdim + lift, DK), bf16),
+        [VMEM_SPEC, VMEM_SPEC],
+        (payload, partner),
+        4 * vdim * DK,
+        8 * vdim * DK,
+    )
+    pair = exchange(pair, "sp", 2)
+    inside, reach_f, reach_b = call(
         functools.partial(within_kernel, heads),
         [
             shape((tokens, vdim), f32),
             shape((tokens, half), bf16),
             shape((tokens, half), bf16),
-            shape((tokens, vdim), f32),
         ],
-        [VMEM_SPEC] * 8,
-        (
-            normed,
-            query_matrix,
-            gate_matrix,
-            keys,
-            values,
-            cum_f,
-            cum_b,
-            output_gain[None],
-        ),
-        2 * tokens * features * (half + vdim),
-        2 * features * (half + vdim),
+        [VMEM_SPEC] * 6,
+        (normed, query_matrix, keys, values, cum_f, cum_b),
+        2 * tokens * features * half,
+        2 * features * half,
+    )
+    far = exchange(other, "sp", 1)
+    gated = call(
+        gated_kernel,
+        shape((tokens, vdim), f32),
+        [VMEM_SPEC] * 3,
+        (normed, gate_matrix, output_gain[None]),
+        2 * tokens * features * vdim,
+        2 * features * vdim,
     )
     heads_out, gates = call(
-        functools.partial(finish_kernel, steps, heads, ctx),
+        functools.partial(finish_kernel, heads, ctx),
         [shape((tokens, vdim), bf16), shape((1, width), f32)],
-        [VMEM_SPEC] * (5 + steps),
-        (payload, *partners, inside, reach_f, reach_b, gated),
+        [VMEM_SPEC] * 9,
+        (extra, partner, other, far, pair, inside, reach_f, reach_b, gated),
         8 * tokens * vdim * DK,
         8 * tokens * vdim,
         [
@@ -1022,6 +984,7 @@
             pltpu.VMEM((vdim, DK), f32),
             pltpu.VMEM((8 * -(-heads // 8), DK), f32),
             pltpu.VMEM((8 * -(-heads // 8), DK), f32),
+            pltpu.VMEM((sp_count, lift + 4 * heads * ctx, DK), bf16),
         ],
     )
     branches = gathered_pieces(heads_out, "tp", "out")
@@ -1067,8 +1030,8 @@
         P("tp", None),
     )
     tp_count, sp_count = (mesh.shape["tp"], mesh.shape["sp"])
-    powers = tp_count & tp_count - 1 == 0 and sp_count & sp_count - 1 == 0
-    direct = 2 <= tp_count <= HEADS and sp_count >= 2 and powers
+    powers = tp_count & tp_count - 1 == 0
+    direct = 2 <= tp_count <= HEADS and sp_count == 4 and powers
     return jax.shard_map(
         local_direct if direct else local_general, mesh=mesh, in_specs=placed, out_specs=P("sp", "tp"), check_vma=False
     )

time: 73.1 us -> 75.3 us (1.030)
  waiting for transfers between devices: 22.6 us -> 26.1 us
  starting transfers between devices: 30 us -> 28.6 us
    ppermute x21 -> x23, waiting for transfers between devices: 22.6 us -> 26.1 us  [exchange(): lax.ppermute(value, axis, [(i, i ^ distance) for i in range(lax.axis_size...]
    ppermute x21 -> x23, starting transfers between devices: 30 us -> 28.6 us  [exchange(): lax.ppermute(value, axis, [(i, i ^ distance) for i in range(lax.axis_size...]
    pallas_call x14 -> x15, Pallas kernels: 13.8 us -> 13.8 us  [call(): pl.pallas_call(kernel, out_shape=out_shapes, in_specs=in_specs, out_specs...]
  transfers between devices with their start and end apart: 21 -> 23, of which waited for: 14 -> 12; matrix products, arithmetic and copies ran while one was open for 0% -> 0% of each run, Pallas kernels for 7% -> 6%
where the time goes in v2:
time: 75.3 us; the launch traced here: 75 us
  starting transfers between devices  28.6 us (38%)
  waiting for transfers between devices  26.1 us (35%)
  Pallas kernels  13.8 us (18%)
  local copies, waits for them, and re-layouts  6.25 us (8%)
    ppermute x23, starting transfers between devices, exchange(): lax.ppermute(value, axis, [(i, i ^ distance) for i in range(lax.axis_size...  28.6 us
    ppermute x23, waiting for transfers between devices, exchange(): lax.ppermute(value, axis, [(i, i ^ distance) for i in range(lax.axis_size...  26.1 us
    pallas_call x15, Pallas kernels, call(): pl.pallas_call(kernel, out_shape=out_shapes, in_specs=in_specs, out_specs...  13.8 us
    unnamed x30, local copies, waits for them, and re-layouts  6.25 us
  transfers between devices with their start and end apart: 23, of which 12 were waited for; matrix products, arithmetic and copies ran while one was open for 0% of the time, Pallas kernels for 6%

profile of v2, /device:TPU:0, one launch (start us, length us, event | category | flops | bytes accessed | tf_op | source)
XLA Modules:
  0.0 75.0 jit_solution(6823530929519269587)
XLA Ops:
  0.0 2.7 %shard_map.163 = (f32[8,512]{1,0:T(8,128)}, bf16[144,512]{1,0:T(8,128)(2,1)}) custom-call(bf16[8,128]{1,0:T(8,128)(2,1)} %bitcast.9, bf16[8,128]{1,0:T(8,128)(2,1)} %bitcast.12, bf16[512,1024]{1,0:T(8,128)(2,1)} %refs_2_.1, bf16[512,1024]{1,0:T(8,128)(2,1)} %refs_3_.2, bf16[128,512]{1,0:T(8,128)(2,1)} %refs_5_.5, bf16[16,512]{1,0:T(8,128)(2,1)} %refs_5_.3), custom_call_target="tpu_custom_call" | custom-call | flops 16777216 | bytes 2097152 | tf_op jit(solution)/shard_map/pallas_call | solution.py:364
  2.7 3.1 %collective-permute-start.1 = (bf16[144,512]{1,0:T(8,128)(2,1)}, bf16[144,512]{1,0:T(8,128)(2,1)S(1)}, u32[]{:S(2)}, u32[]{:S(2)}) collective-permute-start(bf16[144,512]{1,0:T(8,128)(2,1)} %get-tuple-element.21.refs_0_), channel_id=1, source_target_pairs={{0,2},{1,3},{2,0},{3,1},{4,6},{5,7},{6,4},{7,5},{8,10},{9,11},{10,... | collective-permute-start | bytes 442376 | tf_op jit(solution)/shard_map/ppermute | solution.py:325
  5.9 2.6 %collective-permute-start.3 = (bf16[144,512]{1,0:T(8,128)(2,1)}, bf16[144,512]{1,0:T(8,128)(2,1)S(1)}, u32[]{:S(2)}, u32[]{:S(2)}) collective-permute-start(bf16[144,512]{1,0:T(8,128)(2,1)} %get-tuple-element.21.refs_0_), channel_id=1, source_target_pairs={{0,4},{1,5},{2,6},{3,7},{4,0},{5,1},{6,2},{7,3},{8,12},{9,13},{10,... | collective-permute-start | bytes 442376 | tf_op jit(solution)/shard_map/ppermute | solution.py:325
  8.5 1.5 %collective-permute-start = (bf16[144,512]{1,0:T(8,128)(2,1)}, bf16[144,512]{1,0:T(8,128)(2,1)S(1)}, u32[]{:S(2)}, u32[]{:S(2)}) collective-permute-start(bf16[144,512]{1,0:T(8,128)(2,1)} %get-tuple-element.21.refs_0_), channel_id=1, source_target_pairs={{0,1},{1,0},{2,3},{3,2},{4,5},{5,4},{6,7},{7,6},{8,9},{9,8},{10,11... | collective-permute-start | bytes 442376 | tf_op jit(solution)/shard_map/ppermute | solution.py:325
  10.0 2.5 %collective-permute-done.1.refs_1_.refs_2_ = bf16[144,512]{1,0:T(8,128)(2,1)S(1)} collective-permute-done((bf16[144,512]{1,0:T(8,128)(2,1)}, bf16[144,512]{1,0:T(8,128)(2,1)S(1)}, u32[]{:S(2)}, u32[]{:S(2)}) %collective-permute-start.1) | collective-permute-done | bytes 147488 | tf_op jit(solution)/shard_map/ppermute | solution.py:325
  12.5 1.8 %collective-permute-start.2 = (bf16[144,512]{1,0:T(8,128)(2,1)S(1)}, bf16[144,512]{1,0:T(8,128)(2,1)S(1)}, u32[]{:S(2)}, u32[]{:S(2)}) collective-permute-start(bf16[144,512]{1,0:T(8,128)(2,1)S(1)} %collective-permute-done.1.refs_1_.refs_2_), channel_id=1, source_target_pairs={{0,1},{1,0},{2,3},{3,2},{4,5},{5,4},{6,7},{7,6},{8,9},{9,8},{10,11... | collective-permute-start | bytes 442376 | tf_op jit(solution)/shard_map/ppermute | solution.py:325
  14.3 0.0 collective-permute-start.7
  14.3 1.4 %collective-permute-done.7.theirs = f32[8,512]{1,0:T(8,128)S(1)} collective-permute-done((f32[8,512]{1,0:T(8,128)}, f32[8,512]{1,0:T(8,128)S(1)}, u32[]{:S(2)}, u32[]{:S(2)}) %collective-permute-start.7) | collective-permute-done | bytes 16416 | tf_op jit(solution)/shard_map/ppermute | solution.py:325
  15.7 0.7 copy-done.12
  16.4 1.5 %collective-permute-start.8 = (f32[8,512]{1,0:T(8,128)S(1)}, f32[8,512]{1,0:T(8,128)S(1)}, u32[]{:S(2)}, u32[]{:S(2)}) collective-permute-start(f32[8,512]{1,0:T(8,128)S(1)} %shard_map.164.mine), channel_id=1, source_target_pairs={{0,16},{8,24},{16,0},{24,8},{1,17},{9,25},{17,1},{25,9},{2,18},{10... | collective-permute-start | bytes 49160 | tf_op jit(solution)/shard_map/ppermute | solution.py:325
  17.9 2.2 %collective-permute-done.8.theirs = f32[8,512]{1,0:T(8,128)S(1)} collective-permute-done((f32[8,512]{1,0:T(8,128)S(1)}, f32[8,512]{1,0:T(8,128)S(1)}, u32[]{:S(2)}, u32[]{:S(2)}) %collective-permute-start.8) | collective-permute-done | bytes 16416 | tf_op jit(solution)/shard_map/ppermute | solution.py:325
  20.2 0.2 collective-permute-start.9
  20.3 3.5 %collective-permute-done.9.refs_1_.refs_9_ = f32[4,512]{1,0:T(4,128)S(1)} collective-permute-done((f32[4,512]{1,0:T(4,128)S(1)}, f32[4,512]{1,0:T(4,128)S(1)}, u32[]{:S(2)}, u32[]{:S(2)}) %collective-permute-start.9) | collective-permute-done | bytes 8224 | tf_op jit(solution)/shard_map/ppermute | solution.py:325
  23.8 0.0 collective-permute-start.10
  23.8 2.8 %collective-permute-start.6 = (bf16[144,512]{1,0:T(8,128)(2,1)}, bf16[144,512]{1,0:T(8,128)(2,1)S(1)}, u32[]{:S(2)}, u32[]{:S(2)}) collective-permute-start(bf16[144,512]{1,0:T(8,128)(2,1)} %get-tuple-element.21.refs_0_), channel_id=1, source_target_pairs={{0,7},{1,6},{2,5},{3,4},{4,3},{5,2},{6,1},{7,0},{8,15},{9,14},{10,... | collective-permute-start | bytes 442376 | tf_op jit(solution)/shard_map/ppermute | solution.py:325
  26.6 2.2 %copy-done.1 = bf16[512,4096]{1,0:T(8,128)(2,1)S(1)} copy-done((bf16[512,4096]{1,0:T(8,128)(2,1)S(1)}, bf16[512,4096]{1,0:T(8,128)(2,1)}, u32[]{:S(2)}) %copy-start.1) | copy-done | bytes 4194328
  28.8 1.6 %copy-done.3 = bf16[256,4096]{1,0:T(8,128)(2,1)S(1)} copy-done((bf16[256,4096]{1,0:T(8,128)(2,1)S(1)}, bf16[256,4096]{1,0:T(8,128)(2,1)}, u32[]{:S(2)}) %copy-start.3) | copy-done | bytes 2097176
  30.4 0.9 %copy-done.7 = bf16[2,4096,16]{1,2,0:T(8,128)(2,1)S(1)} copy-done((bf16[2,4096,16]{1,2,0:T(8,128)(2,1)S(1)}, bf16[2,4096,16]{1,2,0:T(8,128)(2,1)}, u32[]{:S(2)}) %copy-start.7) | copy-done | bytes 262168
  31.3 0.5 shard_map.168.refs_12_
  31.8 0.7 copy-done.5
  32.6 0.4 shard_map.170.refs_16_
  33.0 0.0 collective-permute-done.10.refs_2_.refs_10_
  33.0 0.0 copy-start.9
  33.0 0.0 copy-start.10
  33.0 0.0 copy-start.11
  33.0 0.7 collective-permute-start.11
  33.7 0.0 collective-permute-done.3.refs_4_
  33.7 0.7 collective-permute-start.5
  34.4 1.8 %collective-permute-start.4 = (bf16[144,512]{1,0:T(8,128)(2,1)S(1)}, bf16[144,512]{1,0:T(8,128)(2,1)S(1)}, u32[]{:S(2)}, u32[]{:S(2)}) collective-permute-start(bf16[144,512]{1,0:T(8,128)(2,1)S(1)} %collective-permute-done.3.refs_4_), channel_id=1, source_target_pairs={{0,1},{1,0},{2,3},{3,2},{4,5},{5,4},{6,7},{7,6},{8,9},{9,8},{10,11... | collective-permute-start | bytes 442376 | tf_op jit(solution)/shard_map/ppermute | solution.py:325
  36.2 0.0 collective-permute-done.2.refs_2_.refs_3_
  36.2 0.1 shard_map.169
  36.3 1.7 %collective-permute-done.11.refs_11_ = f32[16,512]{1,0:T(8,128)S(1)} collective-permute-done((f32[16,512]{1,0:T(8,128)S(1)}, f32[16,512]{1,0:T(8,128)S(1)}, u32[]{:S(2)}, u32[]{:S(2)}) %collective-permute-start.11) | collective-permute-done | bytes 32800 | tf_op jit(solution)/shard_map/ppermute | solution.py:325
  38.0 0.0 collective-permute-done.6.refs_7_
  38.0 1.2 %collective-permute-done.5.refs_6_ = bf16[144,512]{1,0:T(8,128)(2,1)S(1)} collective-permute-done((bf16[144,512]{1,0:T(8,128)(2,1)S(1)}, bf16[144,512]{1,0:T(8,128)(2,1)S(1)}, u32[]{:S(2)}, u32[]{:S(2)}) %collective-permute-start.5) | collective-permute-done | bytes 147488 | tf_op jit(solution)/shard_map/ppermute | solution.py:325
  39.2 0.3 collective-permute-done.4.refs_5_
  39.6 0.0 copy-start.4
  39.6 4.1 %shard_map.171 = (bf16[144,4096]{1,0:T(8,128)(2,1)S(1)}, bf16[128,256]{1,0:T(8,128)(2,1)S(1)}, bf16[128,512]{1,0:T(8,128)(2,1)S(1)}, f32[128,256]{1,0:T(8,128)S(...) custom-call(bf16[144,512]{1,0:T(8,128)(2,1)S(1)} %copy-done.8, ...), custom_call_target="tpu_custom_call" | custom-call | flops 905969664 | bytes 6291456 | tf_op jit(solution)/shard_map/pallas_call | solution.py:364
  43.7 0.0 copy-start.2
  43.7 0.0 copy-start.14
  43.7 0.1 collective-permute-start.12
  43.8 1.6 %collective-permute-done.12.partner.refs_1_ = bf16[1184,128]{1,0:T(8,128)(2,1)S(1)} collective-permute-done((bf16[1184,128]{1,0:T(8,128)(2,1)S(1)}, bf16[1184,128]{1,0:T(8,128)(2,1)S(1)}, u32[]{:S(2)}, u32[]{:S(2)}) %collective-permute-start.12) | collective-permute-done | bytes 303136 | tf_op jit(solution)/shard_map/ppermute | solution.py:325
  45.3 0.1 shard_map.172
  45.4 1.8 %collective-permute-start.15 = (bf16[528,128]{1,0:T(8,128)(2,1)S(1)}, bf16[528,128]{1,0:T(8,128)(2,1)S(1)}, u32[]{:S(2)}, u32[]{:S(2)}) collective-permute-start(bf16[528,128]{1,0:T(8,128)(2,1)S(1)} %shard_map.172), channel_id=1, source_target_pairs={{0,16},{8,24},{16,0},{24,8},{1,17},{9,25},{17,1},{25,9},{2,18},{10... | collective-permute-start | bytes 405512 | tf_op jit(solution)/shard_map/ppermute | solution.py:325
  47.2 0.3 collective-permute-start.13
  47.5 1.5 %shard_map.173 = (f32[128,512]{1,0:T(8,128)S(1)}, bf16[128,256]{1,0:T(8,128)(2,1)S(1)}, bf16[128,256]{1,0:T(8,128)(2,1)S(1)}) custom-call(bf16[144,4096]{1,0:T(8,128)(2,1)S(1)} %get-tuple-element.27.normed, bf16[256,4096]{1,0:T(8,128)(2,1)S(1)} %copy-done.4, bf16[128,256]{1,0:T(8,128)(2,1)S(1)} %get-tuple-element.28.keys, ...), custom_call_target="tpu_custom_call" | custom-call | flops 268435456 | bytes 2097152 | tf_op jit(solution)/shard_map/pallas_call | solution.py:364
  49.0 0.0 copy-start
  49.0 3.0 %collective-permute-done.13.refs_2_ = bf16[160,128]{1,0:T(8,128)(2,1)S(1)} collective-permute-done((bf16[160,128]{1,0:T(8,128)(2,1)S(1)}, bf16[160,128]{1,0:T(8,128)(2,1)S(1)}, u32[]{:S(2)}, u32[]{:S(2)}) %collective-permute-start.13) | collective-permute-done | bytes 40992 | tf_op jit(solution)/shard_map/ppermute | solution.py:325
  52.0 0.0 collective-permute-start.14
  52.0 1.3 %shard_map.174.refs_8_ = f32[128,512]{1,0:T(8,128)S(1)} custom-call(bf16[144,4096]{1,0:T(8,128)(2,1)S(1)} %get-tuple-element.27.normed, bf16[512,4096]{1,0:T(8,128)(2,1)S(1)} %copy-done.2, f32[1,512]{1,0:T(1,128)S(1)} %bitcast.11), custom_call_target="tpu_custom_call" | custom-call | flops 536870912 | bytes 4194304 | tf_op jit(solution)/shard_map/pallas_call | solution.py:364
  53.3 0.0 copy-start.6
  53.3 0.0 collective-permute-done.14.refs_3_
  53.4 0.8 %shard_map.175 = (bf16[128,512]{1,0:T(8,128)(2,1)S(1)}, f32[1,512]{1,0:T(1,128)S(1)}) custom-call(bf16[160,128]{1,0:T(8,128)(2,1)S(1)} %get-tuple-element.25.refs_0_, bf16[1184,128]{1,0:T(8,128)(2,1)S(1)} %collective-permute-done.12.partner.refs_1_, bf16[160,128]{1,0:T(8,128)(2,1)S(1)} %collective-permute-done.13.refs_2_, ...), custom_call_target="tpu_custom_call" | custom-call | flops 67108864 | bytes 524288 | tf_op jit(solution)/shard_map/pallas_call | solution.py:364
  54.2 1.4 %collective-permute-start.21 = (bf16[128,512]{1,0:T(8,128)(2,1)S(1)}, bf16[128,512]{1,0:T(8,128)(2,1)S(1)}, u32[]{:S(2)}, u32[]{:S(2)}) collective-permute-start(bf16[128,512]{1,0:T(8,128)(2,1)S(1)} %get-tuple-element.35.refs_0_), channel_id=1, source_target_pairs={{0,2},{1,3},{2,0},{3,1},{4,6},{5,7},{6,4},{7,5},{8,10},{9,11},{10,... | collective-permute-start | bytes 393224 | tf_op jit(solution)/shard_map/ppermute | solution.py:325
  55.6 2.3 %collective-permute-start.16 = (bf16[128,512]{1,0:T(8,128)(2,1)S(1)}, bf16[128,512]{1,0:T(8,128)(2,1)S(1)}, u32[]{:S(2)}, u32[]{:S(2)}) collective-permute-start(bf16[128,512]{1,0:T(8,128)(2,1)S(1)} %get-tuple-element.35.refs_0_), channel_id=1, source_target_pairs={{0,4},{1,5},{2,6},{3,7},{4,0},{5,1},{6,2},{7,3},{8,12},{9,13},{10,... | collective-permute-start | bytes 393224 | tf_op jit(solution)/shard_map/ppermute | solution.py:325
  57.9 1.5 %collective-permute-start.20 = (bf16[128,512]{1,0:T(8,128)(2,1)S(1)}, bf16[128,512]{1,0:T(8,128)(2,1)S(1)}, u32[]{:S(2)}, u32[]{:S(2)}) collective-permute-start(bf16[128,512]{1,0:T(8,128)(2,1)S(1)} %get-tuple-element.35.refs_0_), channel_id=1, source_target_pairs={{0,1},{1,0},{2,3},{3,2},{4,5},{5,4},{6,7},{7,6},{8,9},{9,8},{10,11... | collective-permute-start | bytes 393224 | tf_op jit(solution)/shard_map/ppermute | solution.py:325
  59.4 3.5 %collective-permute-done.21.refs_2_ = bf16[128,512]{1,0:T(8,128)(2,1)S(1)} collective-permute-done((bf16[128,512]{1,0:T(8,128)(2,1)S(1)}, bf16[128,512]{1,0:T(8,128)(2,1)S(1)}, u32[]{:S(2)}, u32[]{:S(2)}) %collective-permute-start.21) | collective-permute-done | bytes 131104 | tf_op jit(solution)/shard_map/ppermute | solution.py:325
  62.9 1.8 %collective-permute-start.22 = (bf16[128,512]{1,0:T(8,128)(2,1)S(1)}, bf16[128,512]{1,0:T(8,128)(2,1)S(1)}, u32[]{:S(2)}, u32[]{:S(2)}) collective-permute-start(bf16[128,512]{1,0:T(8,128)(2,1)S(1)} %collective-permute-done.21.refs_2_), channel_id=1, source_target_pairs={{0,1},{1,0},{2,3},{3,2},{4,5},{5,4},{6,7},{7,6},{8,9},{9,8},{10,11... | collective-permute-start | bytes 393224 | tf_op jit(solution)/shard_map/ppermute | solution.py:325
  64.7 1.2 %collective-permute-start.19 = (bf16[128,512]{1,0:T(8,128)(2,1)S(1)}, bf16[128,512]{1,0:T(8,128)(2,1)S(1)}, u32[]{:S(2)}, u32[]{:S(2)}) collective-permute-start(bf16[128,512]{1,0:T(8,128)(2,1)S(1)} %get-tuple-element.35.refs_0_), channel_id=1, source_target_pairs={{0,7},{1,6},{2,5},{3,4},{4,3},{5,2},{6,1},{7,0},{8,15},{9,14},{10,... | collective-permute-start | bytes 393224 | tf_op jit(solution)/shard_map/ppermute | solution.py:325
  65.9 1.6 %collective-permute-start.17 = (bf16[128,512]{1,0:T(8,128)(2,1)S(1)}, bf16[128,512]{1,0:T(8,128)(2,1)S(1)}, u32[]{:S(2)}, u32[]{:S(2)}) collective-permute-start(bf16[128,512]{1,0:T(8,128)(2,1)S(1)} %collective-permute-done.16.refs_4_), channel_id=1, source_target_pairs={{0,1},{1,0},{2,3},{3,2},{4,5},{5,4},{6,7},{7,6},{8,9},{9,8},{10,11... | collective-permute-start | bytes 393224 | tf_op jit(solution)/shard_map/ppermute | solution.py:325
  67.5 1.8 %collective-permute-done.22.refs_3_ = bf16[128,512]{1,0:T(8,128)(2,1)S(1)} collective-permute-done((bf16[128,512]{1,0:T(8,128)(2,1)S(1)}, bf16[128,512]{1,0:T(8,128)(2,1)S(1)}, u32[]{:S(2)}, u32[]{:S(2)}) %collective-permute-start.22) | collective-permute-done | bytes 131104 | tf_op jit(solution)/shard_map/ppermute | solution.py:325
  69.3 1.0 %shard_map.176.refs_4_ = f32[128,512]{1,0:T(8,128)S(1)} custom-call(bf16[128,512]{1,0:T(8,128)(2,1)S(1)} %get-tuple-element.35.refs_0_, bf16[128,512]{1,0:T(8,128)(2,1)S(1)} %collective-permute-done.20.refs_1_, bf16[128,512]{1,0:T(8,128)(2,1)S(1)} %collective-permute-done.21.refs_2_, bf16[128,512]{1,0:T(8,128)(2,1)S(1)} %collective-permute-done.22.refs_3_, ...), custom_call_target="tpu_custom_call" | custom-call | flops 335544320 | bytes 2621440 | tf_op jit(solution)/shard_map/pallas_call | solution.py:364
  70.3 3.3 %collective-permute-done.19.refs_2_ = bf16[128,512]{1,0:T(8,128)(2,1)S(1)} collective-permute-done((bf16[128,512]{1,0:T(8,128)(2,1)S(1)}, bf16[128,512]{1,0:T(8,128)(2,1)S(1)}, u32[]{:S(2)}, u32[]{:S(2)}) %collective-permute-start.19) | collective-permute-done | bytes 131104 | tf_op jit(solution)/shard_map/ppermute | solution.py:325
  73.6 0.0 collective-permute-done.17.refs_0_
  73.7 1.3 %shard_map.177 = bf16[128,512]{1,0:T(8,128)(2,1)} custom-call(bf16[128,512]{1,0:T(8,128)(2,1)S(1)} %collective-permute-done.17.refs_0_, bf16[128,512]{1,0:T(8,128)(2,1)S(1)} %collective-permute-done.18.refs_1_, bf16[128,512]{1,0:T(8,128)(2,1)S(1)} %collective-permute-done.19.refs_2_, bf16[512,4096]{1,0:T(8,128)(2,1)S(1)} %copy-done, ...), custom_call_target="tpu_custom_call" | custom-call | flops 201326592 | bytes 1572864 | tf_op jit(solution)/shard_map/pallas_call | solution.py:364
  (27 shorter events, 0.1 us)
Async XLA Ops:
  2.7 9.7 %collective-permute-start.1 = (bf16[144,512]{1,0:T(8,128)(2,1)}, bf16[144,512]{1,0:T(8,128)(2,1)S(1)}, u32[]{:S(2)}, u32[]{:S(2)}) collective-permute-start(bf16[144,512]{1,0:T(8,128)(2,1)} %get-tuple-element.21.refs_0_), channel_id=1, source_target_pairs={{0,2},{1,3},{2,0},{3,1},{4,6},{5,7},{6,4},{7,5},{8,10},{9,11},{10,... | collective-permute-start | bytes 442376 | tf_op jit(solution)/shard_map/ppermute | solution.py:325
  5.9 27.8 %collective-permute-start.3 = (bf16[144,512]{1,0:T(8,128)(2,1)}, bf16[144,512]{1,0:T(8,128)(2,1)S(1)}, u32[]{:S(2)}, u32[]{:S(2)}) collective-permute-start(bf16[144,512]{1,0:T(8,128)(2,1)} %get-tuple-element.21.refs_0_), channel_id=1, source_target_pairs={{0,4},{1,5},{2,6},{3,7},{4,0},{5,1},{6,2},{7,3},{8,12},{9,13},{10,... | collective-permute-start | bytes 442376 | tf_op jit(solution)/shard_map/ppermute | solution.py:325
  8.5 25.9 %collective-permute-start = (bf16[144,512]{1,0:T(8,128)(2,1)}, bf16[144,512]{1,0:T(8,128)(2,1)S(1)}, u32[]{:S(2)}, u32[]{:S(2)}) collective-permute-start(bf16[144,512]{1,0:T(8,128)(2,1)} %get-tuple-element.21.refs_0_), channel_id=1, source_target_pairs={{0,1},{1,0},{2,3},{3,2},{4,5},{5,4},{6,7},{7,6},{8,9},{9,8},{10,11... | collective-permute-start | bytes 442376 | tf_op jit(solution)/shard_map/ppermute | solution.py:325
  12.5 23.7 %collective-permute-start.2 = (bf16[144,512]{1,0:T(8,128)(2,1)S(1)}, bf16[144,512]{1,0:T(8,128)(2,1)S(1)}, u32[]{:S(2)}, u32[]{:S(2)}) collective-permute-start(bf16[144,512]{1,0:T(8,128)(2,1)S(1)} %collective-permute-done.1.refs_1_.refs_2_), channel_id=1, source_target_pairs={{0,1},{1,0},{2,3},{3,2},{4,5},{5,4},{6,7},{7,6},{8,9},{9,8},{10,11... | collective-permute-start | bytes 442376 | tf_op jit(solution)/shard_map/ppermute | solution.py:325
  14.3 1.4 %collective-permute-start.7 = (f32[8,512]{1,0:T(8,128)}, f32[8,512]{1,0:T(8,128)S(1)}, u32[]{:S(2)}, u32[]{:S(2)}) collective-permute-start(f32[8,512]{1,0:T(8,128)} %get-tuple-element.22.mine), channel_id=1, source_target_pairs={{0,8},{8,0},{16,24},{24,16},{1,9},{9,1},{17,25},{25,17},{2,10},{10... | collective-permute-start | bytes 49160 | tf_op jit(solution)/shard_map/ppermute | solution.py:325
  15.7 0.7 copy-start.12
  16.4 3.7 %collective-permute-start.8 = (f32[8,512]{1,0:T(8,128)S(1)}, f32[8,512]{1,0:T(8,128)S(1)}, u32[]{:S(2)}, u32[]{:S(2)}) collective-permute-start(f32[8,512]{1,0:T(8,128)S(1)} %shard_map.164.mine), channel_id=1, source_target_pairs={{0,16},{8,24},{16,0},{24,8},{1,17},{9,25},{17,1},{25,9},{2,18},{10... | collective-permute-start | bytes 49160 | tf_op jit(solution)/shard_map/ppermute | solution.py:325
  20.2 3.7 %collective-permute-start.9 = (f32[4,512]{1,0:T(4,128)S(1)}, f32[4,512]{1,0:T(4,128)S(1)}, u32[]{:S(2)}, u32[]{:S(2)}) collective-permute-start(f32[4,512]{1,0:T(4,128)S(1)} %shard_map.165.refs_0_.refs_8_), channel_id=1, source_target_pairs={{0,1},{1,0},{2,3},{3,2},{4,5},{5,4},{6,7},{7,6},{8,9},{9,8},{10,11... | collective-permute-start | bytes 24584 | tf_op jit(solution)/shard_map/ppermute | solution.py:325
  23.8 9.1 %collective-permute-start.10 = (f32[8,512]{1,0:T(8,128)S(1)}, f32[8,512]{1,0:T(8,128)S(1)}, u32[]{:S(2)}, u32[]{:S(2)}) collective-permute-start(f32[8,512]{1,0:T(8,128)S(1)} %shard_map.166), channel_id=1, source_target_pairs={{0,2},{1,3},{2,0},{3,1},{4,6},{5,7},{6,4},{7,5},{8,10},{9,11},{10,... | collective-permute-start | bytes 49160 | tf_op jit(solution)/shard_map/ppermute | solution.py:325
  23.8 14.2 %collective-permute-start.6 = (bf16[144,512]{1,0:T(8,128)(2,1)}, bf16[144,512]{1,0:T(8,128)(2,1)S(1)}, u32[]{:S(2)}, u32[]{:S(2)}) collective-permute-start(bf16[144,512]{1,0:T(8,128)(2,1)} %get-tuple-element.21.refs_0_), channel_id=1, source_target_pairs={{0,7},{1,6},{2,5},{3,4},{4,3},{5,2},{6,1},{7,0},{8,15},{9,14},{10,... | collective-permute-start | bytes 442376 | tf_op jit(solution)/shard_map/ppermute | solution.py:325
  26.6 2.2 %copy-start.1 = (bf16[512,4096]{1,0:T(8,128)(2,1)S(1)}, bf16[512,4096]{1,0:T(8,128)(2,1)}, u32[]{:S(2)}) copy-start(bf16[512,4096]{1,0:T(8,128)(2,1)} %refs_1_.1) | copy-start | bytes 12582916
  28.8 1.6 %copy-start.3 = (bf16[256,4096]{1,0:T(8,128)(2,1)S(1)}, bf16[256,4096]{1,0:T(8,128)(2,1)}, u32[]{:S(2)}) copy-start(bf16[256,4096]{1,0:T(8,128)(2,1)} %refs_0_.1) | copy-start | bytes 6291460
  30.4 0.9 %copy-start.7 = (bf16[2,4096,16]{1,2,0:T(8,128)(2,1)S(1)}, bf16[2,4096,16]{1,2,0:T(8,128)(2,1)}, u32[]{:S(2)}) copy-start(bf16[2,4096,16]{1,2,0:T(8,128)(2,1)} %param.28) | copy-start | bytes 786436
  31.3 1.2 %copy-start.5 = (bf16[512,1024]{1,0:T(8,128)(2,1)S(1)}, bf16[512,1024]{1,0:T(8,128)(2,1)}, u32[]{:S(2)}) copy-start(bf16[512,1024]{1,0:T(8,128)(2,1)} %weight.1) | copy-start | bytes 3145732
  31.3 1.2 %copy-start.13 = (bf16[1024]{0:T(1024)(128)(2,1)S(1)}, bf16[1024]{0:T(1024)(128)(2,1)}, u32[]{:S(2)}) copy-start(bf16[1024]{0:T(1024)(128)(2,1)} %param.19) | copy-start | bytes 6148
  33.0 6.6 %copy-start.8 = (bf16[144,512]{1,0:T(8,128)(2,1)S(1)}, bf16[144,512]{1,0:T(8,128)(2,1)}, u32[]{:S(2)}) copy-start(bf16[144,512]{1,0:T(8,128)(2,1)} %get-tuple-element.21.refs_0_) | copy-start | bytes 442372
  33.0 6.5 %copy-start.9 = (bf16[2,16,2048]{2,1,0:T(8,128)(2,1)S(1)}, bf16[2,16,2048]{2,1,0:T(8,128)(2,1)}, u32[]{:S(2)}) copy-start(bf16[2,16,2048]{2,1,0:T(8,128)(2,1)} %refs_17_.1) | copy-start | bytes 393220
  33.0 6.5 %copy-start.10 = (f32[2,128,16]{1,2,0:T(8,128)S(1)}, f32[2,128,16]{1,2,0:T(8,128)}, u32[]{:S(2)}) copy-start(f32[2,128,16]{1,2,0:T(8,128)} %param.31) | copy-start | bytes 49156
  33.0 6.5 %copy-start.11 = (f32[2,2048]{1,0:T(2,128)S(1)}, f32[2,2048]{1,0:T(2,128)}, u32[]{:S(2)}) copy-start(f32[2,2048]{1,0:T(2,128)} %refs_18_.1) | copy-start | bytes 49156
  33.0 5.0 %collective-permute-start.11 = (f32[16,512]{1,0:T(8,128)S(1)}, f32[16,512]{1,0:T(8,128)S(1)}, u32[]{:S(2)}, u32[]{:S(2)}) collective-permute-start(f32[16,512]{1,0:T(8,128)S(1)} %shard_map.167), channel_id=1, source_target_pairs={{0,4},{1,5},{2,6},{3,7},{4,0},{5,1},{6,2},{7,3},{8,12},{9,13},{10,... | collective-permute-start | bytes 98312 | tf_op jit(solution)/shard_map/ppermute | solution.py:325
  33.7 5.5 %collective-permute-start.5 = (bf16[144,512]{1,0:T(8,128)(2,1)S(1)}, bf16[144,512]{1,0:T(8,128)(2,1)S(1)}, u32[]{:S(2)}, u32[]{:S(2)}) collective-permute-start(bf16[144,512]{1,0:T(8,128)(2,1)S(1)} %collective-permute-done.3.refs_4_), channel_id=1, source_target_pairs={{0,2},{1,3},{2,0},{3,1},{4,6},{5,7},{6,4},{7,5},{8,10},{9,11},{10,... | collective-permute-start | bytes 442376 | tf_op jit(solution)/shard_map/ppermute | solution.py:325
  34.4 5.1 %collective-permute-start.4 = (bf16[144,512]{1,0:T(8,128)(2,1)S(1)}, bf16[144,512]{1,0:T(8,128)(2,1)S(1)}, u32[]{:S(2)}, u32[]{:S(2)}) collective-permute-start(bf16[144,512]{1,0:T(8,128)(2,1)S(1)} %collective-permute-done.3.refs_4_), channel_id=1, source_target_pairs={{0,1},{1,0},{2,3},{3,2},{4,5},{5,4},{6,7},{7,6},{8,9},{9,8},{10,11... | collective-permute-start | bytes 442376 | tf_op jit(solution)/shard_map/ppermute | solution.py:325
  39.6 7.9 %copy-start.4 = (bf16[256,4096]{1,0:T(8,128)(2,1)S(1)}, bf16[256,4096]{1,0:T(8,128)(2,1)}, u32[]{:S(2)}) copy-start(bf16[256,4096]{1,0:T(8,128)(2,1)} %query_w.1) | copy-start | bytes 6291460
  43.7 8.3 %copy-start.2 = (bf16[512,4096]{1,0:T(8,128)(2,1)S(1)}, bf16[512,4096]{1,0:T(8,128)(2,1)}, u32[]{:S(2)}) copy-start(bf16[512,4096]{1,0:T(8,128)(2,1)} %gate_w.1) | copy-start | bytes 12582916
  43.7 8.3 %copy-start.14 = (f32[512]{0:T(512)S(1)}, f32[512]{0:T(512)}, u32[]{:S(2)}) copy-start(f32[512]{0:T(512)} %param.32) | copy-start | bytes 6148
  43.7 1.7 %collective-permute-start.12 = (bf16[1184,128]{1,0:T(8,128)(2,1)S(1)}, bf16[1184,128]{1,0:T(8,128)(2,1)S(1)}, u32[]{:S(2)}, u32[]{:S(2)}) collective-permute-start(bf16[1184,128]{1,0:T(8,128)(2,1)S(1)} %get-tuple-element.26.own), channel_id=1, source_target_pairs={{0,8},{8,0},{16,24},{24,16},{1,9},{9,1},{17,25},{25,17},{2,10},{10... | collective-permute-start | bytes 909320 | tf_op jit(solution)/shard_map/ppermute | solution.py:325
  45.4 8.0 %collective-permute-start.15 = (bf16[528,128]{1,0:T(8,128)(2,1)S(1)}, bf16[528,128]{1,0:T(8,128)(2,1)S(1)}, u32[]{:S(2)}, u32[]{:S(2)}) collective-permute-start(bf16[528,128]{1,0:T(8,128)(2,1)S(1)} %shard_map.172), channel_id=1, source_target_pairs={{0,16},{8,24},{16,0},{24,8},{1,17},{9,25},{17,1},{25,9},{2,18},{10... | collective-permute-start | bytes 405512 | tf_op jit(solution)/shard_map/ppermute | solution.py:325
  47.2 4.8 %collective-permute-start.13 = (bf16[160,128]{1,0:T(8,128)(2,1)S(1)}, bf16[160,128]{1,0:T(8,128)(2,1)S(1)}, u32[]{:S(2)}, u32[]{:S(2)}) collective-permute-start(bf16[160,128]{1,0:T(8,128)(2,1)S(1)} %get-tuple-element.25.refs_0_), channel_id=1, source_target_pairs={{0,16},{8,24},{16,0},{24,8},{1,17},{9,25},{17,1},{25,9},{2,18},{10... | collective-permute-start | bytes 122888 | tf_op jit(solution)/shard_map/ppermute | solution.py:325
  49.0 20.3 %copy-start = (bf16[512,4096]{1,0:T(8,128)(2,1)S(1)}, bf16[512,4096]{1,0:T(8,128)(2,1)}, u32[]{:S(2)}) copy-start(bf16[512,4096]{1,0:T(8,128)(2,1)} %refs_3_.3) | copy-start | bytes 12582916
  52.0 1.4 %collective-permute-start.14 = (bf16[160,128]{1,0:T(8,128)(2,1)S(1)}, bf16[160,128]{1,0:T(8,128)(2,1)S(1)}, u32[]{:S(2)}, u32[]{:S(2)}) collective-permute-start(bf16[160,128]{1,0:T(8,128)(2,1)S(1)} %collective-permute-done.13.refs_2_), channel_id=1, source_target_pairs={{0,8},{8,0},{16,24},{24,16},{1,9},{9,1},{17,25},{25,17},{2,10},{10... | collective-permute-start | bytes 122888 | tf_op jit(solution)/shard_map/ppermute | solution.py:325
  53.3 20.3 %copy-start.6 = (bf16[128,512]{1,0:T(8,128)(2,1)S(1)}, bf16[128,512]{1,0:T(8,128)(2,1)}, u32[]{:S(2)}) copy-start(bf16[128,512]{1,0:T(8,128)(2,1)} %refs_5_.5) | copy-start | bytes 393220
  54.2 8.8 %collective-permute-start.21 = (bf16[128,512]{1,0:T(8,128)(2,1)S(1)}, bf16[128,512]{1,0:T(8,128)(2,1)S(1)}, u32[]{:S(2)}, u32[]{:S(2)}) collective-permute-start(bf16[128,512]{1,0:T(8,128)(2,1)S(1)} %get-tuple-element.35.refs_0_), channel_id=1, source_target_pairs={{0,2},{1,3},{2,0},{3,1},{4,6},{5,7},{6,4},{7,5},{8,10},{9,11},{10,... | collective-permute-start | bytes 393224 | tf_op jit(solution)/shard_map/ppermute | solution.py:325
  55.6 10.3 %collective-permute-start.16 = (bf16[128,512]{1,0:T(8,128)(2,1)S(1)}, bf16[128,512]{1,0:T(8,128)(2,1)S(1)}, u32[]{:S(2)}, u32[]{:S(2)}) collective-permute-start(bf16[128,512]{1,0:T(8,128)(2,1)S(1)} %get-tuple-element.35.refs_0_), channel_id=1, source_target_pairs={{0,4},{1,5},{2,6},{3,7},{4,0},{5,1},{6,2},{7,3},{8,12},{9,13},{10,... | collective-permute-start | bytes 393224 | tf_op jit(solution)/shard_map/ppermute | solution.py:325
  57.9 9.6 %collective-permute-start.20 = (bf16[128,512]{1,0:T(8,128)(2,1)S(1)}, bf16[128,512]{1,0:T(8,128)(2,1)S(1)}, u32[]{:S(2)}, u32[]{:S(2)}) collective-permute-start(bf16[128,512]{1,0:T(8,128)(2,1)S(1)} %get-tuple-element.35.refs_0_), channel_id=1, source_target_pairs={{0,1},{1,0},{2,3},{3,2},{4,5},{5,4},{6,7},{7,6},{8,9},{9,8},{10,11... | collective-permute-start | bytes 393224 | tf_op jit(solution)/shard_map/ppermute | solution.py:325
  62.9 6.4 %collective-permute-start.22 = (bf16[128,512]{1,0:T(8,128)(2,1)S(1)}, bf16[128,512]{1,0:T(8,128)(2,1)S(1)}, u32[]{:S(2)}, u32[]{:S(2)}) collective-permute-start(bf16[128,512]{1,0:T(8,128)(2,1)S(1)} %collective-permute-done.21.refs_2_), channel_id=1, source_target_pairs={{0,1},{1,0},{2,3},{3,2},{4,5},{5,4},{6,7},{7,6},{8,9},{9,8},{10,11... | collective-permute-start | bytes 393224 | tf_op jit(solution)/shard_map/ppermute | solution.py:325
  64.7 8.9 %collective-permute-start.19 = (bf16[128,512]{1,0:T(8,128)(2,1)S(1)}, bf16[128,512]{1,0:T(8,128)(2,1)S(1)}, u32[]{:S(2)}, u32[]{:S(2)}) collective-permute-start(bf16[128,512]{1,0:T(8,128)(2,1)S(1)} %get-tuple-element.35.refs_0_), channel_id=1, source_target_pairs={{0,7},{1,6},{2,5},{3,4},{4,3},{5,2},{6,1},{7,0},{8,15},{9,14},{10,... | collective-permute-start | bytes 393224 | tf_op jit(solution)/shard_map/ppermute | solution.py:325
  65.9 7.7 %collective-permute-start.18 = (bf16[128,512]{1,0:T(8,128)(2,1)S(1)}, bf16[128,512]{1,0:T(8,128)(2,1)S(1)}, u32[]{:S(2)}, u32[]{:S(2)}) collective-permute-start(bf16[128,512]{1,0:T(8,128)(2,1)S(1)} %collective-permute-done.16.refs_4_), channel_id=1, source_target_pairs={{0,2},{1,3},{2,0},{3,1},{4,6},{5,7},{6,4},{7,5},{8,10},{9,11},{10,... | collective-permute-start | bytes 393224 | tf_op jit(solution)/shard_map/ppermute | solution.py:325
  65.9 7.8 %collective-permute-start.17 = (bf16[128,512]{1,0:T(8,128)(2,1)S(1)}, bf16[128,512]{1,0:T(8,128)(2,1)S(1)}, u32[]{:S(2)}, u32[]{:S(2)}) collective-permute-start(bf16[128,512]{1,0:T(8,128)(2,1)S(1)} %collective-permute-done.16.refs_4_), channel_id=1, source_target_pairs={{0,1},{1,0},{2,3},{3,2},{4,5},{5,4},{6,7},{7,6},{8,9},{9,8},{10,11... | collective-permute-start | bytes 393224 | tf_op jit(solution)/shard_map/ppermute | solution.py:325

commit v3 on v2

--- a/solution.py
+++ b/solution.py
@@ -353,6 +353,8 @@
 SURVEY_FLOPS = 15 * 10**9
 SURVEY_BYTES = 40 * 10**6
 MOD_STEPS = (1, 2, 4)
+LATE = (5, 6)
+MIDDLE = (7,)
 PLANS = {
     "lat": ((4, 0), (2, 0), (1, 0), (7, 0), (3, 2), (5, 4), (6, 4)),
     "out": ((2, 0), (4, 0), (1, 0), (3, 2), (7, 0), (5, 4), (6, 4)),
@@ -791,6 +793,11 @@
     out[...] = branch_of(order, refs[:-2], weight)
 
 
+def middle_kernel(order, *refs):
+    weight, early, out = refs[-3:]
+    out[...] = early[...] + branch_of(order, refs[:-3], weight)
+
+
 def output_kernel(order, *refs):
     weight, early, latent, gates, out = refs[-5:]
     branch = early[...] + branch_of(order, refs[:-5], weight)
@@ -988,8 +995,9 @@
         ],
     )
     branches = gathered_pieces(heads_out, "tp", "out")
-    late = [k for k in range(1, tp_count) if k >= tp_count - 3]
-    soon = [k for k in range(tp_count) if k not in late]
+    late = LATE if tp_count == 8 else list(range(max(1, tp_count - 2), tp_count))
+    middle = MIDDLE if tp_count == 8 else []
+    soon = [k for k in range(tp_count) if k not in late and k not in middle]
     cost = 2 * width * vdim
     early = call(
         functools.partial(early_kernel, soon),
@@ -999,6 +1007,15 @@
         tokens * cost * len(soon),
         cost * len(soon),
     )
+    if middle:
+        early = call(
+            functools.partial(middle_kernel, middle),
+            shape((tokens, width), f32),
+            [VMEM_SPEC] * (len(middle) + 2),
+            (*(branches[k] for k in middle), output_matrix, early),
+            tokens * cost * len(middle),
+            cost * len(middle),
+        )
     return call(
         functools.partial(output_kernel, late),
         shape((tokens, width), bf16),

time: 75.3 us -> 75.5 us (level)
    pallas_call x15 -> x16, Pallas kernels: 13.8 us -> 14 us  [call(): pl.pallas_call(kernel, out_shape=out_shapes, in_specs=in_specs, out_specs...]
  transfers between devices with their start and end apart: 23 -> 23, of which waited for: 12 -> 12; matrix products, arithmetic and copies ran while one was open for 0% -> 0% of each run, Pallas kernels for 6% -> 7%
where the time goes in v3:
time: 75.5 us; the launch traced here: 75.2 us
  starting transfers between devices  28.6 us (38%)
  waiting for transfers between devices  26.1 us (35%)
  Pallas kernels  14 us (19%)
  local copies, waits for them, and re-layouts  6.25 us (8%)
    ppermute x23, starting transfers between devices, exchange(): lax.ppermute(value, axis, [(i, i ^ distance) for i in range(lax.axis_size...  28.6 us
    ppermute x23, waiting for transfers between devices, exchange(): lax.ppermute(value, axis, [(i, i ^ distance) for i in range(lax.axis_size...  26.1 us
    pallas_call x16, Pallas kernels, call(): pl.pallas_call(kernel, out_shape=out_shapes, in_specs=in_specs, out_specs...  14 us
    unnamed x30, local copies, waits for them, and re-layouts  6.25 us
  transfers between devices with their start and end apart: 23, of which 12 were waited for; matrix products, arithmetic and copies ran while one was open for 0% of the time, Pallas kernels for 7%

profile of v3, /device:TPU:0, one launch (start us, length us, event | category | flops | bytes accessed | tf_op | source)
XLA Modules:
  0.0 75.2 jit_solution(592635451877173627)
XLA Ops:
  0.0 2.7 %shard_map.163 = (f32[8,512]{1,0:T(8,128)}, bf16[144,512]{1,0:T(8,128)(2,1)}) custom-call(bf16[8,128]{1,0:T(8,128)(2,1)} %bitcast.9, bf16[8,128]{1,0:T(8,128)(2,1)} %bitcast.12, bf16[512,1024]{1,0:T(8,128)(2,1)} %refs_2_.2, bf16[512,1024]{1,0:T(8,128)(2,1)} %refs_3_.1, bf16[128,512]{1,0:T(8,128)(2,1)} %refs_4_.3, bf16[16,512]{1,0:T(8,128)(2,1)} %refs_5_.2), custom_call_target="tpu_custom_call" | custom-call | flops 16777216 | bytes 2097152 | tf_op jit(solution)/shard_map/pallas_call | solution.py:366
  2.7 3.1 %collective-permute-start.1 = (bf16[144,512]{1,0:T(8,128)(2,1)}, bf16[144,512]{1,0:T(8,128)(2,1)S(1)}, u32[]{:S(2)}, u32[]{:S(2)}) collective-permute-start(bf16[144,512]{1,0:T(8,128)(2,1)} %get-tuple-element.21.refs_0_), channel_id=1, source_target_pairs={{0,2},{1,3},{2,0},{3,1},{4,6},{5,7},{6,4},{7,5},{8,10},{9,11},{10,... | collective-permute-start | bytes 442376 | tf_op jit(solution)/shard_map/ppermute | solution.py:325
  5.9 2.6 %collective-permute-start.3 = (bf16[144,512]{1,0:T(8,128)(2,1)}, bf16[144,512]{1,0:T(8,128)(2,1)S(1)}, u32[]{:S(2)}, u32[]{:S(2)}) collective-permute-start(bf16[144,512]{1,0:T(8,128)(2,1)} %get-tuple-element.21.refs_0_), channel_id=1, source_target_pairs={{0,4},{1,5},{2,6},{3,7},{4,0},{5,1},{6,2},{7,3},{8,12},{9,13},{10,... | collective-permute-start | bytes 442376 | tf_op jit(solution)/shard_map/ppermute | solution.py:325
  8.5 1.5 %collective-permute-start = (bf16[144,512]{1,0:T(8,128)(2,1)}, bf16[144,512]{1,0:T(8,128)(2,1)S(1)}, u32[]{:S(2)}, u32[]{:S(2)}) collective-permute-start(bf16[144,512]{1,0:T(8,128)(2,1)} %get-tuple-element.21.refs_0_), channel_id=1, source_target_pairs={{0,1},{1,0},{2,3},{3,2},{4,5},{5,4},{6,7},{7,6},{8,9},{9,8},{10,11... | collective-permute-start | bytes 442376 | tf_op jit(solution)/shard_map/ppermute | solution.py:325
  10.0 2.5 %collective-permute-done.1.refs_1_.refs_2_ = bf16[144,512]{1,0:T(8,128)(2,1)S(1)} collective-permute-done((bf16[144,512]{1,0:T(8,128)(2,1)}, bf16[144,512]{1,0:T(8,128)(2,1)S(1)}, u32[]{:S(2)}, u32[]{:S(2)}) %collective-permute-start.1) | collective-permute-done | bytes 147488 | tf_op jit(solution)/shard_map/ppermute | solution.py:325
  12.5 1.8 %collective-permute-start.2 = (bf16[144,512]{1,0:T(8,128)(2,1)S(1)}, bf16[144,512]{1,0:T(8,128)(2,1)S(1)}, u32[]{:S(2)}, u32[]{:S(2)}) collective-permute-start(bf16[144,512]{1,0:T(8,128)(2,1)S(1)} %collective-permute-done.1.refs_1_.refs_2_), channel_id=1, source_target_pairs={{0,1},{1,0},{2,3},{3,2},{4,5},{5,4},{6,7},{7,6},{8,9},{9,8},{10,11... | collective-permute-start | bytes 442376 | tf_op jit(solution)/shard_map/ppermute | solution.py:325
  14.3 0.0 collective-permute-start.7
  14.3 1.4 %collective-permute-done.7.theirs = f32[8,512]{1,0:T(8,128)S(1)} collective-permute-done((f32[8,512]{1,0:T(8,128)}, f32[8,512]{1,0:T(8,128)S(1)}, u32[]{:S(2)}, u32[]{:S(2)}) %collective-permute-start.7) | collective-permute-done | bytes 16416 | tf_op jit(solution)/shard_map/ppermute | solution.py:325
  15.7 0.7 copy-done.12
  16.4 1.5 %collective-permute-start.8 = (f32[8,512]{1,0:T(8,128)S(1)}, f32[8,512]{1,0:T(8,128)S(1)}, u32[]{:S(2)}, u32[]{:S(2)}) collective-permute-start(f32[8,512]{1,0:T(8,128)S(1)} %shard_map.164.mine), channel_id=1, source_target_pairs={{0,16},{8,24},{16,0},{24,8},{1,17},{9,25},{17,1},{25,9},{2,18},{10... | collective-permute-start | bytes 49160 | tf_op jit(solution)/shard_map/ppermute | solution.py:325
  17.9 2.2 %collective-permute-done.8.theirs = f32[8,512]{1,0:T(8,128)S(1)} collective-permute-done((f32[8,512]{1,0:T(8,128)S(1)}, f32[8,512]{1,0:T(8,128)S(1)}, u32[]{:S(2)}, u32[]{:S(2)}) %collective-permute-start.8) | collective-permute-done | bytes 16416 | tf_op jit(solution)/shard_map/ppermute | solution.py:325
  20.2 0.2 collective-permute-start.9
  20.3 3.5 %collective-permute-done.9.refs_1_.refs_9_ = f32[4,512]{1,0:T(4,128)S(1)} collective-permute-done((f32[4,512]{1,0:T(4,128)S(1)}, f32[4,512]{1,0:T(4,128)S(1)}, u32[]{:S(2)}, u32[]{:S(2)}) %collective-permute-start.9) | collective-permute-done | bytes 8224 | tf_op jit(solution)/shard_map/ppermute | solution.py:325
  23.8 0.0 collective-permute-start.10
  23.8 2.8 %collective-permute-start.6 = (bf16[144,512]{1,0:T(8,128)(2,1)}, bf16[144,512]{1,0:T(8,128)(2,1)S(1)}, u32[]{:S(2)}, u32[]{:S(2)}) collective-permute-start(bf16[144,512]{1,0:T(8,128)(2,1)} %get-tuple-element.21.refs_0_), channel_id=1, source_target_pairs={{0,7},{1,6},{2,5},{3,4},{4,3},{5,2},{6,1},{7,0},{8,15},{9,14},{10,... | collective-permute-start | bytes 442376 | tf_op jit(solution)/shard_map/ppermute | solution.py:325
  26.6 2.2 %copy-done.1 = bf16[512,4096]{1,0:T(8,128)(2,1)S(1)} copy-done((bf16[512,4096]{1,0:T(8,128)(2,1)S(1)}, bf16[512,4096]{1,0:T(8,128)(2,1)}, u32[]{:S(2)}) %copy-start.1) | copy-done | bytes 4194328
  28.8 1.6 %copy-done.3 = bf16[256,4096]{1,0:T(8,128)(2,1)S(1)} copy-done((bf16[256,4096]{1,0:T(8,128)(2,1)S(1)}, bf16[256,4096]{1,0:T(8,128)(2,1)}, u32[]{:S(2)}) %copy-start.3) | copy-done | bytes 2097176
  30.4 0.9 %copy-done.7 = bf16[2,4096,16]{1,2,0:T(8,128)(2,1)S(1)} copy-done((bf16[2,4096,16]{1,2,0:T(8,128)(2,1)S(1)}, bf16[2,4096,16]{1,2,0:T(8,128)(2,1)}, u32[]{:S(2)}) %copy-start.7) | copy-done | bytes 262168
  31.3 0.5 shard_map.168.refs_12_
  31.8 0.7 copy-done.5
  32.6 0.4 shard_map.170.refs_16_
  33.0 0.0 collective-permute-done.10.refs_2_.refs_10_
  33.0 0.0 copy-start.9
  33.0 0.0 copy-start.10
  33.0 0.0 copy-start.11
  33.0 0.7 collective-permute-start.11
  33.7 0.0 collective-permute-done.3.refs_4_
  33.7 0.7 collective-permute-start.5
  34.4 1.8 %collective-permute-start.4 = (bf16[144,512]{1,0:T(8,128)(2,1)S(1)}, bf16[144,512]{1,0:T(8,128)(2,1)S(1)}, u32[]{:S(2)}, u32[]{:S(2)}) collective-permute-start(bf16[144,512]{1,0:T(8,128)(2,1)S(1)} %collective-permute-done.3.refs_4_), channel_id=1, source_target_pairs={{0,1},{1,0},{2,3},{3,2},{4,5},{5,4},{6,7},{7,6},{8,9},{9,8},{10,11... | collective-permute-start | bytes 442376 | tf_op jit(solution)/shard_map/ppermute | solution.py:325
  36.2 0.0 collective-permute-done.2.refs_2_.refs_3_
  36.2 0.1 shard_map.169
  36.3 1.7 %collective-permute-done.11.refs_11_ = f32[16,512]{1,0:T(8,128)S(1)} collective-permute-done((f32[16,512]{1,0:T(8,128)S(1)}, f32[16,512]{1,0:T(8,128)S(1)}, u32[]{:S(2)}, u32[]{:S(2)}) %collective-permute-start.11) | collective-permute-done | bytes 32800 | tf_op jit(solution)/shard_map/ppermute | solution.py:325
  38.0 0.0 collective-permute-done.6.refs_7_
  38.0 1.2 %collective-permute-done.5.refs_6_ = bf16[144,512]{1,0:T(8,128)(2,1)S(1)} collective-permute-done((bf16[144,512]{1,0:T(8,128)(2,1)S(1)}, bf16[144,512]{1,0:T(8,128)(2,1)S(1)}, u32[]{:S(2)}, u32[]{:S(2)}) %collective-permute-start.5) | collective-permute-done | bytes 147488 | tf_op jit(solution)/shard_map/ppermute | solution.py:325
  39.2 0.3 collective-permute-done.4.refs_5_
  39.6 0.0 copy-start.4
  39.6 4.1 %shard_map.171 = (bf16[144,4096]{1,0:T(8,128)(2,1)S(1)}, bf16[128,256]{1,0:T(8,128)(2,1)S(1)}, bf16[128,512]{1,0:T(8,128)(2,1)S(1)}, f32[128,256]{1,0:T(8,128)S(...) custom-call(bf16[144,512]{1,0:T(8,128)(2,1)S(1)} %copy-done.8, ...), custom_call_target="tpu_custom_call" | custom-call | flops 905969664 | bytes 6291456 | tf_op jit(solution)/shard_map/pallas_call | solution.py:366
  43.7 0.0 copy-start.2
  43.7 0.0 copy-start.14
  43.7 0.1 collective-permute-start.12
  43.8 1.6 %collective-permute-done.12.partner.refs_1_ = bf16[1184,128]{1,0:T(8,128)(2,1)S(1)} collective-permute-done((bf16[1184,128]{1,0:T(8,128)(2,1)S(1)}, bf16[1184,128]{1,0:T(8,128)(2,1)S(1)}, u32[]{:S(2)}, u32[]{:S(2)}) %collective-permute-start.12) | collective-permute-done | bytes 303136 | tf_op jit(solution)/shard_map/ppermute | solution.py:325
  45.3 0.1 shard_map.172
  45.4 1.8 %collective-permute-start.15 = (bf16[528,128]{1,0:T(8,128)(2,1)S(1)}, bf16[528,128]{1,0:T(8,128)(2,1)S(1)}, u32[]{:S(2)}, u32[]{:S(2)}) collective-permute-start(bf16[528,128]{1,0:T(8,128)(2,1)S(1)} %shard_map.172), channel_id=1, source_target_pairs={{0,16},{8,24},{16,0},{24,8},{1,17},{9,25},{17,1},{25,9},{2,18},{10... | collective-permute-start | bytes 405512 | tf_op jit(solution)/shard_map/ppermute | solution.py:325
  47.2 0.3 collective-permute-start.13
  47.5 1.5 %shard_map.173 = (f32[128,512]{1,0:T(8,128)S(1)}, bf16[128,256]{1,0:T(8,128)(2,1)S(1)}, bf16[128,256]{1,0:T(8,128)(2,1)S(1)}) custom-call(bf16[144,4096]{1,0:T(8,128)(2,1)S(1)} %get-tuple-element.27.normed, bf16[256,4096]{1,0:T(8,128)(2,1)S(1)} %copy-done.4, bf16[128,256]{1,0:T(8,128)(2,1)S(1)} %get-tuple-element.28.keys, ...), custom_call_target="tpu_custom_call" | custom-call | flops 268435456 | bytes 2097152 | tf_op jit(solution)/shard_map/pallas_call | solution.py:366
  49.0 0.0 copy-start
  49.0 3.0 %collective-permute-done.13.refs_2_ = bf16[160,128]{1,0:T(8,128)(2,1)S(1)} collective-permute-done((bf16[160,128]{1,0:T(8,128)(2,1)S(1)}, bf16[160,128]{1,0:T(8,128)(2,1)S(1)}, u32[]{:S(2)}, u32[]{:S(2)}) %collective-permute-start.13) | collective-permute-done | bytes 40992 | tf_op jit(solution)/shard_map/ppermute | solution.py:325
  52.0 0.0 collective-permute-start.14
  52.0 1.3 %shard_map.174.refs_8_ = f32[128,512]{1,0:T(8,128)S(1)} custom-call(bf16[144,4096]{1,0:T(8,128)(2,1)S(1)} %get-tuple-element.27.normed, bf16[512,4096]{1,0:T(8,128)(2,1)S(1)} %copy-done.2, f32[1,512]{1,0:T(1,128)S(1)} %bitcast.11), custom_call_target="tpu_custom_call" | custom-call | flops 536870912 | bytes 4194304 | tf_op jit(solution)/shard_map/pallas_call | solution.py:366
  53.3 0.0 collective-permute-done.14.refs_3_
  53.4 0.8 %shard_map.175 = (bf16[128,512]{1,0:T(8,128)(2,1)S(1)}, f32[1,512]{1,0:T(1,128)S(1)}) custom-call(bf16[160,128]{1,0:T(8,128)(2,1)S(1)} %get-tuple-element.25.refs_0_, bf16[1184,128]{1,0:T(8,128)(2,1)S(1)} %collective-permute-done.12.partner.refs_1_, bf16[160,128]{1,0:T(8,128)(2,1)S(1)} %collective-permute-done.13.refs_2_, ...), custom_call_target="tpu_custom_call" | custom-call | flops 67108864 | bytes 524288 | tf_op jit(solution)/shard_map/pallas_call | solution.py:366
  54.2 0.0 copy-start.6
  54.2 1.4 %collective-permute-start.21 = (bf16[128,512]{1,0:T(8,128)(2,1)S(1)}, bf16[128,512]{1,0:T(8,128)(2,1)S(1)}, u32[]{:S(2)}, u32[]{:S(2)}) collective-permute-start(bf16[128,512]{1,0:T(8,128)(2,1)S(1)} %get-tuple-element.35.refs_0_), channel_id=1, source_target_pairs={{0,2},{1,3},{2,0},{3,1},{4,6},{5,7},{6,4},{7,5},{8,10},{9,11},{10,... | collective-permute-start | bytes 393224 | tf_op jit(solution)/shard_map/ppermute | solution.py:325
  55.6 2.3 %collective-permute-start.16 = (bf16[128,512]{1,0:T(8,128)(2,1)S(1)}, bf16[128,512]{1,0:T(8,128)(2,1)S(1)}, u32[]{:S(2)}, u32[]{:S(2)}) collective-permute-start(bf16[128,512]{1,0:T(8,128)(2,1)S(1)} %get-tuple-element.35.refs_0_), channel_id=1, source_target_pairs={{0,4},{1,5},{2,6},{3,7},{4,0},{5,1},{6,2},{7,3},{8,12},{9,13},{10,... | collective-permute-start | bytes 393224 | tf_op jit(solution)/shard_map/ppermute | solution.py:325
  57.9 1.5 %collective-permute-start.20 = (bf16[128,512]{1,0:T(8,128)(2,1)S(1)}, bf16[128,512]{1,0:T(8,128)(2,1)S(1)}, u32[]{:S(2)}, u32[]{:S(2)}) collective-permute-start(bf16[128,512]{1,0:T(8,128)(2,1)S(1)} %get-tuple-element.35.refs_0_), channel_id=1, source_target_pairs={{0,1},{1,0},{2,3},{3,2},{4,5},{5,4},{6,7},{7,6},{8,9},{9,8},{10,11... | collective-permute-start | bytes 393224 | tf_op jit(solution)/shard_map/ppermute | solution.py:325
  59.4 3.5 %collective-permute-done.21.refs_2_ = bf16[128,512]{1,0:T(8,128)(2,1)S(1)} collective-permute-done((bf16[128,512]{1,0:T(8,128)(2,1)S(1)}, bf16[128,512]{1,0:T(8,128)(2,1)S(1)}, u32[]{:S(2)}, u32[]{:S(2)}) %collective-permute-start.21) | collective-permute-done | bytes 131104 | tf_op jit(solution)/shard_map/ppermute | solution.py:325
  62.9 1.8 %collective-permute-start.22 = (bf16[128,512]{1,0:T(8,128)(2,1)S(1)}, bf16[128,512]{1,0:T(8,128)(2,1)S(1)}, u32[]{:S(2)}, u32[]{:S(2)}) collective-permute-start(bf16[128,512]{1,0:T(8,128)(2,1)S(1)} %collective-permute-done.21.refs_2_), channel_id=1, source_target_pairs={{0,1},{1,0},{2,3},{3,2},{4,5},{5,4},{6,7},{7,6},{8,9},{9,8},{10,11... | collective-permute-start | bytes 393224 | tf_op jit(solution)/shard_map/ppermute | solution.py:325
  64.7 1.2 %collective-permute-start.19 = (bf16[128,512]{1,0:T(8,128)(2,1)S(1)}, bf16[128,512]{1,0:T(8,128)(2,1)S(1)}, u32[]{:S(2)}, u32[]{:S(2)}) collective-permute-start(bf16[128,512]{1,0:T(8,128)(2,1)S(1)} %get-tuple-element.35.refs_0_), channel_id=1, source_target_pairs={{0,7},{1,6},{2,5},{3,4},{4,3},{5,2},{6,1},{7,0},{8,15},{9,14},{10,... | collective-permute-start | bytes 393224 | tf_op jit(solution)/shard_map/ppermute | solution.py:325
  65.9 1.6 %collective-permute-start.17 = (bf16[128,512]{1,0:T(8,128)(2,1)S(1)}, bf16[128,512]{1,0:T(8,128)(2,1)S(1)}, u32[]{:S(2)}, u32[]{:S(2)}) collective-permute-start(bf16[128,512]{1,0:T(8,128)(2,1)S(1)} %collective-permute-done.16.refs_4_), channel_id=1, source_target_pairs={{0,1},{1,0},{2,3},{3,2},{4,5},{5,4},{6,7},{7,6},{8,9},{9,8},{10,11... | collective-permute-start | bytes 393224 | tf_op jit(solution)/shard_map/ppermute | solution.py:325
  67.5 1.9 %collective-permute-done.22.refs_3_ = bf16[128,512]{1,0:T(8,128)(2,1)S(1)} collective-permute-done((bf16[128,512]{1,0:T(8,128)(2,1)S(1)}, bf16[128,512]{1,0:T(8,128)(2,1)S(1)}, u32[]{:S(2)}, u32[]{:S(2)}) %collective-permute-start.22) | collective-permute-done | bytes 131104 | tf_op jit(solution)/shard_map/ppermute | solution.py:325
  69.3 1.0 %shard_map.176.refs_2_ = f32[128,512]{1,0:T(8,128)S(1)} custom-call(bf16[128,512]{1,0:T(8,128)(2,1)S(1)} %get-tuple-element.35.refs_0_, bf16[128,512]{1,0:T(8,128)(2,1)S(1)} %collective-permute-done.20.refs_1_, bf16[128,512]{1,0:T(8,128)(2,1)S(1)} %collective-permute-done.21.refs_2_, bf16[128,512]{1,0:T(8,128)(2,1)S(1)} %collective-permute-done.22.refs_3_, ...), custom_call_target="tpu_custom_call" | custom-call | flops 335544320 | bytes 2621440 | tf_op jit(solution)/shard_map/pallas_call | solution.py:366
  70.3 3.3 %collective-permute-done.19.refs_0_ = bf16[128,512]{1,0:T(8,128)(2,1)S(1)} collective-permute-done((bf16[128,512]{1,0:T(8,128)(2,1)S(1)}, bf16[128,512]{1,0:T(8,128)(2,1)S(1)}, u32[]{:S(2)}, u32[]{:S(2)}) %collective-permute-start.19) | collective-permute-done | bytes 131104 | tf_op jit(solution)/shard_map/ppermute | solution.py:325
  73.6 0.3 shard_map.177.refs_3_
  74.0 1.2 %shard_map.178 = bf16[128,512]{1,0:T(8,128)(2,1)} custom-call(bf16[128,512]{1,0:T(8,128)(2,1)S(1)} %collective-permute-done.17.refs_0_, bf16[128,512]{1,0:T(8,128)(2,1)S(1)} %collective-permute-done.18.refs_1_, bf16[512,4096]{1,0:T(8,128)(2,1)S(1)} %copy-done, f32[128,512]{1,0:T(8,128)S(1)} %shard_map.177.refs_3_, bf16[128,512]{1,0:T(8,128)(2,1)S(1)} %copy-done.6, ...), custom_call_target="tpu_custom_call" | custom-call | flops 134217728 | bytes 1048576 | tf_op jit(solution)/shard_map/pallas_call | solution.py:366
  (28 shorter events, 0.1 us)
Async XLA Ops:
  2.7 9.7 %collective-permute-start.1 = (bf16[144,512]{1,0:T(8,128)(2,1)}, bf16[144,512]{1,0:T(8,128)(2,1)S(1)}, u32[]{:S(2)}, u32[]{:S(2)}) collective-permute-start(bf16[144,512]{1,0:T(8,128)(2,1)} %get-tuple-element.21.refs_0_), channel_id=1, source_target_pairs={{0,2},{1,3},{2,0},{3,1},{4,6},{5,7},{6,4},{7,5},{8,10},{9,11},{10,... | collective-permute-start | bytes 442376 | tf_op jit(solution)/shard_map/ppermute | solution.py:325
  5.9 27.8 %collective-permute-start.3 = (bf16[144,512]{1,0:T(8,128)(2,1)}, bf16[144,512]{1,0:T(8,128)(2,1)S(1)}, u32[]{:S(2)}, u32[]{:S(2)}) collective-permute-start(bf16[144,512]{1,0:T(8,128)(2,1)} %get-tuple-element.21.refs_0_), channel_id=1, source_target_pairs={{0,4},{1,5},{2,6},{3,7},{4,0},{5,1},{6,2},{7,3},{8,12},{9,13},{10,... | collective-permute-start | bytes 442376 | tf_op jit(solution)/shard_map/ppermute | solution.py:325
  8.5 25.9 %collective-permute-start = (bf16[144,512]{1,0:T(8,128)(2,1)}, bf16[144,512]{1,0:T(8,128)(2,1)S(1)}, u32[]{:S(2)}, u32[]{:S(2)}) collective-permute-start(bf16[144,512]{1,0:T(8,128)(2,1)} %get-tuple-element.21.refs_0_), channel_id=1, source_target_pairs={{0,1},{1,0},{2,3},{3,2},{4,5},{5,4},{6,7},{7,6},{8,9},{9,8},{10,11... | collective-permute-start | bytes 442376 | tf_op jit(solution)/shard_map/ppermute | solution.py:325
  12.5 23.7 %collective-permute-start.2 = (bf16[144,512]{1,0:T(8,128)(2,1)S(1)}, bf16[144,512]{1,0:T(8,128)(2,1)S(1)}, u32[]{:S(2)}, u32[]{:S(2)}) collective-permute-start(bf16[144,512]{1,0:T(8,128)(2,1)S(1)} %collective-permute-done.1.refs_1_.refs_2_), channel_id=1, source_target_pairs={{0,1},{1,0},{2,3},{3,2},{4,5},{5,4},{6,7},{7,6},{8,9},{9,8},{10,11... | collective-permute-start | bytes 442376 | tf_op jit(solution)/shard_map/ppermute | solution.py:325
  14.3 1.4 %collective-permute-start.7 = (f32[8,512]{1,0:T(8,128)}, f32[8,512]{1,0:T(8,128)S(1)}, u32[]{:S(2)}, u32[]{:S(2)}) collective-permute-start(f32[8,512]{1,0:T(8,128)} %get-tuple-element.22.mine), channel_id=1, source_target_pairs={{0,8},{8,0},{16,24},{24,16},{1,9},{9,1},{17,25},{25,17},{2,10},{10... | collective-permute-start | bytes 49160 | tf_op jit(solution)/shard_map/ppermute | solution.py:325
  15.7 0.7 copy-start.12
  16.4 3.7 %collective-permute-start.8 = (f32[8,512]{1,0:T(8,128)S(1)}, f32[8,512]{1,0:T(8,128)S(1)}, u32[]{:S(2)}, u32[]{:S(2)}) collective-permute-start(f32[8,512]{1,0:T(8,128)S(1)} %shard_map.164.mine), channel_id=1, source_target_pairs={{0,16},{8,24},{16,0},{24,8},{1,17},{9,25},{17,1},{25,9},{2,18},{10... | collective-permute-start | bytes 49160 | tf_op jit(solution)/shard_map/ppermute | solution.py:325
  20.2 3.7 %collective-permute-start.9 = (f32[4,512]{1,0:T(4,128)S(1)}, f32[4,512]{1,0:T(4,128)S(1)}, u32[]{:S(2)}, u32[]{:S(2)}) collective-permute-start(f32[4,512]{1,0:T(4,128)S(1)} %shard_map.165.refs_0_.refs_8_), channel_id=1, source_target_pairs={{0,1},{1,0},{2,3},{3,2},{4,5},{5,4},{6,7},{7,6},{8,9},{9,8},{10,11... | collective-permute-start | bytes 24584 | tf_op jit(solution)/shard_map/ppermute | solution.py:325
  23.8 9.1 %collective-permute-start.10 = (f32[8,512]{1,0:T(8,128)S(1)}, f32[8,512]{1,0:T(8,128)S(1)}, u32[]{:S(2)}, u32[]{:S(2)}) collective-permute-start(f32[8,512]{1,0:T(8,128)S(1)} %shard_map.166), channel_id=1, source_target_pairs={{0,2},{1,3},{2,0},{3,1},{4,6},{5,7},{6,4},{7,5},{8,10},{9,11},{10,... | collective-permute-start | bytes 49160 | tf_op jit(solution)/shard_map/ppermute | solution.py:325
  23.8 14.2 %collective-permute-start.6 = (bf16[144,512]{1,0:T(8,128)(2,1)}, bf16[144,512]{1,0:T(8,128)(2,1)S(1)}, u32[]{:S(2)}, u32[]{:S(2)}) collective-permute-start(bf16[144,512]{1,0:T(8,128)(2,1)} %get-tuple-element.21.refs_0_), channel_id=1, source_target_pairs={{0,7},{1,6},{2,5},{3,4},{4,3},{5,2},{6,1},{7,0},{8,15},{9,14},{10,... | collective-permute-start | bytes 442376 | tf_op jit(solution)/shard_map/ppermute | solution.py:325
  26.6 2.2 %copy-start.1 = (bf16[512,4096]{1,0:T(8,128)(2,1)S(1)}, bf16[512,4096]{1,0:T(8,128)(2,1)}, u32[]{:S(2)}) copy-start(bf16[512,4096]{1,0:T(8,128)(2,1)} %refs_1_.2) | copy-start | bytes 12582916
  28.8 1.6 %copy-start.3 = (bf16[256,4096]{1,0:T(8,128)(2,1)S(1)}, bf16[256,4096]{1,0:T(8,128)(2,1)}, u32[]{:S(2)}) copy-start(bf16[256,4096]{1,0:T(8,128)(2,1)} %refs_0_.1) | copy-start | bytes 6291460
  30.4 0.9 %copy-start.7 = (bf16[2,4096,16]{1,2,0:T(8,128)(2,1)S(1)}, bf16[2,4096,16]{1,2,0:T(8,128)(2,1)}, u32[]{:S(2)}) copy-start(bf16[2,4096,16]{1,2,0:T(8,128)(2,1)} %param.28) | copy-start | bytes 786436
  31.3 1.2 %copy-start.5 = (bf16[512,1024]{1,0:T(8,128)(2,1)S(1)}, bf16[512,1024]{1,0:T(8,128)(2,1)}, u32[]{:S(2)}) copy-start(bf16[512,1024]{1,0:T(8,128)(2,1)} %weight.1) | copy-start | bytes 3145732
  31.3 1.2 %copy-start.13 = (bf16[1024]{0:T(1024)(128)(2,1)S(1)}, bf16[1024]{0:T(1024)(128)(2,1)}, u32[]{:S(2)}) copy-start(bf16[1024]{0:T(1024)(128)(2,1)} %param.19) | copy-start | bytes 6148
  33.0 6.6 %copy-start.8 = (bf16[144,512]{1,0:T(8,128)(2,1)S(1)}, bf16[144,512]{1,0:T(8,128)(2,1)}, u32[]{:S(2)}) copy-start(bf16[144,512]{1,0:T(8,128)(2,1)} %get-tuple-element.21.refs_0_) | copy-start | bytes 442372
  33.0 6.5 %copy-start.9 = (bf16[2,16,2048]{2,1,0:T(8,128)(2,1)S(1)}, bf16[2,16,2048]{2,1,0:T(8,128)(2,1)}, u32[]{:S(2)}) copy-start(bf16[2,16,2048]{2,1,0:T(8,128)(2,1)} %refs_17_.1) | copy-start | bytes 393220
  33.0 6.5 %copy-start.10 = (f32[2,128,16]{1,2,0:T(8,128)S(1)}, f32[2,128,16]{1,2,0:T(8,128)}, u32[]{:S(2)}) copy-start(f32[2,128,16]{1,2,0:T(8,128)} %param.31) | copy-start | bytes 49156
  33.0 6.5 %copy-start.11 = (f32[2,2048]{1,0:T(2,128)S(1)}, f32[2,2048]{1,0:T(2,128)}, u32[]{:S(2)}) copy-start(f32[2,2048]{1,0:T(2,128)} %refs_18_.1) | copy-start | bytes 49156
  33.0 5.0 %collective-permute-start.11 = (f32[16,512]{1,0:T(8,128)S(1)}, f32[16,512]{1,0:T(8,128)S(1)}, u32[]{:S(2)}, u32[]{:S(2)}) collective-permute-start(f32[16,512]{1,0:T(8,128)S(1)} %shard_map.167), channel_id=1, source_target_pairs={{0,4},{1,5},{2,6},{3,7},{4,0},{5,1},{6,2},{7,3},{8,12},{9,13},{10,... | collective-permute-start | bytes 98312 | tf_op jit(solution)/shard_map/ppermute | solution.py:325
  33.7 5.5 %collective-permute-start.5 = (bf16[144,512]{1,0:T(8,128)(2,1)S(1)}, bf16[144,512]{1,0:T(8,128)(2,1)S(1)}, u32[]{:S(2)}, u32[]{:S(2)}) collective-permute-start(bf16[144,512]{1,0:T(8,128)(2,1)S(1)} %collective-permute-done.3.refs_4_), channel_id=1, source_target_pairs={{0,2},{1,3},{2,0},{3,1},{4,6},{5,7},{6,4},{7,5},{8,10},{9,11},{10,... | collective-permute-start | bytes 442376 | tf_op jit(solution)/shard_map/ppermute | solution.py:325
  34.4 5.1 %collective-permute-start.4 = (bf16[144,512]{1,0:T(8,128)(2,1)S(1)}, bf16[144,512]{1,0:T(8,128)(2,1)S(1)}, u32[]{:S(2)}, u32[]{:S(2)}) collective-permute-start(bf16[144,512]{1,0:T(8,128)(2,1)S(1)} %collective-permute-done.3.refs_4_), channel_id=1, source_target_pairs={{0,1},{1,0},{2,3},{3,2},{4,5},{5,4},{6,7},{7,6},{8,9},{9,8},{10,11... | collective-permute-start | bytes 442376 | tf_op jit(solution)/shard_map/ppermute | solution.py:325
  39.6 7.9 %copy-start.4 = (bf16[256,4096]{1,0:T(8,128)(2,1)S(1)}, bf16[256,4096]{1,0:T(8,128)(2,1)}, u32[]{:S(2)}) copy-start(bf16[256,4096]{1,0:T(8,128)(2,1)} %query_w.1) | copy-start | bytes 6291460
  43.7 8.3 %copy-start.2 = (bf16[512,4096]{1,0:T(8,128)(2,1)S(1)}, bf16[512,4096]{1,0:T(8,128)(2,1)}, u32[]{:S(2)}) copy-start(bf16[512,4096]{1,0:T(8,128)(2,1)} %gate_w.1) | copy-start | bytes 12582916
  43.7 8.3 %copy-start.14 = (f32[512]{0:T(512)S(1)}, f32[512]{0:T(512)}, u32[]{:S(2)}) copy-start(f32[512]{0:T(512)} %param.32) | copy-start | bytes 6148
  43.7 1.7 %collective-permute-start.12 = (bf16[1184,128]{1,0:T(8,128)(2,1)S(1)}, bf16[1184,128]{1,0:T(8,128)(2,1)S(1)}, u32[]{:S(2)}, u32[]{:S(2)}) collective-permute-start(bf16[1184,128]{1,0:T(8,128)(2,1)S(1)} %get-tuple-element.26.own), channel_id=1, source_target_pairs={{0,8},{8,0},{16,24},{24,16},{1,9},{9,1},{17,25},{25,17},{2,10},{10... | collective-permute-start | bytes 909320 | tf_op jit(solution)/shard_map/ppermute | solution.py:325
  45.4 7.9 %collective-permute-start.15 = (bf16[528,128]{1,0:T(8,128)(2,1)S(1)}, bf16[528,128]{1,0:T(8,128)(2,1)S(1)}, u32[]{:S(2)}, u32[]{:S(2)}) collective-permute-start(bf16[528,128]{1,0:T(8,128)(2,1)S(1)} %shard_map.172), channel_id=1, source_target_pairs={{0,16},{8,24},{16,0},{24,8},{1,17},{9,25},{17,1},{25,9},{2,18},{10... | collective-permute-start | bytes 405512 | tf_op jit(solution)/shard_map/ppermute | solution.py:325
  47.2 4.8 %collective-permute-start.13 = (bf16[160,128]{1,0:T(8,128)(2,1)S(1)}, bf16[160,128]{1,0:T(8,128)(2,1)S(1)}, u32[]{:S(2)}, u32[]{:S(2)}) collective-permute-start(bf16[160,128]{1,0:T(8,128)(2,1)S(1)} %get-tuple-element.25.refs_0_), channel_id=1, source_target_pairs={{0,16},{8,24},{16,0},{24,8},{1,17},{9,25},{17,1},{25,9},{2,18},{10... | collective-permute-start | bytes 122888 | tf_op jit(solution)/shard_map/ppermute | solution.py:325
  49.0 20.3 %copy-start = (bf16[512,4096]{1,0:T(8,128)(2,1)S(1)}, bf16[512,4096]{1,0:T(8,128)(2,1)}, u32[]{:S(2)}) copy-start(bf16[512,4096]{1,0:T(8,128)(2,1)} %refs_2_.3) | copy-start | bytes 12582916
  52.0 1.4 %collective-permute-start.14 = (bf16[160,128]{1,0:T(8,128)(2,1)S(1)}, bf16[160,128]{1,0:T(8,128)(2,1)S(1)}, u32[]{:S(2)}, u32[]{:S(2)}) collective-permute-start(bf16[160,128]{1,0:T(8,128)(2,1)S(1)} %collective-permute-done.13.refs_2_), channel_id=1, source_target_pairs={{0,8},{8,0},{16,24},{24,16},{1,9},{9,1},{17,25},{25,17},{2,10},{10... | collective-permute-start | bytes 122888 | tf_op jit(solution)/shard_map/ppermute | solution.py:325
  54.2 19.8 %copy-start.6 = (bf16[128,512]{1,0:T(8,128)(2,1)S(1)}, bf16[128,512]{1,0:T(8,128)(2,1)}, u32[]{:S(2)}) copy-start(bf16[128,512]{1,0:T(8,128)(2,1)} %refs_4_.3) | copy-start | bytes 393220
  54.2 8.8 %collective-permute-start.21 = (bf16[128,512]{1,0:T(8,128)(2,1)S(1)}, bf16[128,512]{1,0:T(8,128)(2,1)S(1)}, u32[]{:S(2)}, u32[]{:S(2)}) collective-permute-start(bf16[128,512]{1,0:T(8,128)(2,1)S(1)} %get-tuple-element.35.refs_0_), channel_id=1, source_target_pairs={{0,2},{1,3},{2,0},{3,1},{4,6},{5,7},{6,4},{7,5},{8,10},{9,11},{10,... | collective-permute-start | bytes 393224 | tf_op jit(solution)/shard_map/ppermute | solution.py:325
  55.6 10.3 %collective-permute-start.16 = (bf16[128,512]{1,0:T(8,128)(2,1)S(1)}, bf16[128,512]{1,0:T(8,128)(2,1)S(1)}, u32[]{:S(2)}, u32[]{:S(2)}) collective-permute-start(bf16[128,512]{1,0:T(8,128)(2,1)S(1)} %get-tuple-element.35.refs_0_), channel_id=1, source_target_pairs={{0,4},{1,5},{2,6},{3,7},{4,0},{5,1},{6,2},{7,3},{8,12},{9,13},{10,... | collective-permute-start | bytes 393224 | tf_op jit(solution)/shard_map/ppermute | solution.py:325
  57.9 9.6 %collective-permute-start.20 = (bf16[128,512]{1,0:T(8,128)(2,1)S(1)}, bf16[128,512]{1,0:T(8,128)(2,1)S(1)}, u32[]{:S(2)}, u32[]{:S(2)}) collective-permute-start(bf16[128,512]{1,0:T(8,128)(2,1)S(1)} %get-tuple-element.35.refs_0_), channel_id=1, source_target_pairs={{0,1},{1,0},{2,3},{3,2},{4,5},{5,4},{6,7},{7,6},{8,9},{9,8},{10,11... | collective-permute-start | bytes 393224 | tf_op jit(solution)/shard_map/ppermute | solution.py:325
  62.9 6.4 %collective-permute-start.22 = (bf16[128,512]{1,0:T(8,128)(2,1)S(1)}, bf16[128,512]{1,0:T(8,128)(2,1)S(1)}, u32[]{:S(2)}, u32[]{:S(2)}) collective-permute-start(bf16[128,512]{1,0:T(8,128)(2,1)S(1)} %collective-permute-done.21.refs_2_), channel_id=1, source_target_pairs={{0,1},{1,0},{2,3},{3,2},{4,5},{5,4},{6,7},{7,6},{8,9},{9,8},{10,11... | collective-permute-start | bytes 393224 | tf_op jit(solution)/shard_map/ppermute | solution.py:325
  64.7 8.9 %collective-permute-start.19 = (bf16[128,512]{1,0:T(8,128)(2,1)S(1)}, bf16[128,512]{1,0:T(8,128)(2,1)S(1)}, u32[]{:S(2)}, u32[]{:S(2)}) collective-permute-start(bf16[128,512]{1,0:T(8,128)(2,1)S(1)} %get-tuple-element.35.refs_0_), channel_id=1, source_target_pairs={{0,7},{1,6},{2,5},{3,4},{4,3},{5,2},{6,1},{7,0},{8,15},{9,14},{10,... | collective-permute-start | bytes 393224 | tf_op jit(solution)/shard_map/ppermute | solution.py:325
  65.9 8.1 %collective-permute-start.18 = (bf16[128,512]{1,0:T(8,128)(2,1)S(1)}, bf16[128,512]{1,0:T(8,128)(2,1)S(1)}, u32[]{:S(2)}, u32[]{:S(2)}) collective-permute-start(bf16[128,512]{1,0:T(8,128)(2,1)S(1)} %collective-permute-done.16.refs_4_), channel_id=1, source_target_pairs={{0,2},{1,3},{2,0},{3,1},{4,6},{5,7},{6,4},{7,5},{8,10},{9,11},{10,... | collective-permute-start | bytes 393224 | tf_op jit(solution)/shard_map/ppermute | solution.py:325
  65.9 8.1 %collective-permute-start.17 = (bf16[128,512]{1,0:T(8,128)(2,1)S(1)}, bf16[128,512]{1,0:T(8,128)(2,1)S(1)}, u32[]{:S(2)}, u32[]{:S(2)}) collective-permute-start(bf16[128,512]{1,0:T(8,128)(2,1)S(1)} %collective-permute-done.16.refs_4_), channel_id=1, source_target_pairs={{0,1},{1,0},{2,3},{3,2},{4,5},{5,4},{6,7},{7,6},{8,9},{9,8},{10,11... | collective-permute-start | bytes 393224 | tf_op jit(solution)/shard_map/ppermute | solution.py:325
